TPU v7x, 256 devices: a whole 4x4x8 slice. The times are simulated.
256 devices in a mesh: sp: 64 (over z, y, core), tp: 4 (over x).
Axes of the slice: x: 4, y: 4, z: 8, core: 2. Of those that a mesh axis runs over, the one named last changes fastest.
Arguments:
- expert_in: bfloat16 [8192, 2048], P('sp'), may hold values from -6 to 6
- out_cot: bfloat16 [8192, 2048], P('sp'), may hold values from -16 to 16
- route_ids: int32 [8192, 2], P('sp'), may hold values from 0 to 63, all different within a row; in each aligned block of 128 rows (0 to 127, 128 to 255, ...) at most 8 rows name the same one
- route_weights: float32 [8192, 2], P('sp'), may hold values from 0.1 to 1
- w_gate: bfloat16 [64, 2048, 1024], P('sp', None, 'tp'), may hold values from -0.125 to 0.125
- w_up: bfloat16 [64, 2048, 1024], P('sp', None, 'tp'), may hold values from -0.125 to 0.125
- w_down: bfloat16 [64, 1024, 2048], P('sp', 'tp'), may hold values from -0.1875 to 0.1875
- w_out: bfloat16 [2048, 1024], P(None, 'tp'), may hold values from -0.1875 to 0.1875
- mixed_heads: bfloat16 [8192, 1024], P('sp', 'tp'), may hold values from -6 to 6
- queries: bfloat16 [8192, 512], P('sp', 'tp'), may hold values from -0.5 to 0.5
- keys: bfloat16 [8192, 512], P('sp', 'tp'), may hold values from -0.3125 to 0.3125
- values: bfloat16 [8192, 1024], P('sp', 'tp'), may hold values from -6 to 6
- log_decay: float32 [8192, 512], P('sp', 'tp'), may hold values from -0.3 to 0
Outputs:
- grad_gate: float32 [64, 2048, 1024], P('sp', None, 'tp')
- grad_up: float32 [64, 2048, 1024], P('sp', None, 'tp')
- grad_down: float32 [64, 1024, 2048], P('sp', 'tp')
- grad_out_proj: float32 [2048, 1024], P('sp', 'tp')
- grad_queries: bfloat16 [8192, 512], P('sp', 'tp')
- grad_keys: bfloat16 [8192, 512], P('sp', 'tp')
- grad_values: bfloat16 [8192, 1024], P('sp', 'tp')
- grad_decay: float32 [8192, 512], P('sp', 'tp')
Inputs may be any that keep to these rules, and one draw needn't show every extreme that they name: `route_ids`: in the rows of one device no expert is named more than 8 times, a bound that some block reaches.
All inputs are finite; a program needn't handle non-finite values.
Results may differ from a plain program's by a relative error of at most 0.015.
Values may be sent and summed in bfloat16 or wider, within the bound.
No kernel may reach another device: no remote copies, remote signals or barrier semaphores. Data moves between devices by JAX's collectives and lax.ppermute only.
A program may use at most 128 MiB of HBM per device.

v0:
```python
import jax
import jax.numpy as jnp
from jax import lax
from jax.sharding import Mesh
from jax.sharding import PartitionSpec as P

DK = 128
BLK = 128
SP = ("sp_0", "sp_1", "sp_2")


exact_mode = lax.Precision.HIGHEST


def in_blocks(shard, dim, peers):
    lengths = shard.shape
    tiles = shard.reshape(*lengths[:dim], peers, lengths[dim] // peers, *lengths[dim + 1 :])
    return jnp.moveaxis(tiles, dim, 0)


def sent_and_summed(shard, axis, dim):
    peers = lax.axis_size(axis)
    tiles = lax.all_to_all(in_blocks(shard, dim, peers), axis, 0, 0, tiled=True)
    return jnp.sum(tiles.astype(jnp.float32), axis=0)


def neutral_like(shard, identity):
    return jax.tree.map(
        lambda a, e: jnp.broadcast_to(jnp.asarray(e, a.dtype), a.shape), shard, identity
    )


def carried_in(shard, axes, combine, identity, reverse):
    before = start = neutral_like(shard, identity)
    running = shard
    for axis in reversed(axes):
        peers, place = (lax.axis_size(axis), lax.axis_index(axis))
        pieces = jax.tree.map(lambda part: lax.all_gather(part, axis), running)
        inside, running = (start, start)
        for k in reversed(range(peers)) if reverse else range(peers):
            passed = k > place if reverse else k < place
            running = combine(running, jax.tree.map(lambda part: part[k], pieces))
            inside = jax.tree.map(lambda new, old: jnp.where(passed, new, old), running, inside)
        before = combine(inside, before)
    return before


def block_forward(query_blocks, key_blocks, value_blocks, decay_blocks, state_start):
    block_len = query_blocks.shape[1]
    cumulative = jnp.cumsum(decay_blocks, axis=1)
    block_sum = cumulative[:, -1]
    query_decayed = query_blocks * jnp.exp(cumulative)
    key_grown = key_blocks * jnp.exp(-cumulative)
    key_to_end = key_blocks * jnp.exp(block_sum[:, None] - cumulative)
    causal = jnp.tril(jnp.ones((block_len, block_len), dtype=bool))
    scores = jnp.einsum("nchd,nshd->nhcs", query_decayed, key_grown, precision=exact_mode)
    scores = jnp.where(causal, scores, 0.0)
    intra_out = jnp.einsum("nhcs,nshe->nche", scores, value_blocks, precision=exact_mode)

    def advance(state_now, block):
        query_part, key_part, value_part, sum_part = block
        carried = jnp.einsum("chd,hde->che", query_part, state_now, precision=exact_mode)
        state_now = state_now * jnp.exp(sum_part)[..., None] + jnp.einsum(
            "chd,che->hde", key_part, value_part, precision=exact_mode
        )
        return (state_now, carried)

    final_state, carried_out = lax.scan(
        advance, state_start, (query_decayed, key_to_end, value_blocks, block_sum)
    )
    return (intra_out + carried_out, final_state)


def compose(earlier, later):
    return (earlier[0] * later[0], later[0][..., None] * earlier[1] + later[1])


def per_device(
    expert_in,
    out_cot,
    route_ids,
    route_weights,
    w_gate,
    w_up,
    w_down,
    w_out,
    mixed_heads,
    queries,
    keys,
    values,
    log_decay,
):
    n_sp = lax.axis_size(SP)
    n_tp = lax.axis_size("tp")
    tok_dev, width = expert_in.shape
    top_count = route_ids.shape[1]
    exp_dev = w_gate.shape[0]
    experts = exp_dev * n_sp
    capacity = 2 * top_count * tok_dev // experts
    assigned = tok_dev * top_count
    flat_ids = route_ids.reshape(-1)
    onehot = (flat_ids[:, None] == jnp.arange(experts, dtype=jnp.int32)).astype(jnp.int32)
    slot_rank = jnp.sum((jnp.cumsum(onehot, axis=0) - 1) * onehot, axis=1)
    slot_index = flat_ids * capacity + slot_rank
    owners = (
        jnp.full((experts * capacity,), assigned, jnp.int32)
        .at[slot_index]
        .set(jnp.arange(assigned, dtype=jnp.int32))
    )
    is_live = owners < assigned
    owner_safe = jnp.where(is_live, owners, 0)
    owner_token = owner_safe // top_count
    x_rows = jnp.where(
        is_live[:, None], jnp.take(expert_in, owner_token, axis=0), jnp.zeros((), jnp.bfloat16)
    )
    slot_weight = jnp.where(is_live, route_weights.reshape(-1)[owner_safe], 0.0)
    dy_rows = (
        slot_weight[:, None] * jnp.take(out_cot, owner_token, axis=0).astype(jnp.float32)
    ).astype(jnp.bfloat16)
    share_rows = capacity // n_tp
    tp_index = lax.axis_index("tp")

    def take_share(rows):
        grid = rows.reshape(experts, capacity, width)
        picked = lax.dynamic_slice_in_dim(grid, tp_index * share_rows, share_rows, 1)
        return picked.reshape(experts * share_rows, width)

    got_x, got_dy = (
        lax.all_to_all(take_share(x_rows), SP, split_axis=0, concat_axis=0, tiled=True),
        lax.all_to_all(take_share(dy_rows), SP, split_axis=0, concat_axis=0, tiled=True),
    )
    got_x, got_dy = (
        lax.all_gather(got_x.reshape(n_sp * exp_dev, share_rows, width), "tp", axis=1, tiled=True),
        lax.all_gather(got_dy.reshape(n_sp * exp_dev, share_rows, width), "tp", axis=1, tiled=True),
    )

    def per_expert_rows(rows):
        return (
            rows.reshape(n_sp, exp_dev, capacity, width)
            .swapaxes(0, 1)
            .reshape(exp_dev, n_sp * capacity, width)
        )

    got_x = per_expert_rows(got_x)
    got_dy = per_expert_rows(got_dy)
    gate_pre = jnp.einsum("esd,edf->esf", got_x, w_gate, preferred_element_type=jnp.float32)
    up_pre = jnp.einsum("esd,edf->esf", got_x, w_up, preferred_element_type=jnp.float32)
    sigmoid_gate = jax.nn.sigmoid(gate_pre)
    hidden = (gate_pre * sigmoid_gate * up_pre).astype(jnp.bfloat16)
    hidden_cot = jnp.einsum("esd,efd->esf", got_dy, w_down, preferred_element_type=jnp.float32)
    grad_down = jnp.einsum("esf,esd->efd", hidden, got_dy, preferred_element_type=jnp.float32)
    gate_cot = (
        hidden_cot * up_pre * sigmoid_gate * (1.0 + gate_pre * (1.0 - sigmoid_gate))
    ).astype(jnp.bfloat16)
    up_cot = (hidden_cot * gate_pre * sigmoid_gate).astype(jnp.bfloat16)
    grad_gate = jnp.einsum("esd,esf->edf", got_x, gate_cot, preferred_element_type=jnp.float32)
    grad_up = jnp.einsum("esd,esf->edf", got_x, up_cot, preferred_element_type=jnp.float32)
    partial_value = jnp.einsum("esf,edf->esd", gate_cot, w_gate, preferred_element_type=jnp.float32)
    partial_value = partial_value + jnp.einsum(
        "esf,edf->esd", up_cot, w_up, preferred_element_type=jnp.float32
    )
    partial_value = (
        partial_value.reshape(exp_dev, n_sp, capacity, width)
        .swapaxes(0, 1)
        .reshape(n_sp * exp_dev, capacity, width)
    )
    shared = lax.psum_scatter(
        partial_value.astype(jnp.bfloat16), "tp", scatter_dimension=1, tiled=True
    )
    returned = lax.all_to_all(
        shared.reshape(n_sp * exp_dev * share_rows, width),
        SP,
        split_axis=0,
        concat_axis=0,
        tiled=True,
    )
    returned = lax.all_gather(
        returned.reshape(experts, share_rows, width), "tp", axis=1, tiled=True
    )
    returned = returned.reshape(experts * capacity, width)
    per_choice = (
        jnp.take(returned, slot_index, axis=0)
        .astype(jnp.float32)
        .reshape(tok_dev, top_count, width)
    )
    mid_cot = (out_cot.astype(jnp.float32) + jnp.sum(per_choice, axis=1)).astype(jnp.bfloat16)
    head_cot = jnp.dot(mid_cot, w_out, preferred_element_type=jnp.float32)
    grad_out_proj = sent_and_summed(
        jnp.einsum("td,te->de", mid_cot, mixed_heads, preferred_element_type=jnp.float32).astype(
            jnp.bfloat16
        ),
        SP,
        0,
    )
    heads_dev = queries.shape[1] // DK
    value_width = values.shape[1] // heads_dev
    query_heads = queries.astype(jnp.float32).reshape(tok_dev, heads_dev, DK)
    key_heads = keys.astype(jnp.float32).reshape(tok_dev, heads_dev, DK)
    value_heads = values.astype(jnp.float32).reshape(tok_dev, heads_dev, value_width)
    cumulative = jnp.cumsum(log_decay.reshape(tok_dev, heads_dev, DK), axis=0)
    decay_sum = cumulative[-1]
    state_local = jnp.einsum(
        "thd,the->hde",
        key_heads * jnp.exp(decay_sum[None] - cumulative),
        value_heads,
        precision=exact_mode,
    )
    decay_all = jnp.exp(decay_sum)
    identity = (jnp.ones_like(decay_all), jnp.zeros_like(state_local))
    _, state_in = carried_in((decay_all, state_local), SP, compose, identity, False)
    cot_heads = head_cot.reshape(tok_dev, heads_dev, value_width)
    state_pull = jnp.einsum(
        "thd,the->hde", query_heads * jnp.exp(cumulative), cot_heads, precision=exact_mode
    )
    _, state_cot = carried_in((decay_all, state_pull), SP, compose, identity, True)
    blocks = tok_dev // BLK

    def local_pass(query_in, key_in, value_in, decay_in, state_start):
        out, final_state = block_forward(
            query_in.astype(jnp.float32).reshape(blocks, BLK, heads_dev, DK),
            key_in.astype(jnp.float32).reshape(blocks, BLK, heads_dev, DK),
            value_in.astype(jnp.float32).reshape(blocks, BLK, heads_dev, value_width),
            decay_in.reshape(blocks, BLK, heads_dev, DK),
            state_start,
        )
        return (out.reshape(tok_dev, heads_dev * value_width), final_state)

    _, pull_back = jax.vjp(local_pass, queries, keys, values, log_decay, state_in)
    grad_queries, grad_keys, grad_values, grad_decay, _ = pull_back((head_cot, state_cot))
    return (
        grad_gate,
        grad_up,
        grad_down,
        grad_out_proj,
        grad_queries,
        grad_keys,
        grad_values,
        grad_decay,
    )


def solution(mesh):
    finer = Mesh(mesh.devices.reshape(8, 4, 2, mesh.shape["tp"]), ("sp_0", "sp_1", "sp_2", "tp"))
    placed = (
        P(SP, None),
        P(SP, None),
        P(SP, None),
        P(SP, None),
        P(SP, None, "tp"),
        P(SP, None, "tp"),
        P(SP, "tp", None),
        P(None, "tp"),
        P(SP, "tp"),
        P(SP, "tp"),
        P(SP, "tp"),
        P(SP, "tp"),
        P(SP, "tp"),
    )
    return jax.shard_map(
        per_device,
        mesh=finer,
        in_specs=placed,
        out_specs=(
            P(SP, None, "tp"),
            P(SP, None, "tp"),
            P(SP, "tp", None),
            P(SP, "tp"),
            P(SP, "tp"),
            P(SP, "tp"),
            P(SP, "tp"),
            P(SP, "tp"),
        ),
        check_vma=False,
    )
```

profile of v0, /device:TPU:2, one launch (start us, length us, event | category | flops | bytes accessed | tf_op | source)
XLA Modules:
  0.0 348.3 jit_solution(4285810463334410374)
XLA Ops:
  11.8 3.3 gather_fusion.2
  15.1 1.9 fusion.11
  17.6 29.5 %all_to_all.23 = bf16[64,2,2048]{2,1,0:T(2,128)(2,1)S(1)} all-to-all(bf16[64,2,2048]{2,1,0:T(2,128)(2,1)S(1)} %constant_dynamic-slice_fusion.1), channel_id=1, replica_groups=mesh['sp_0'=8,'sp_1'=4,'sp_2'=2,'tp'=4] {'sp_0','sp_1','sp_2'}, dimensions={0} | all-to-all | bytes 1048576 | tf_op jit(solution)/shard_map/all_to_all | solution.py:129
  48.2 3.3 gather_fusion.3
  51.7 3.5 %gather_fusion = f32[512]{0:T(512)S(1)} fusion(f32[256]{0:T(256)S(1)} %reshape.3199, s32[1024]{0:T(1024)S(1)} %pad_clamp_fusion.1), kind=kCustom, calls=%fused_computation.2 | custom fusion | bytes 6144 | tf_op jit(solution)/shard_map/gather | solution.py:116
  55.3 2.3 fusion.1
  58.1 23.1 %all_to_all.24 = bf16[64,2,2048]{2,1,0:T(2,128)(2,1)S(1)} all-to-all(bf16[64,2,2048]{2,1,0:T(2,128)(2,1)S(1)} %constant_dynamic-slice_fusion), channel_id=1, replica_groups=mesh['sp_0'=8,'sp_1'=4,'sp_2'=2,'tp'=4] {'sp_0','sp_1','sp_2'}, dimensions={0} | all-to-all | bytes 1048576 | tf_op jit(solution)/shard_map/all_to_all | solution.py:130
  82.4 3.0 fusion.7
  85.5 2.1 fusion.9
  87.5 25.5 %all-gather.10.cloned.1.call-done = bf16[64,8,2048]{2,0,1:T(8,128)(2,1)} async-done(((bf16[64,2,2048]{2,0,1:T(8,128)(2,1)}), bf16[64,8,2048]{2,0,1:T(8,128)(2,1)}) %all-gather.10.cloned.1.call-update) | async-done | bytes 2097168 | tf_op jit(solution)/shard_map/all_gather | solution.py:134
  113.0 3.5 %multiply_convert_fusion.2 = (bf16[512,256]{1,0:T(8,128)(2,1)S(1)}, bf16[512,256]{1,0:T(8,128)(2,1)S(1)}) fusion(f32[512,256]{1,0:T(8,128)S(1)} %fusion.7, f32[512,256]{1,0:T(8,128)} %fusion.9, bf16[1,256,2048]{2,1,0:T(8,128)(2,1)} %param.21, bf16[64,8,2048]{2,0,1:T(8,128)(2,1)} %all-gather.10.cloned.1.call-done), kind=kOutput, calls=%fused_computation.51 | convolution fusion | flops 538574848 | bytes 4718592 | tf_op jit(solution)/shard_map/esd,efd->esf/dot_general | solution.py:150
  118.1 2.5 copy.101
  120.7 32.1 %reduce-scatter.2.cloned.1.call-done = bf16[64,2,2048]{2,0,1:T(8,128)(2,1)} async-done(((bf16[64,8,2048]{2,0,1:T(8,128)(2,1)}), bf16[64,2,2048]{2,0,1:T(8,128)(2,1)}) %reduce-scatter.2.cloned.1.call-update) | async-done | bytes 524304 | tf_op jit(solution)/shard_map/reduce_scatter | solution.py:167
  154.3 27.9 %all_to_all.25 = bf16[64,2,2048]{2,1,0:T(2,128)(2,1)S(1)} all-to-all(bf16[64,2,2048]{2,1,0:T(2,128)(2,1)S(1)} %copy.102), channel_id=1, replica_groups=mesh['sp_0'=8,'sp_1'=4,'sp_2'=2,'tp'=4] {'sp_0','sp_1','sp_2'}, dimensions={0} | all-to-all | bytes 1048576 | tf_op jit(solution)/shard_map/all_to_all | solution.py:170
  186.1 9.7 %all_gather.61 = f32[4,1,128]{2,1,0:T(1,128)S(1)} all-gather(f32[1,1,128]{2,1,0:T(1,128)S(1)} %get-tuple-element.164), channel_id=1, replica_groups=mesh['sp_0'=8,'sp_1'=4,'sp_2'=2,'tp'=4] {'sp_1'}, dimensions={0}, use_global_device_ids=true | all-gather | bytes 2560 | tf_op jit(solution)/shard_map/all_gather | solution.py:38
  196.1 2.0 all-gather
  198.9 14.4 %all_gather.65 = f32[4,1,128,256]{3,2,1,0:T(8,128)} all-gather(f32[1,1,128,256]{3,2,1,0:T(8,128)S(1)} %bitcast_add_fusion.56), channel_id=1, replica_groups=mesh['sp_0'=8,'sp_1'=4,'sp_2'=2,'tp'=4] {'sp_1'}, dimensions={0}, use_global_device_ids=true | all-gather | bytes 655360 | tf_op jit(solution)/shard_map/all_gather | solution.py:38
  213.9 4.1 %copy.140 = bf16[64,8,2048]{2,1,0:T(8,128)(2,1)} copy(bf16[64,8,2048]{2,0,1:T(8,128)(2,1)} %all-gather.12.cloned.1.call-done) | data formatting | bytes 4194304 | tf_op jit(solution)/shard_map/all_gather | solution.py:177
  218.0 4.2 %gather_fusion.1 = bf16[256,2048]{1,0:T(8,128)(2,1)S(1)} fusion(bf16[512,2048]{1,0:T(8,128)(2,1)} %bitcast.535, s32[1024]{0:T(1024)S(1)} %pad_clamp_fusion), kind=kCustom, calls=%fused_computation.3 | custom fusion | bytes 2098176 | tf_op jit(solution)/shard_map/jit(_take)/gather | solution.py:182
  223.7 5.2 %convert_reduce_fusion.1 = f32[128,2048]{1,0:T(8,128)S(1)} fusion(bf16[128,2,2048]{2,1,0:T(2,128)(2,1)} %gather.14, pred[128,2]{1,0:T(8,128)(4,1)S(1)} %copy.100), kind=kLoop, calls=%fused_computation.26 | loop fusion | flops 1310720 | bytes 2097408 | tf_op jit(solution)/shard_map/reduce_sum | solution.py:186
  229.7 2.0 all-gather.1
  231.8 13.5 %all_gather.70 = f32[4,1,128,256]{3,2,1,0:T(8,128)S(1)} all-gather(f32[1,1,128,256]{3,2,1,0:T(8,128)S(1)} %bitcast_add_fusion.40), channel_id=1, replica_groups=mesh['sp_0'=8,'sp_1'=4,'sp_2'=2,'tp'=4] {'sp_1'}, dimensions={0}, use_global_device_ids=true | all-gather | bytes 655360 | tf_op jit(solution)/shard_map/all_gather | solution.py:38
  246.4 14.4 %all_gather.67 = f32[8,1,128]{2,1,0:T(1,128)S(1)} all-gather(f32[1,1,128]{2,1,0:T(1,128)S(1)} %copy-done.43), channel_id=1, replica_groups=mesh['sp_0'=8,'sp_1'=4,'sp_2'=2,'tp'=4] {'sp_0'}, dimensions={0}, use_global_device_ids=true | all-gather | bytes 4608 | tf_op jit(solution)/shard_map/all_gather | solution.py:38
  260.7 14.5 %all_gather.62 = f32[8,1,128]{2,1,0:T(1,128)S(1)} all-gather(f32[1,1,128]{2,1,0:T(1,128)S(1)} %copy-done.42), channel_id=1, replica_groups=mesh['sp_0'=8,'sp_1'=4,'sp_2'=2,'tp'=4] {'sp_0'}, dimensions={0}, use_global_device_ids=true | all-gather | bytes 4608 | tf_op jit(solution)/shard_map/all_gather | solution.py:38
  279.4 4.5 %convolution_bitcast_fusion.1 = f32[1,2048,256]{2,1,0:T(8,128)} fusion(bf16[512,256]{1,0:T(8,128)(2,1)} %copy-done.22, bf16[64,8,2048]{2,0,1:T(8,128)(2,1)} %all-gather.8.cloned.1.call-done), kind=kOutput, calls=%fused_computation.9 | convolution fusion | flops 536870912 | bytes 4456448 | tf_op jit(solution)/shard_map/esd,esf->edf/dot_general | solution.py:157
  284.0 4.7 %convolution_bitcast_fusion.2 = f32[1,2048,256]{2,1,0:T(8,128)} fusion(bf16[512,256]{1,0:T(8,128)(2,1)} %copy-done.21, bf16[64,8,2048]{2,0,1:T(8,128)(2,1)} %all-gather.8.cloned.1.call-done), kind=kOutput, calls=%fused_computation.10 | convolution fusion | flops 536870912 | bytes 4456448 | tf_op jit(solution)/shard_map/esd,esf->edf/dot_general | solution.py:156
  288.7 2.9 convolution_bitcast_fusion
  293.1 8.4 %all-to-all-start.3 = ((bf16[64,32,256]{2,1,0:T(8,128)(2,1)}), bf16[64,32,256]{2,1,0:T(8,128)(2,1)S(1)}, u32[]{:S(2)}, u32[]{:S(2)}) async-start(bf16[64,32,256]{2,1,0:T(8,128)(2,1)} %bitcast.544), calls=%async_computation.4 | async-start | bytes 2097152 | tf_op jit(solution)/shard_map/all_to_all | solution.py:23
  302.7 2.0 convolution_bitcast_fusion.3
  308.0 1.9 fusion.20
  311.5 20.5 %all-gather.14.cloned.1.call-done = f32[8,1,128,256]{3,2,1,0:T(8,128)} async-done(((f32[1,1,128,256]{3,2,1,0:T(8,128)}), f32[8,1,128,256]{3,2,1,0:T(8,128)}) %all-gather.14.cloned.1.call-update) | async-done | bytes 1048592 | tf_op jit(solution)/shard_map/all_gather | solution.py:38
  332.0 2.2 fusion.30
  (182 shorter events, 38.6 us)
Async XLA Ops:
  7.2 75.2 %copy-start = (bf16[1,2048,256]{2,1,0:T(8,128)(2,1)S(1)}, bf16[1,2048,256]{2,1,0:T(8,128)(2,1)}, u32[]{:S(2)}) copy-start(bf16[1,2048,256]{2,1,0:T(8,128)(2,1)} %param.19) | copy-start | bytes 3145732
  7.2 75.2 %all-gather.8.cloned.1.call-start = ((), (), s32[]{:S(2)}) async-start(), calls=%async_computation.5 | async-start | bytes 2621440 | tf_op jit(solution)/shard_map/all_gather | solution.py:133
  17.0 31.1 %copy-start.1 = (bf16[128,2048]{1,0:T(8,128)(2,1)S(1)}, bf16[128,2048]{1,0:T(8,128)(2,1)}, u32[]{:S(2)}) copy-start(bf16[128,2048]{1,0:T(8,128)(2,1)} %param.16) | copy-start | bytes 1572868
  48.1 64.9 %all-gather.10.cloned.1.call-start = ((), (), s32[]{:S(2)}) async-start(), calls=%async_computation.6 | async-start | bytes 2621440 | tf_op jit(solution)/shard_map/all_gather | solution.py:134
  82.1 70.6 %reduce-scatter.2.cloned.1.call-start = ((), (), s32[]{:S(2)}) async-start(), calls=%async_computation.7 | async-start | bytes 2621440 | tf_op jit(solution)/shard_map/reduce_scatter | solution.py:167
  85.5 27.5 %copy-start.47 = (f32[512,256]{1,0:T(8,128)}, f32[512,256]{1,0:T(8,128)S(1)}, u32[]{:S(2)}) copy-start(f32[512,256]{1,0:T(8,128)S(1)} %fusion.7) | copy-start | bytes 1572868
  120.6 62.9 %copy-start.26 = (s32[128,2]{0,1:T(2,128)S(1)}, s32[128,2]{0,1:T(2,128)}, u32[]{:S(2)}) copy-start(s32[128,2]{0,1:T(2,128)} %param.17) | copy-start | bytes 3076
  120.6 63.1 %copy-start.20 = (f32[128,128]{1,0:T(8,128)S(1)}, f32[128,128]{1,0:T(8,128)}, u32[]{:S(2)}) copy-start(f32[128,128]{1,0:T(8,128)} %param.27) | copy-start | bytes 196612
  120.6 75.2 %copy-start.11 = (bf16[128,128]{1,0:T(8,128)(2,1)S(1)}, bf16[128,128]{1,0:T(8,128)(2,1)}, u32[]{:S(2)}) copy-start(bf16[128,128]{1,0:T(8,128)(2,1)} %param.25) | copy-start | bytes 98308
  120.6 75.2 %copy-start.16 = (bf16[128,256]{1,0:T(8,128)(2,1)S(1)}, bf16[128,256]{1,0:T(8,128)(2,1)}, u32[]{:S(2)}) copy-start(bf16[128,256]{1,0:T(8,128)(2,1)} %param.26) | copy-start | bytes 196612
  120.6 93.3 %all-gather.12.cloned.1.call-start = ((), (), s32[]{:S(2)}) async-start(), calls=%async_computation.8 | async-start | bytes 2621440 | tf_op jit(solution)/shard_map/all_gather | solution.py:177
  183.2 122.4 %all-gather.16.cloned.1.call-start = ((), (), s32[]{:S(2)}) async-start(), calls=%async_computation.10 | async-start | bytes 1179648 | tf_op jit(solution)/shard_map/all_gather | solution.py:38
  185.6 32.4 %copy-start.27 = (f32[2,1,128]{2,1,0:T(1,128)}, f32[2,1,128]{2,1,0:T(1,128)S(1)}, u32[]{:S(2)}) copy-start(f32[2,1,128]{2,1,0:T(1,128)S(1)} %all_gather.60) | copy-start | bytes 3076
  186.1 31.9 %copy-start.38 = (f32[128]{0:T(128)}, f32[128]{0:T(128)S(1)}, u32[]{:S(2)}) copy-start(f32[128]{0:T(128)S(1)} %get-tuple-element.165) | copy-start | bytes 1540
  195.8 22.2 %copy-start.24 = (f32[4,1,128]{2,1,0:T(1,128)}, f32[4,1,128]{2,1,0:T(1,128)S(1)}, u32[]{:S(2)}) copy-start(f32[4,1,128]{2,1,0:T(1,128)S(1)} %all_gather.61) | copy-start | bytes 6148
  198.7 19.3 %copy-start.40 = (f32[128]{0:T(128)}, f32[128]{0:T(128)S(1)}, u32[]{:S(2)}) copy-start(f32[128]{0:T(128)S(1)} %get-tuple-element.159) | copy-start | bytes 1540
  229.0 16.4 %copy-start.3 = (f32[4,1,128,256]{3,2,1,0:T(8,128)S(1)}, f32[4,1,128,256]{3,2,1,0:T(8,128)}, u32[]{:S(2)}) copy-start(f32[4,1,128,256]{3,2,1,0:T(8,128)} %all_gather.65) | copy-start | bytes 1572868
  229.0 16.3 %copy-start.30 = (f32[128]{0:T(128)S(1)}, f32[128]{0:T(128)}, u32[]{:S(2)}) copy-start(f32[128]{0:T(128)} %get-tuple-element.157) | copy-start | bytes 1540
  229.0 16.3 %copy-start.33 = (f32[128]{0:T(128)S(1)}, f32[128]{0:T(128)}, u32[]{:S(2)}) copy-start(f32[128]{0:T(128)} %get-tuple-element.154) | copy-start | bytes 1540
  229.0 16.3 %copy-start.35 = (f32[128]{0:T(128)S(1)}, f32[128]{0:T(128)}, u32[]{:S(2)}) copy-start(f32[128]{0:T(128)} %get-tuple-element.155) | copy-start | bytes 1540
  229.0 16.3 %copy-start.36 = (f32[128]{0:T(128)S(1)}, f32[128]{0:T(128)}, u32[]{:S(2)}) copy-start(f32[128]{0:T(128)} %get-tuple-element.156) | copy-start | bytes 1540
  229.0 16.3 %copy-start.39 = (f32[128]{0:T(128)S(1)}, f32[128]{0:T(128)}, u32[]{:S(2)}) copy-start(f32[128]{0:T(128)} %get-tuple-element.158) | copy-start | bytes 1540
  229.0 16.3 %copy-start.41 = (f32[128]{0:T(128)S(1)}, f32[128]{0:T(128)}, u32[]{:S(2)}) copy-start(f32[128]{0:T(128)} %get-tuple-element.153) | copy-start | bytes 1540
  229.4 16.9 %copy-start.8 = (f32[128,256]{1,0:T(8,128)}, f32[128,256]{1,0:T(8,128)S(1)}, u32[]{:S(2)}) copy-start(f32[128,256]{1,0:T(8,128)S(1)} %fusion.165) | copy-start | bytes 393220
  229.4 45.9 %copy-start.25 = (f32[4,1,128]{2,1,0:T(1,128)S(1)}, f32[4,1,128]{2,1,0:T(1,128)}, u32[]{:S(2)}) copy-start(f32[4,1,128]{2,1,0:T(1,128)} %copy-done.24) | copy-start | bytes 6148
  229.4 45.9 %copy-start.28 = (f32[2,1,128]{2,1,0:T(1,128)S(1)}, f32[2,1,128]{2,1,0:T(1,128)}, u32[]{:S(2)}) copy-start(f32[2,1,128]{2,1,0:T(1,128)} %copy-done.27) | copy-start | bytes 3076
  229.7 16.6 %copy-start.43 = (f32[1,1,128]{2,1,0:T(1,128)S(1)}, f32[1,1,128]{2,1,0:T(1,128)}, u32[]{:S(2)}) copy-start(f32[1,1,128]{2,1,0:T(1,128)} %get-tuple-element.151) | copy-start | bytes 1540
  229.7 31.0 %copy-start.42 = (f32[1,1,128]{2,1,0:T(1,128)S(1)}, f32[1,1,128]{2,1,0:T(1,128)}, u32[]{:S(2)}) copy-start(f32[1,1,128]{2,1,0:T(1,128)} %get-tuple-element.152) | copy-start | bytes 1540
  246.3 85.7 %all-gather.14.cloned.1.call-start = ((), (), s32[]{:S(2)}) async-start(), calls=%async_computation.9 | async-start | bytes 1179648 | tf_op jit(solution)/shard_map/all_gather | solution.py:38
  293.1 12.5 %copy-start.34 = (f32[128]{0:T(128)S(1)}, f32[128]{0:T(128)}, u32[]{:S(2)}) copy-start(f32[128]{0:T(128)} %get-tuple-element.154) | copy-start | bytes 1540
  293.1 47.2 %all-to-all-start.3 = ((bf16[64,32,256]{2,1,0:T(8,128)(2,1)}), bf16[64,32,256]{2,1,0:T(8,128)(2,1)S(1)}, u32[]{:S(2)}, u32[]{:S(2)}) async-start(bf16[64,32,256]{2,1,0:T(8,128)(2,1)} %bitcast.544), calls=%async_computation.4 | async-start | bytes 2097152 | tf_op jit(solution)/shard_map/all_to_all | solution.py:23
  301.5 30.5 %copy-start.4 = (f32[4,1,128,256]{3,2,1,0:T(8,128)S(1)}, f32[4,1,128,256]{3,2,1,0:T(8,128)}, u32[]{:S(2)}) copy-start(f32[4,1,128,256]{3,2,1,0:T(8,128)} %all_gather.65) | copy-start | bytes 1572868
  (25 other events, 93.1 us)
Sparse Core Ops, SparseCore 0:
  48.2 28.9 all-gather.7
  82.2 30.7 all-gather.9
  120.7 32.0 reduce-scatter.1
  183.3 28.6 all-gather.11
  246.4 37.2 all-gather.15
  285.3 46.5 all-gather.13
where the time goes:
time: 355 us; the launch traced here: 348 us
  blocking collectives  153 us (43%)
  waiting for transfers between devices  78.1 us (22%)
  matrix products  36.4 us (10%)
  local copies, waits for them, and re-layouts  34.6 us (10%)
  other arithmetic  22.4 us (6%)
  between operations  15.4 us (4%)
  starting transfers between devices  8.82 us (2%)
    all_gather x8, blocking collectives, carried_in(): pieces = jax.tree.map(lambda part: lax.all_gather(part, axis), running)  72.2 us
    reduce_scatter x1, waiting for transfers between devices, per_device(): lax.psum_scatter(partial_value.astype(jnp.bfloat16), 'tp', scatter_dimens...  32.1 us
    all_to_all x1, blocking collectives, per_device(): lax.all_to_all(take_share(x_rows), SP, split_axis=0, concat_axis=0, tiled...  29.5 us
    all_to_all x1, blocking collectives, per_device(): lax.all_to_all(shared.reshape(n_sp * exp_dev * share_rows, width), SP, sp...  27.9 us
    all_gather x1, waiting for transfers between devices, per_device(): lax.all_gather(got_dy.reshape(n_sp * exp_dev, share_rows, width), 'tp', a...  25.5 us
    all_to_all x1, blocking collectives, per_device(): lax.all_to_all(take_share(dy_rows), SP, split_axis=0, concat_axis=0, tile...  23.1 us
    all_gather x2, waiting for transfers between devices, carried_in(): pieces = jax.tree.map(lambda part: lax.all_gather(part, axis), running)  20.5 us
    all_to_all x1, starting transfers between devices, sent_and_summed(): tiles = lax.all_to_all(in_blocks(shard, dim, peers), axis, 0, 0, tiled=True)  8.4 us
  transfers between devices with their start and end apart: 7, of which 3 were waited for; matrix products, arithmetic and copies ran while one was open for 15% of the time, Pallas kernels for 0%

commit v1 on v0

v1 whole, which is shorter than its diff:
```python
import functools

import jax
import jax.numpy as jnp
from jax import lax
from jax.experimental import pallas as pl
from jax.experimental.pallas import tpu as pltpu
from jax.sharding import PartitionSpec as P

BF = jnp.bfloat16
F32 = jnp.float32
HI = lax.Precision.HIGHEST

TOK = 128
EXPERTS = 64
CAP = 8
SLOTS = EXPERTS * CAP
WIDTH = 2048
QUART = 512
FF = 256
DK = 128
DV = 256
LANES = 128
HALF = 64


def dot(a, b, ca, cb, precision=None):
    return lax.dot_general(
        a, b, (((ca,), (cb,)), ((), ())), preferred_element_type=F32, precision=precision
    )


def iota(shape, dim):
    return lax.broadcasted_iota(jnp.int32, shape, dim)


def rounded(x):
    return x.astype(BF).astype(F32)


def lower_lanes(shape):
    return iota(shape, len(shape) - 1) < HALF


def call(kernel, out_shape, args, *, index=None, in_specs=None, out_specs=None, flops=0):
    nbytes = sum(a.size * a.dtype.itemsize for a in args)
    outs = jax.tree.leaves(out_shape)
    nbytes += sum(o.size * o.dtype.itemsize for o in outs)

    def whole(a):
        rank = len(a.shape)
        return pl.BlockSpec(a.shape, lambda i, q: (0,) * rank)

    specs = [whole(a) if s is None else s for a, s in zip(args, in_specs or [None] * len(args))]
    out_blocks = jax.tree.map(whole, out_shape)
    return pl.pallas_call(
        kernel,
        out_shape=out_shape,
        grid_spec=pltpu.PrefetchScalarGridSpec(
            num_scalar_prefetch=1, grid=(1,), in_specs=specs, out_specs=out_blocks
        ),
        compiler_params=pltpu.CompilerParams(vmem_limit_bytes=24 * 2**20),
        cost_estimate=pl.CostEstimate(
            flops=int(flops), bytes_accessed=int(nbytes), transcendentals=0
        ),
    )(index, *args)


def sds(shape, dtype):
    return jax.ShapeDtypeStruct(shape, dtype)


def quarter_rows(q):
    return pl.ds(pl.multiple_of(q * QUART, QUART), QUART)


def cumulative_sum(g):
    lower = (iota((TOK, TOK), 0) >= iota((TOK, TOK), 1)).astype(F32)
    return dot(lower, g, 1, 0, HI)


def tiles_of(state, fill=None):
    out = []
    for b in range(4):
        t = state[:, LANES * (b // 2) : LANES * (b // 2 + 1)]
        r = pltpu.roll(t, HALF, 1)
        low, up = (t, r) if b % 2 == 0 else (r, t)
        upper = fill if fill is not None else up - rounded(up)
        tile = jnp.where(lower_lanes(t.shape), rounded(low), upper)
        out.append(tile.reshape(16, 8, LANES))
    return jnp.concatenate(out, axis=1).reshape(SLOTS, LANES)


def state_of(tiles):
    both = tiles + pltpu.roll(tiles, HALF, 1)
    t = both.reshape(16, 32, LANES)
    part = [t[:, 8 * b : 8 * b + 8, :].reshape(DK, LANES) for b in range(4)]
    low = lower_lanes((DK, LANES))
    return jnp.concatenate(
        [jnp.where(low, part[0], part[1]), jnp.where(low, part[2], part[3])], axis=1
    )


def prep_kernel(q_ref, ids_ref, w_ref, x_ref, oc_ref, k_ref, v_ref, g_ref, pay_ref, pick_ref):
    expert = iota((EXPERTS, TOK), 0)
    id0, id1 = ids_ref[0:1, :], ids_ref[1:2, :]
    hit0, hit1 = expert == id0, expert == id1
    named = (hit0.astype(F32) + hit1.astype(F32)).astype(BF)
    before = (iota((TOK, TOK), 0) < iota((TOK, TOK), 1)).astype(F32).astype(BF)
    count = dot(named, before, 1, 0)
    rank0 = jnp.sum(jnp.where(hit0, count, 0.0), axis=0, keepdims=True)
    rank1 = jnp.sum(jnp.where(hit1, count, 0.0), axis=0, keepdims=True)
    slot0 = id0 * CAP + rank0.astype(jnp.int32)
    slot1 = id1 * CAP + rank1.astype(jnp.int32)
    slot = iota((SLOTS, TOK), 0)
    at0, at1 = slot == slot0, slot == slot1
    pick = (at0.astype(F32) + at1.astype(F32)).astype(BF)
    pick_ref[...] = pick
    weight = jnp.sum(
        jnp.where(at0, w_ref[0:1, :], 0.0) + jnp.where(at1, w_ref[1:2, :], 0.0),
        axis=1,
        keepdims=True,
    )
    pay_ref[:, :QUART] = dot(pick, x_ref[...], 1, 0).astype(BF)
    pay_ref[:, QUART : 2 * QUART] = (dot(pick, oc_ref[...], 1, 0) * weight).astype(BF)
    g = g_ref[...]
    cum = cumulative_sum(g)
    to_end = k_ref[...].astype(F32) * jnp.exp(cum[TOK - 1 : TOK, :] - cum)
    state = dot(to_end.T, v_ref[...].astype(F32), 1, 0, HI)
    factor = jnp.exp(jnp.sum(g.T, axis=1, keepdims=True))
    high = rounded(factor)
    lane = iota((DK, LANES), 1)
    fill = jnp.where(lane < 96, high, factor - high)
    pay_ref[:, 2 * QUART :] = tiles_of(state, fill).astype(BF)


def prefix_kernel(q_ref, in_ref, out_ref, factor_ref, work_ref):
    tiles = in_ref[...].astype(F32)
    work_ref[...] = tiles
    factor_ref[...] = jnp.broadcast_to(tiles[:, 64:65] + tiles[:, 96:97], tiles.shape)
    carry = jnp.zeros((8, LANES), F32)
    for s in range(EXPERTS):
        rows = slice(8 * s, 8 * s + 8)
        now = work_ref[rows, :]
        work_ref[rows, :] = carry
        carry = carry * factor_ref[rows, :] + now
    pre = work_ref[...]
    low = rounded(pre)
    rest = pltpu.roll(pre - low, HALF, 1)
    out_ref[...] = jnp.where(lower_lanes(pre.shape), low, rest).astype(BF)


def suffix_kernel(q_ref, in_ref, factor_ref, out_ref, work_ref):
    tiles = in_ref[...].astype(F32)
    work_ref[...] = tiles + pltpu.roll(tiles, HALF, 1)
    carry = jnp.zeros((8, LANES), F32)
    for s in reversed(range(EXPERTS)):
        rows = slice(8 * s, 8 * s + 8)
        now = work_ref[rows, :]
        work_ref[rows, :] = carry
        carry = carry * factor_ref[rows, :] + now
    suf = work_ref[...]
    low = rounded(suf)
    out_ref[...] = jnp.where(lower_lanes(suf.shape), low, suf - low).astype(BF)


def near_kernel(q_ref, own_ref, a_ref, b_ref, wg_ref, wu_ref, wd_ref, g_ref, u_ref, h_ref):
    g = u = h = None
    for n, ref in enumerate((own_ref, a_ref, b_ref)):
        rows = quarter_rows(q_ref[n])
        x, dy = ref[:, :QUART], ref[:, QUART : 2 * QUART]
        g1 = dot(x, wg_ref[rows, :], 1, 0)
        u1 = dot(x, wu_ref[rows, :], 1, 0)
        h1 = dot(dy, wd_ref[:, rows], 1, 1)
        g, u, h = (g1, u1, h1) if g is None else (g + g1, u + u1, h + h1)
    g_ref[...] = g
    u_ref[...] = u
    h_ref[...] = h


def far_kernel(
    q_ref, g_ref, u_ref, h_ref, c_ref, d_ref, wg_ref, wu_ref, wd_ref,
    far_ref, right_ref, left_ref, own_ref, hid_ref, gu_ref,
):
    rows = quarter_rows(q_ref[3])
    x = jnp.concatenate([c_ref[:, :QUART], d_ref[:, :QUART]], axis=0)
    dy = jnp.concatenate([c_ref[:, QUART:], d_ref[:, QUART:]], axis=0)
    g = g_ref[...] + dot(x, wg_ref[rows, :], 1, 0)
    u = u_ref[...] + dot(x, wu_ref[rows, :], 1, 0)
    h = h_ref[...] + dot(dy, wd_ref[:, rows], 1, 1)
    sig = jax.nn.sigmoid(g)
    hid_ref[...] = (g * sig * u).astype(BF)
    gate_cot = (h * u * sig * (1.0 + g * (1.0 - sig))).astype(BF)
    up_cot = (h * g * sig).astype(BF)
    gu_ref[:, :FF] = gate_cot
    gu_ref[:, FF:] = up_cot
    for n, ref in ((3, far_ref), (2, right_ref), (1, left_ref), (0, own_ref)):
        rows = quarter_rows(q_ref[n])
        part = dot(gate_cot, wg_ref[rows, :], 1, 1) + dot(up_cot, wu_ref[rows, :], 1, 1)
        ref[...] = part.astype(BF)


def weight_kernel(
    q_ref, own_ref, a_ref, b_ref, c_ref, d_ref, hid_ref, gu_ref, gg_ref, gup_ref, gd_ref
):
    hid_t = hid_ref[...].T
    gu = gu_ref[...]
    for n in range(4):
        rows = quarter_rows(q_ref[n])
        if n < 3:
            ref = (own_ref, a_ref, b_ref)[n]
            x, dy = ref[:, :QUART], ref[:, QUART : 2 * QUART]
        else:
            x = jnp.concatenate([c_ref[:, :QUART], d_ref[:, :QUART]], axis=0)
            dy = jnp.concatenate([c_ref[:, QUART:], d_ref[:, QUART:]], axis=0)
        both = dot(x.T, gu, 1, 0)
        gg_ref[rows, :] = both[:, :FF]
        gup_ref[rows, :] = both[:, FF:]
        gd_ref[:, rows] = dot(hid_t, dy, 1, 0)


def sum_kernel(q_ref, p0_ref, p1_ref, p2_ref, p3_ref, st_ref, out_ref):
    total = p0_ref[...].astype(F32) + p1_ref[...].astype(F32)
    total = total + p2_ref[...].astype(F32) + p3_ref[...].astype(F32)
    out_ref[:, :QUART] = total.astype(BF)
    out_ref[:, QUART:] = st_ref[...]


def combine_kernel(q_ref, rows_ref, pick_ref, oc_ref, out_ref):
    routed = dot(pick_ref[...].T, rows_ref[...], 1, 0)
    out_ref[...] = (oc_ref[...].astype(F32) + routed).astype(BF)


def head_kernel(q_ref, m0_ref, m1_ref, m2_ref, m3_ref, w_ref, qry_ref, g_ref, h_ref, pull_ref):
    head = None
    for n, ref in enumerate((m0_ref, m1_ref, m2_ref, m3_ref)):
        part = dot(ref[...], w_ref[quarter_rows(q_ref[n]), :], 1, 0)
        head = part if head is None else head + part
    h_ref[...] = head
    decayed = qry_ref[...].astype(F32) * jnp.exp(cumulative_sum(g_ref[...]))
    pull_ref[...] = tiles_of(dot(decayed.T, head, 1, 0, HI)).astype(BF)


def out_proj_kernel(q_ref, m0_ref, m1_ref, m2_ref, m3_ref, mixed_ref, out_ref):
    mixed = mixed_ref[...]
    for n, ref in enumerate((m0_ref, m1_ref, m2_ref, m3_ref)):
        out_ref[quarter_rows(q_ref[n]), :] = dot(ref[...].T, mixed, 1, 0).astype(BF)


def attend_kernel(
    q_ref, qry_ref, k_ref, v_ref, g_ref, h_ref, st_ref, cot_ref,
    gq_ref, gk_ref, gv_ref, gg_ref,
):
    qry, k, v = qry_ref[...].astype(F32), k_ref[...].astype(F32), v_ref[...].astype(F32)
    head = h_ref[...]
    state = state_of(st_ref[...].astype(F32))
    cot = state_of(cot_ref[...].astype(F32))
    cum = cumulative_sum(g_ref[...])
    last = cum[TOK - 1 : TOK, :]
    grow, shrink, to_end = jnp.exp(cum), jnp.exp(-cum), jnp.exp(last - cum)
    q_dec, k_grown, k_end = qry * grow, k * shrink, k * to_end
    causal = iota((TOK, TOK), 0) >= iota((TOK, TOK), 1)
    score = jnp.where(causal, dot(q_dec, k_grown, 1, 1, HI), 0.0)
    d_score = jnp.where(causal, dot(head, v, 1, 1, HI), 0.0)
    d_q = dot(d_score, k_grown, 1, 0, HI) + dot(head, state, 1, 1, HI)
    d_kg = dot(d_score.T, q_dec, 1, 0, HI)
    d_ke = dot(v, cot, 1, 1, HI)
    d_v = dot(score.T, head, 1, 0, HI) + dot(k_end, cot, 1, 0, HI)
    gq_ref[...] = (d_q * grow).astype(BF)
    gk_ref[...] = (d_kg * shrink + d_ke * to_end).astype(BF)
    gv_ref[...] = d_v.astype(BF)
    end = d_ke * k_end
    d_cum = d_q * q_dec - d_kg * k_grown - end
    carried = jnp.sum((state * cot).T, axis=0, keepdims=True)
    d_last = jnp.sum(end, axis=0, keepdims=True) + jnp.exp(last) * carried
    upper = (iota((TOK, TOK), 0) <= iota((TOK, TOK), 1)).astype(F32)
    gg_ref[...] = dot(upper, d_cum, 1, 0, HI) + d_last


def per_device(
    expert_in, out_cot, route_ids, route_weights, w_gate, w_up, w_down, w_out,
    mixed_heads, queries, keys, values, log_decay,
):
    me = lax.axis_index("tp")
    order = (me + jnp.array([0, 3, 1, 2], jnp.int32)) % 4
    to_right = [(i, (i + 1) % 4) for i in range(4)]
    to_left = [(i, (i + 3) % 4) for i in range(4)]
    across = [(i, (i + 2) % 4) for i in range(4)]
    wg, wu, wd = w_gate[0], w_up[0], w_down[0]
    run = functools.partial(call, index=order)

    def exchange(rows):
        width = rows.shape[1]
        got = lax.all_to_all(rows.reshape(EXPERTS, CAP, width), "sp", 0, 0, tiled=True)
        return got.reshape(SLOTS, width)

    def quarter_block():
        return pl.BlockSpec((TOK, QUART), lambda i, q: (0, q[0]))

    def lane_tile(n):
        return pl.BlockSpec((SLOTS, LANES), lambda i, q: (0, n))

    with jax.named_scope("prep"):
        pay, pick = run(
            prep_kernel,
            (sds((SLOTS, 2 * QUART + LANES), BF), sds((SLOTS, TOK), BF)),
            (route_ids.T, route_weights.T, expert_in, out_cot, keys, values, log_decay),
            in_specs=[None, None, quarter_block(), quarter_block(), None, None, None],
            flops=4e8,
        )
    with jax.named_scope("dispatch"):
        got = exchange(pay)
        rows = got[:, : 2 * QUART]
        left = lax.ppermute(rows, "tp", to_right)
        right = lax.ppermute(rows, "tp", to_left)
        far_top = lax.ppermute(left[: SLOTS // 2], "tp", to_right)
        far_bottom = lax.ppermute(right[SLOTS // 2 :], "tp", to_left)
    with jax.named_scope("near"):
        g, u, h = run(
            near_kernel,
            (sds((SLOTS, FF), F32),) * 3,
            (got, left, right, wg, wu, wd),
            flops=1.2e9,
        )
    with jax.named_scope("far"):
        p_far, p_right, p_left, p_own, hidden, gate_up = run(
            far_kernel,
            (sds((SLOTS, QUART), BF),) * 4 + (sds((SLOTS, FF), BF), sds((SLOTS, 2 * FF), BF)),
            (g, u, h, far_top, far_bottom, wg, wu, wd),
            flops=1.5e9,
        )
    with jax.named_scope("scatter"):
        r_far = lax.ppermute(p_far, "tp", across)
        r_left = lax.ppermute(p_right, "tp", to_right)
        r_right = lax.ppermute(p_left, "tp", to_left)
    with jax.named_scope("prefix"):
        state_back, factor = pl.pallas_call(
            prefix_kernel,
            out_shape=(sds((SLOTS, LANES), BF), sds((SLOTS, LANES), F32)),
            grid_spec=pltpu.PrefetchScalarGridSpec(
                num_scalar_prefetch=1,
                grid=(1,),
                in_specs=[lane_tile(2 * QUART // LANES)],
                out_specs=(lane_tile(0), lane_tile(0)),
                scratch_shapes=[pltpu.VMEM((SLOTS, LANES), F32)],
            ),
            compiler_params=pltpu.CompilerParams(vmem_limit_bytes=8 * 2**20),
            cost_estimate=pl.CostEstimate(flops=10**8, bytes_accessed=10**6, transcendentals=0),
        )(order, got)
    with jax.named_scope("weights"):
        grad_gate, grad_up, grad_down = run(
            weight_kernel,
            (sds((WIDTH, FF), F32), sds((WIDTH, FF), F32), sds((FF, WIDTH), F32)),
            (got, left, right, far_top, far_bottom, hidden, gate_up),
            flops=1.6e9 * 4,
        )
    with jax.named_scope("back"):
        total = run(
            sum_kernel,
            sds((SLOTS, QUART + LANES), BF),
            (p_own, r_far, r_left, r_right, state_back),
            flops=1e6,
        )
        back = exchange(total)
        mid = run(
            combine_kernel,
            sds((TOK, QUART), BF),
            (back, pick, out_cot),
            in_specs=[pl.BlockSpec((SLOTS, QUART), lambda i, q: (0, 0)), None, quarter_block()],
            flops=7e7,
        )
        m_left = lax.ppermute(mid, "tp", to_right)
        m_right = lax.ppermute(mid, "tp", to_left)
        m_far = lax.ppermute(mid, "tp", across)
    with jax.named_scope("head"):
        head, pull = run(
            head_kernel,
            (sds((TOK, DV), F32), sds((SLOTS, LANES), BF)),
            (mid, m_left, m_right, m_far, w_out, queries, log_decay),
            flops=2e8,
        )
        pulled = exchange(pull)
    with jax.named_scope("out_proj"):
        part = run(
            out_proj_kernel,
            sds((WIDTH, DV), BF),
            (mid, m_left, m_right, m_far, mixed_heads),
            flops=1.4e8,
        )
        parts = lax.all_to_all(part.reshape(64, 32, DV), "sp", 0, 0, tiled=True)
        grad_out_proj = jnp.sum(parts.astype(F32), axis=0)
    with jax.named_scope("suffix"):
        cot_back = pl.pallas_call(
            suffix_kernel,
            out_shape=sds((SLOTS, LANES), BF),
            grid_spec=pltpu.PrefetchScalarGridSpec(
                num_scalar_prefetch=1,
                grid=(1,),
                in_specs=[lane_tile(0), lane_tile(0)],
                out_specs=lane_tile(0),
                scratch_shapes=[pltpu.VMEM((SLOTS, LANES), F32)],
            ),
            compiler_params=pltpu.CompilerParams(vmem_limit_bytes=8 * 2**20),
            cost_estimate=pl.CostEstimate(flops=10**8, bytes_accessed=10**6, transcendentals=0),
        )(order, pulled, factor)
        cot = exchange(cot_back)
    with jax.named_scope("attend"):
        grad_queries, grad_keys, grad_values, grad_decay = run(
            attend_kernel,
            (sds((TOK, DK), BF), sds((TOK, DK), BF), sds((TOK, DV), BF), sds((TOK, DK), F32)),
            (queries, keys, values, log_decay, head, back, cot),
            in_specs=[None] * 5 + [lane_tile(QUART // LANES), None],
            flops=6e8,
        )
    return (
        grad_gate[None],
        grad_up[None],
        grad_down[None],
        grad_out_proj,
        grad_queries,
        grad_keys,
        grad_values,
        grad_decay,
    )


def solution(mesh):
    return jax.shard_map(
        per_device,
        mesh=mesh,
        in_specs=(
            P("sp", None),
            P("sp", None),
            P("sp", None),
            P("sp", None),
            P("sp", None, "tp"),
            P("sp", None, "tp"),
            P("sp", "tp", None),
            P(None, "tp"),
            P("sp", "tp"),
            P("sp", "tp"),
            P("sp", "tp"),
            P("sp", "tp"),
            P("sp", "tp"),
        ),
        out_specs=(
            P("sp", None, "tp"),
            P("sp", None, "tp"),
            P("sp", "tp", None),
            P("sp", "tp"),
            P("sp", "tp"),
            P("sp", "tp"),
            P("sp", "tp"),
            P("sp", "tp"),
        ),
        check_vma=False,
    )
```

time: 355 us -> 234 us (0.66)
  blocking collectives: 153 us -> 89.4 us
  matrix products: 36.4 us -> 0 us
  Pallas kernels: 0 us -> 21.2 us
  local copies, waits for them, and re-layouts: 34.6 us -> 14.6 us
  other arithmetic: 22.4 us -> 2.68 us
  starting transfers between devices: 8.82 us -> 23.6 us
  between operations: 15.4 us -> 0.94 us
    all_gather x8 -> x0, blocking collectives: 72.2 us -> none  [carried_in(): pieces = jax.tree.map(lambda part: lax.all_gather(part, axis), running)]
    ppermute x0 -> x10, waiting for transfers between devices: none -> 56.9 us  [the longest x1 22 us: per_device(): right = lax.ppermute(rows, 'tp', to_left)]
    all_gather x5 -> x0, waiting for transfers between devices: 46 us -> none  [the longest x1 25.5 us: per_device(): lax.all_gather(got_dy.reshape(n_sp * exp_dev, share_rows, width), 'tp', a...]
    dot_general x20 -> x0, matrix products: 36.4 us -> none  [the longest x1 4.65 us: per_device(): jnp.einsum('esd,esf->edf', got_x, gate_cot, preferred_element_type=jnp.fl...]
    reduce_scatter x1 -> x0, waiting for transfers between devices: 32.1 us -> none  [per_device(): lax.psum_scatter(partial_value.astype(jnp.bfloat16), 'tp', scatter_dimens...]
    all_to_all x1 -> x2, waiting for transfers between devices: 0.01 us -> 21.3 us  [the longest x1 15.9 us: per_device(): parts = lax.all_to_all(part.reshape(64, 32, DV), 'sp', 0, 0, tiled=True)]
    pallas_call x0 -> x11, Pallas kernels: none -> 21.2 us  [the longest x9 19.5 us: call(): pl.pallas_call(kernel, out_shape=out_shape, grid_spec=pltpu.PrefetchScala...]
    gather x5 -> x0, local copies, waits for them, and re-layouts: 15.8 us -> none  [the longest x2 5.73 us: per_device(): jnp.take(returned, slot_index, axis=0).astype(jnp.float32)]
  transfers between devices with their start and end apart: 7 -> 12, of which waited for: 3 -> 11; matrix products, arithmetic and copies ran while one was open for 15% -> 0% of each run, Pallas kernels for 0% -> 6%
where the time goes in v1:
time: 234 us; the launch traced here: 231 us
  blocking collectives  89.4 us (38%)
  waiting for transfers between devices  78.2 us (33%)
  starting transfers between devices  23.6 us (10%)
  Pallas kernels  21.2 us (9%)
  local copies, waits for them, and re-layouts  14.6 us (6%)
  other arithmetic  2.68 us (1%)
    all_to_all x3, blocking collectives, exchange(): lax.all_to_all(rows.reshape(EXPERTS, CAP, width), 'sp', 0, 0, tiled=True)  89.4 us
    ppermute x1, waiting for transfers between devices, per_device(): right = lax.ppermute(rows, 'tp', to_left)  22 us
    pallas_call x9, Pallas kernels, call(): pl.pallas_call(kernel, out_shape=out_shape, grid_spec=pltpu.PrefetchScala...  19.5 us
    all_to_all x1, waiting for transfers between devices, per_device(): parts = lax.all_to_all(part.reshape(64, 32, DV), 'sp', 0, 0, tiled=True)  15.9 us
    unnamed x72, local copies, waits for them, and re-layouts  14.4 us
    ppermute x1, waiting for transfers between devices, per_device(): r_far = lax.ppermute(p_far, 'tp', across)  11 us
    ppermute x1, waiting for transfers between devices, per_device(): far_bottom = lax.ppermute(right[SLOTS // 2:], 'tp', to_left)  7.86 us
    ppermute x1, waiting for transfers between devices, per_device(): r_left = lax.ppermute(p_right, 'tp', to_right)  6.99 us
  transfers between devices with their start and end apart: 12, of which 11 were waited for; matrix products, arithmetic and copies ran while one was open for 0% of the time, Pallas kernels for 6%

profile of v1, /device:TPU:2, one launch (start us, length us, event | category | flops | bytes accessed | tf_op | source)
XLA Modules:
  0.0 230.6 jit_solution(12149939281988960629)
XLA Ops:
  1.3 1.0 copy-done.15
  3.2 1.0 copy-done.23
  7.2 1.8 prep.1
  9.0 43.6 %all_to_all.25 = bf16[64,8,1152]{2,1,0:T(8,128)(2,1)S(1)} all-to-all(bf16[64,8,1152]{2,1,0:T(8,128)(2,1)S(1)} %bitcast.30), channel_id=1, replica_groups=mesh['sp'=64,'tp'=4] {'sp'}, dimensions={0} | all-to-all | bytes 2359296 | tf_op jit(solution)/shard_map/dispatch/all_to_all | solution.py:294
  53.3 1.5 collective-permute-start
  54.8 22.0 %collective-permute-done.1.b_ref = bf16[512,1024]{1,0:T(8,128)(2,1)S(1)} collective-permute-done((bf16[512,1024]{1,0:T(8,128)(2,1)S(1)}, bf16[512,1024]{1,0:T(8,128)(2,1)S(1)}, u32[]{:S(2)}, u32[]{:S(2)}) %collective-permute-start.1) | collective-permute-done | bytes 1048608 | tf_op jit(solution)/shard_map/dispatch/ppermute | solution.py:315
  79.1 1.9 near.1
  81.1 7.9 %collective-permute-done.3.d_ref = bf16[256,1024]{1,0:T(8,128)(2,1)S(1)} collective-permute-done((bf16[256,1024]{1,0:T(8,128)(2,1)S(1)}, bf16[256,1024]{1,0:T(8,128)(2,1)S(1)}, u32[]{:S(2)}, u32[]{:S(2)}) %collective-permute-start.3) | collective-permute-done | bytes 524320 | tf_op jit(solution)/shard_map/dispatch/ppermute | solution.py:317
  88.9 2.6 %collective-permute-done.2.c_ref = bf16[256,1024]{1,0:T(8,128)(2,1)S(1)} collective-permute-done((bf16[256,1024]{1,0:T(8,128)(2,1)S(1)}, bf16[256,1024]{1,0:T(8,128)(2,1)S(1)}, u32[]{:S(2)}, u32[]{:S(2)}) %collective-permute-start.2) | collective-permute-done | bytes 524320 | tf_op jit(solution)/shard_map/dispatch/ppermute | solution.py:316
  91.6 2.3 %far.1 = (bf16[512,512]{1,0:T(8,128)(2,1)S(1)}, bf16[512,512]{1,0:T(8,128)(2,1)S(1)}, bf16[512,512]{1,0:T(8,128)(2,1)S(1)}, bf16[512,512]{1,0:T(8,128)(2,1)S(1)}...) custom-call(s32[4]{0:T(128)S(1)} %and_select_fusion.q_ref, f32[512,256]{1,0:T(8,128)S(1)} %get-tuple-element.31.g_ref, ...), custom_call_target="tpu_custom_call" | custom-call | flops 1500000000 | bytes 8650752 | tf_op jit(solution)/shard_map/far/pallas_call | solution.py:56
  93.9 2.0 collective-permute-start.4
  95.9 2.5 %collective-permute-start.5 = (bf16[512,512]{1,0:T(8,128)(2,1)S(1)}, bf16[512,512]{1,0:T(8,128)(2,1)S(1)}, u32[]{:S(2)}, u32[]{:S(2)}) collective-permute-start(bf16[512,512]{1,0:T(8,128)(2,1)S(1)} %get-tuple-element.41), channel_id=1, source_target_pairs={{0,1},{1,2},{2,3},{3,0},{4,5},{5,6},{6,7},{7,4},{8,9},{9,10},{10,1... | collective-permute-start | bytes 1572872 | tf_op jit(solution)/shard_map/scatter/ppermute | solution.py:334
  99.3 11.0 %collective-permute-done.4.p1_ref = bf16[512,512]{1,0:T(8,128)(2,1)S(1)} collective-permute-done((bf16[512,512]{1,0:T(8,128)(2,1)S(1)}, bf16[512,512]{1,0:T(8,128)(2,1)S(1)}, u32[]{:S(2)}, u32[]{:S(2)}) %collective-permute-start.4) | collective-permute-done | bytes 524320 | tf_op jit(solution)/shard_map/scatter/ppermute | solution.py:333
  110.3 7.0 %collective-permute-done.5.p2_ref = bf16[512,512]{1,0:T(8,128)(2,1)S(1)} collective-permute-done((bf16[512,512]{1,0:T(8,128)(2,1)S(1)}, bf16[512,512]{1,0:T(8,128)(2,1)S(1)}, u32[]{:S(2)}, u32[]{:S(2)}) %collective-permute-start.5) | collective-permute-done | bytes 524320 | tf_op jit(solution)/shard_map/scatter/ppermute | solution.py:334
  118.7 29.5 %all_to_all.26 = bf16[64,8,640]{2,1,0:T(8,128)(2,1)S(1)} all-to-all(bf16[64,8,640]{2,1,0:T(8,128)(2,1)S(1)} %bitcast.29), channel_id=1, replica_groups=mesh['sp'=64,'tp'=4] {'sp'}, dimensions={0} | all-to-all | bytes 1310720 | tf_op jit(solution)/shard_map/back/all_to_all | solution.py:294
  149.0 2.2 collective-permute-start.9
  152.1 1.2 collective-permute-start.7
  153.2 3.7 %collective-permute-done.9.m3_ref = bf16[128,512]{1,0:T(8,128)(2,1)S(1)} collective-permute-done((bf16[128,512]{1,0:T(8,128)(2,1)S(1)}, bf16[128,512]{1,0:T(8,128)(2,1)S(1)}, u32[]{:S(2)}, u32[]{:S(2)}) %collective-permute-start.9) | collective-permute-done | bytes 131104 | tf_op jit(solution)/shard_map/back/ppermute | solution.py:374
  157.0 1.8 collective-permute-done.8.m2_ref
  158.8 1.4 head.1
  160.3 16.3 %all_to_all.27 = bf16[64,8,128]{2,1,0:T(8,128)(2,1)S(1)} all-to-all(bf16[64,8,128]{2,1,0:T(8,128)(2,1)S(1)} %bitcast.33), channel_id=1, replica_groups=mesh['sp'=64,'tp'=4] {'sp'}, dimensions={0} | all-to-all | bytes 262144 | tf_op jit(solution)/shard_map/head/all_to_all | solution.py:294
  178.0 5.4 %all-to-all-start.4 = ((bf16[64,8,128]{2,1,0:T(8,128)(2,1)}), bf16[64,8,128]{2,1,0:T(8,128)(2,1)}, u32[]{:S(2)}, u32[]{:S(2)}) async-start(bf16[64,8,128]{2,1,0:T(8,128)(2,1)} %bitcast.31), calls=%async_computation.4 | async-start | bytes 262144 | tf_op jit(solution)/shard_map/suffix/all_to_all | solution.py:294
  187.0 2.0 out_proj.1
  189.0 5.4 %all-to-all-done.4 = bf16[64,8,128]{2,1,0:T(8,128)(2,1)} async-done(((bf16[64,8,128]{2,1,0:T(8,128)(2,1)}), bf16[64,8,128]{2,1,0:T(8,128)(2,1)}, u32[]{:S(2)}, u32[]{:S(2)}) %all-to-all-start.4) | async-done | bytes 131104 | tf_op jit(solution)/shard_map/suffix/all_to_all | solution.py:294
  194.4 5.5 %all-to-all-start.2 = ((bf16[64,32,256]{2,1,0:T(8,128)(2,1)}), bf16[64,32,256]{2,1,0:T(8,128)(2,1)}, u32[]{:S(2)}, u32[]{:S(2)}) async-start(bf16[64,32,256]{2,1,0:T(8,128)(2,1)} %bitcast.12), calls=%async_computation.2 | async-start | bytes 2097152 | tf_op jit(solution)/shard_map/out_proj/all_to_all | solution.py:390
  199.9 1.2 copy-done.4
  201.2 1.0 copy-done.7
  202.2 1.0 copy-done.25
  204.2 4.9 %weights.1 = (f32[2048,256]{1,0:T(8,128)}, f32[2048,256]{1,0:T(8,128)}, f32[256,2048]{1,0:T(8,128)}) custom-call(s32[4]{0:T(128)S(1)} %and_select_fusion.q_ref, bf16[512,1152]{1,0:T(8,128)(2,1)S(1)} %bitcast.20, bf16[512,1024]{1,0:T(8,128)(2,1)S(1)} %copy-done.4, bf16[512,1024]{1,0:T(8,128)(2,1)S(1)} %collective-permute-done.1.b_ref, ...), custom_call_target="tpu_custom_call" | custom-call | flops 6400000000 | bytes 11403264 | tf_op jit(solution)/shard_map/weights/pallas_call | solution.py:56
  209.2 3.5 %attend.1 = (bf16[128,128]{1,0:T(8,128)(2,1)}, bf16[128,128]{1,0:T(8,128)(2,1)}, bf16[128,256]{1,0:T(8,128)(2,1)}, f32[128,128]{1,0:T(8,128)}) custom-call(s32[4]{0:T(128)S(1)} %and_select_fusion.q_ref, bf16[128,128]{1,0:T(8,128)(2,1)S(1)} %copy-done.22, bf16[128,128]{1,0:T(8,128)(2,1)S(1)} %copy-done.33, bf16[128,256]{1,0:T(8,128)(2,1)S(1)} %copy-done.31, ...), custom_call_target="tpu_custom_call" | custom-call | flops 600000000 | bytes 1310720 | tf_op jit(solution)/shard_map/attend/pallas_call | solution.py:56
  212.7 15.9 %all-to-all-done.2 = bf16[64,32,256]{2,1,0:T(8,128)(2,1)} async-done(((bf16[64,32,256]{2,1,0:T(8,128)(2,1)}), bf16[64,32,256]{2,1,0:T(8,128)(2,1)}, u32[]{:S(2)}, u32[]{:S(2)}) %all-to-all-start.2) | async-done | bytes 1048608 | tf_op jit(solution)/shard_map/out_proj/all_to_all | solution.py:390
  228.6 2.0 convert_reduce_fusion
  (83 shorter events, 17.4 us)
Async XLA Ops:
  52.6 26.6 %copy-start = (bf16[1,2048,256]{2,1,0:T(8,128)(2,1)S(1)}, bf16[1,2048,256]{2,1,0:T(8,128)(2,1)}, u32[]{:S(2)}) copy-start(bf16[1,2048,256]{2,1,0:T(8,128)(2,1)} %param.18) | copy-start | bytes 3145732
  52.6 26.6 %copy-start.1 = (bf16[1,2048,256]{2,1,0:T(8,128)(2,1)S(1)}, bf16[1,2048,256]{2,1,0:T(8,128)(2,1)}, u32[]{:S(2)}) copy-start(bf16[1,2048,256]{2,1,0:T(8,128)(2,1)} %param.19) | copy-start | bytes 3145732
  52.6 26.6 %copy-start.2 = (bf16[1,256,2048]{2,1,0:T(8,128)(2,1)S(1)}, bf16[1,256,2048]{2,1,0:T(8,128)(2,1)}, u32[]{:S(2)}) copy-start(bf16[1,256,2048]{2,1,0:T(8,128)(2,1)} %param.20) | copy-start | bytes 3145732
  52.7 24.1 %collective-permute-start.1 = (bf16[512,1024]{1,0:T(8,128)(2,1)S(1)}, bf16[512,1024]{1,0:T(8,128)(2,1)S(1)}, u32[]{:S(2)}, u32[]{:S(2)}) collective-permute-start(bf16[512,1024]{1,0:T(8,128)(2,1)S(1)} %slice.12), channel_id=1, source_target_pairs={{0,3},{1,0},{2,1},{3,2},{4,7},{5,4},{6,5},{7,6},{8,11},{9,8},{10,9... | collective-permute-start | bytes 3145736 | tf_op jit(solution)/shard_map/dispatch/ppermute | solution.py:315
  53.3 24.8 %collective-permute-start = (bf16[512,1024]{1,0:T(8,128)(2,1)S(1)}, bf16[512,1024]{1,0:T(8,128)(2,1)S(1)}, u32[]{:S(2)}, u32[]{:S(2)}) collective-permute-start(bf16[512,1024]{1,0:T(8,128)(2,1)S(1)} %slice.12), channel_id=1, source_target_pairs={{0,1},{1,2},{2,3},{3,0},{4,5},{5,6},{6,7},{7,4},{8,9},{9,10},{10,1... | collective-permute-start | bytes 3145736 | tf_op jit(solution)/shard_map/dispatch/ppermute | solution.py:314
  76.9 12.0 %collective-permute-start.3 = (bf16[256,1024]{1,0:T(8,128)(2,1)S(1)}, bf16[256,1024]{1,0:T(8,128)(2,1)S(1)}, u32[]{:S(2)}, u32[]{:S(2)}) collective-permute-start(bf16[256,1024]{1,0:T(8,128)(2,1)S(1)} %slice.14), channel_id=1, source_target_pairs={{0,3},{1,0},{2,1},{3,2},{4,7},{5,4},{6,5},{7,6},{8,11},{9,8},{10,9... | collective-permute-start | bytes 1572872 | tf_op jit(solution)/shard_map/dispatch/ppermute | solution.py:317
  78.1 2.9 %copy-start.3 = (bf16[512,1024]{1,0:T(8,128)(2,1)}, bf16[512,1024]{1,0:T(8,128)(2,1)S(1)}, u32[]{:S(2)}) copy-start(bf16[512,1024]{1,0:T(8,128)(2,1)S(1)} %collective-permute-done.a_ref) | copy-start | bytes 3145732
  78.2 13.4 %collective-permute-start.2 = (bf16[256,1024]{1,0:T(8,128)(2,1)S(1)}, bf16[256,1024]{1,0:T(8,128)(2,1)S(1)}, u32[]{:S(2)}, u32[]{:S(2)}) collective-permute-start(bf16[256,1024]{1,0:T(8,128)(2,1)S(1)} %slice.13), channel_id=1, source_target_pairs={{0,1},{1,2},{2,3},{3,0},{4,5},{5,6},{6,7},{7,4},{8,9},{9,10},{10,1... | collective-permute-start | bytes 1572872 | tf_op jit(solution)/shard_map/dispatch/ppermute | solution.py:316
  91.6 2.3 %copy-start.6 = (bf16[256,1024]{1,0:T(8,128)(2,1)}, bf16[256,1024]{1,0:T(8,128)(2,1)S(1)}, u32[]{:S(2)}) copy-start(bf16[256,1024]{1,0:T(8,128)(2,1)S(1)} %collective-permute-done.2.c_ref) | copy-start | bytes 1572868
  93.9 54.3 %copy-start.24 = (bf16[512,512]{1,0:T(8,128)(2,1)}, bf16[512,512]{1,0:T(8,128)(2,1)S(1)}, u32[]{:S(2)}) copy-start(bf16[512,512]{1,0:T(8,128)(2,1)S(1)} %get-tuple-element.35.gu_ref) | copy-start | bytes 1572868
  93.9 54.3 %copy-start.26 = (bf16[512,256]{1,0:T(8,128)(2,1)}, bf16[512,256]{1,0:T(8,128)(2,1)S(1)}, u32[]{:S(2)}) copy-start(bf16[512,256]{1,0:T(8,128)(2,1)S(1)} %get-tuple-element.34.hid_ref) | copy-start | bytes 786436
  93.9 16.4 %collective-permute-start.4 = (bf16[512,512]{1,0:T(8,128)(2,1)S(1)}, bf16[512,512]{1,0:T(8,128)(2,1)S(1)}, u32[]{:S(2)}, u32[]{:S(2)}) collective-permute-start(bf16[512,512]{1,0:T(8,128)(2,1)S(1)} %get-tuple-element.40), channel_id=1, source_target_pairs={{0,2},{1,3},{2,0},{3,1},{4,6},{5,7},{6,4},{7,5},{8,10},{9,11},{10,... | collective-permute-start | bytes 1572872 | tf_op jit(solution)/shard_map/scatter/ppermute | solution.py:333
  95.9 21.4 %collective-permute-start.5 = (bf16[512,512]{1,0:T(8,128)(2,1)S(1)}, bf16[512,512]{1,0:T(8,128)(2,1)S(1)}, u32[]{:S(2)}, u32[]{:S(2)}) collective-permute-start(bf16[512,512]{1,0:T(8,128)(2,1)S(1)} %get-tuple-element.41), channel_id=1, source_target_pairs={{0,1},{1,2},{2,3},{3,0},{4,5},{5,6},{6,7},{7,4},{8,9},{9,10},{10,1... | collective-permute-start | bytes 1572872 | tf_op jit(solution)/shard_map/scatter/ppermute | solution.py:334
  98.4 19.4 %collective-permute-start.6 = (bf16[512,512]{1,0:T(8,128)(2,1)S(1)}, bf16[512,512]{1,0:T(8,128)(2,1)S(1)}, u32[]{:S(2)}, u32[]{:S(2)}) collective-permute-start(bf16[512,512]{1,0:T(8,128)(2,1)S(1)} %get-tuple-element.42), channel_id=1, source_target_pairs={{0,3},{1,0},{2,1},{3,2},{4,7},{5,4},{6,5},{7,6},{8,11},{9,8},{10,9... | collective-permute-start | bytes 1572872 | tf_op jit(solution)/shard_map/scatter/ppermute | solution.py:335
  117.9 30.4 %copy-start.16 = (bf16[128,2048]{1,0:T(8,128)(2,1)S(1)}, bf16[128,2048]{1,0:T(8,128)(2,1)}, u32[]{:S(2)}) copy-start(bf16[128,2048]{1,0:T(8,128)(2,1)} %oc_ref.3) | copy-start | bytes 1572868
  118.7 40.1 %copy-start.5 = (bf16[2048,256]{1,0:T(8,128)(2,1)S(1)}, bf16[2048,256]{1,0:T(8,128)(2,1)}, u32[]{:S(2)}) copy-start(bf16[2048,256]{1,0:T(8,128)(2,1)} %w_ref.1) | copy-start | bytes 3145732
  118.7 40.1 %copy-start.19 = (f32[128,128]{1,0:T(8,128)S(1)}, f32[128,128]{1,0:T(8,128)}, u32[]{:S(2)}) copy-start(f32[128,128]{1,0:T(8,128)} %g_ref.5) | copy-start | bytes 196612
  118.7 40.1 %copy-start.21 = (bf16[128,128]{1,0:T(8,128)(2,1)S(1)}, bf16[128,128]{1,0:T(8,128)(2,1)}, u32[]{:S(2)}) copy-start(bf16[128,128]{1,0:T(8,128)(2,1)} %qry_ref.3) | copy-start | bytes 98308
  149.0 8.0 %collective-permute-start.9 = (bf16[128,512]{1,0:T(8,128)(2,1)S(1)}, bf16[128,512]{1,0:T(8,128)(2,1)S(1)}, u32[]{:S(2)}, u32[]{:S(2)}) collective-permute-start(bf16[128,512]{1,0:T(8,128)(2,1)S(1)} %back.3.m0_ref), channel_id=1, source_target_pairs={{0,2},{1,3},{2,0},{3,1},{4,6},{5,7},{6,4},{7,5},{8,10},{9,11},{10,... | collective-permute-start | bytes 393224 | tf_op jit(solution)/shard_map/back/ppermute | solution.py:374
  151.2 7.6 %collective-permute-start.8 = (bf16[128,512]{1,0:T(8,128)(2,1)S(1)}, bf16[128,512]{1,0:T(8,128)(2,1)S(1)}, u32[]{:S(2)}, u32[]{:S(2)}) collective-permute-start(bf16[128,512]{1,0:T(8,128)(2,1)S(1)} %back.3.m0_ref), channel_id=1, source_target_pairs={{0,3},{1,0},{2,1},{3,2},{4,7},{5,4},{6,5},{7,6},{8,11},{9,8},{10,9... | collective-permute-start | bytes 393224 | tf_op jit(solution)/shard_map/back/ppermute | solution.py:373
  152.1 6.7 %collective-permute-start.7 = (bf16[128,512]{1,0:T(8,128)(2,1)S(1)}, bf16[128,512]{1,0:T(8,128)(2,1)S(1)}, u32[]{:S(2)}, u32[]{:S(2)}) collective-permute-start(bf16[128,512]{1,0:T(8,128)(2,1)S(1)} %back.3.m0_ref), channel_id=1, source_target_pairs={{0,1},{1,2},{2,3},{3,0},{4,5},{5,6},{6,7},{7,4},{8,9},{9,10},{10,1... | collective-permute-start | bytes 393224 | tf_op jit(solution)/shard_map/back/ppermute | solution.py:372
  157.0 3.2 %copy-start.8 = (bf16[128,512]{1,0:T(8,128)(2,1)}, bf16[128,512]{1,0:T(8,128)(2,1)S(1)}, u32[]{:S(2)}) copy-start(bf16[128,512]{1,0:T(8,128)(2,1)S(1)} %collective-permute-done.9.m3_ref) | copy-start | bytes 393220
  158.8 1.5 copy-start.10
  158.8 1.4 copy-start.12
  160.2 17.1 %copy-start.28 = (f32[128,256]{1,0:T(8,128)}, f32[128,256]{1,0:T(8,128)S(1)}, u32[]{:S(2)}) copy-start(f32[128,256]{1,0:T(8,128)S(1)} %get-tuple-element.45.h_ref) | copy-start | bytes 393220
  178.0 16.4 %all-to-all-start.4 = ((bf16[64,8,128]{2,1,0:T(8,128)(2,1)}), bf16[64,8,128]{2,1,0:T(8,128)(2,1)}, u32[]{:S(2)}, u32[]{:S(2)}) async-start(bf16[64,8,128]{2,1,0:T(8,128)(2,1)} %bitcast.31), calls=%async_computation.4 | async-start | bytes 262144 | tf_op jit(solution)/shard_map/suffix/all_to_all | solution.py:294
  194.4 34.2 %all-to-all-start.2 = ((bf16[64,32,256]{2,1,0:T(8,128)(2,1)}), bf16[64,32,256]{2,1,0:T(8,128)(2,1)}, u32[]{:S(2)}, u32[]{:S(2)}) async-start(bf16[64,32,256]{2,1,0:T(8,128)(2,1)} %bitcast.12), calls=%async_computation.2 | async-start | bytes 2097152 | tf_op jit(solution)/shard_map/out_proj/all_to_all | solution.py:390
  204.2 5.0 %copy-start.20 = (f32[128,128]{1,0:T(8,128)S(1)}, f32[128,128]{1,0:T(8,128)}, u32[]{:S(2)}) copy-start(f32[128,128]{1,0:T(8,128)} %g_ref.5) | copy-start | bytes 196612
  204.2 5.0 %copy-start.22 = (bf16[128,128]{1,0:T(8,128)(2,1)S(1)}, bf16[128,128]{1,0:T(8,128)(2,1)}, u32[]{:S(2)}) copy-start(bf16[128,128]{1,0:T(8,128)(2,1)} %qry_ref.3) | copy-start | bytes 98308
  204.2 5.0 %copy-start.29 = (f32[128,256]{1,0:T(8,128)S(1)}, f32[128,256]{1,0:T(8,128)}, u32[]{:S(2)}) copy-start(f32[128,256]{1,0:T(8,128)} %copy-done.28) | copy-start | bytes 393220
  204.2 5.0 %copy-start.31 = (bf16[128,256]{1,0:T(8,128)(2,1)S(1)}, bf16[128,256]{1,0:T(8,128)(2,1)}, u32[]{:S(2)}) copy-start(bf16[128,256]{1,0:T(8,128)(2,1)} %v_ref.3) | copy-start | bytes 196612
  204.2 5.0 %copy-start.33 = (bf16[128,128]{1,0:T(8,128)(2,1)S(1)}, bf16[128,128]{1,0:T(8,128)(2,1)}, u32[]{:S(2)}) copy-start(bf16[128,128]{1,0:T(8,128)(2,1)} %k_ref.3) | copy-start | bytes 98308
  (16 other events, 14.4 us)

commit v2 on v1

v2 whole, which is shorter than its diff:
```python
import functools

import jax
import jax.numpy as jnp
from jax import lax
from jax.experimental import pallas as pl
from jax.experimental.pallas import tpu as pltpu
from jax.sharding import PartitionSpec as P


BF = jnp.bfloat16
F32 = jnp.float32
HI = lax.Precision.HIGHEST

TOK = 128
EXPERTS = 64
CAP = 8
SLOTS = EXPERTS * CAP
WIDTH = 2048
QUART = 512
FF = 256
DK = 128
DV = 256
LANES = 128
HALF = 64


def dot(a, b, ca, cb, precision=None):
    return lax.dot_general(
        a, b, (((ca,), (cb,)), ((), ())), preferred_element_type=F32, precision=precision
    )


def iota(shape, dim):
    return lax.broadcasted_iota(jnp.int32, shape, dim)


def rounded(x):
    return x.astype(BF).astype(F32)


def lower_lanes(shape):
    return iota(shape, len(shape) - 1) < HALF


def call(kernel, out_shape, args, *, index, in_specs=None, flops=0, vmem=24, scratch=()):
    nbytes = sum(a.size * a.dtype.itemsize for a in args)
    nbytes += sum(o.size * o.dtype.itemsize for o in jax.tree.leaves(out_shape))

    def whole(a):
        rank = len(a.shape)
        return pl.BlockSpec(a.shape, lambda i, q: (0,) * rank)

    specs = [whole(a) if s is None else s for a, s in zip(args, in_specs or [None] * len(args))]
    return pl.pallas_call(
        kernel,
        out_shape=out_shape,
        grid_spec=pltpu.PrefetchScalarGridSpec(
            num_scalar_prefetch=1,
            grid=(1,),
            in_specs=specs,
            out_specs=jax.tree.map(whole, out_shape),
            scratch_shapes=scratch,
        ),
        compiler_params=pltpu.CompilerParams(vmem_limit_bytes=vmem * 2**20),
        cost_estimate=pl.CostEstimate(
            flops=int(flops), bytes_accessed=int(nbytes), transcendentals=0
        ),
    )(index, *args)


def in_hbm(a):
    return pltpu.with_memory_space_constraint(a, pltpu.HBM)


def sds(shape, dtype):
    return jax.ShapeDtypeStruct(shape, dtype)


def quarter_rows(q):
    return pl.ds(pl.multiple_of(q * QUART, QUART), QUART)


def cumulative_sum(g):
    lower = (iota((TOK, TOK), 0) >= iota((TOK, TOK), 1)).astype(F32)
    return dot(lower, g, 1, 0, HI)


def tiles_of(state, fill=None):
    out = []
    for b in range(4):
        t = state[:, LANES * (b // 2) : LANES * (b // 2 + 1)]
        r = pltpu.roll(t, HALF, 1)
        low, up = (t, r) if b % 2 == 0 else (r, t)
        upper = fill if fill is not None else up - rounded(up)
        tile = jnp.where(lower_lanes(t.shape), rounded(low), upper)
        out.append(tile.reshape(16, 8, LANES))
    return jnp.concatenate(out, axis=1).reshape(SLOTS, LANES)


def state_of(tiles, upper):
    other = pltpu.roll(tiles, HALF, 1)
    even, odd = (other, tiles) if upper else (tiles, other)
    even, odd = even.reshape(16, 32, LANES), odd.reshape(16, 32, LANES)
    low = lower_lanes((DK, LANES))
    halves = []
    for b in (0, 2):
        first = even[:, 8 * b : 8 * b + 8, :].reshape(DK, LANES)
        second = odd[:, 8 * b + 8 : 8 * b + 16, :].reshape(DK, LANES)
        halves.append(jnp.where(low, first, second))
    return jnp.concatenate(halves, axis=1)


def pick_kernel(q_ref, ids_ref, x_ref, rows_ref, pick_ref, slot_ref):
    expert = iota((EXPERTS, TOK), 0)
    id0, id1 = ids_ref[0:1, :], ids_ref[1:2, :]
    hit0, hit1 = expert == id0, expert == id1
    named = (hit0.astype(F32) + hit1.astype(F32)).astype(BF)
    before = (iota((TOK, TOK), 0) < iota((TOK, TOK), 1)).astype(F32).astype(BF)
    count = dot(named, before, 1, 0)
    rank0 = jnp.sum(jnp.where(hit0, count, 0.0), axis=0, keepdims=True)
    rank1 = jnp.sum(jnp.where(hit1, count, 0.0), axis=0, keepdims=True)
    slot0 = id0 * CAP + rank0.astype(jnp.int32)
    slot1 = id1 * CAP + rank1.astype(jnp.int32)
    slot_ref[0:1, :] = slot0
    slot_ref[1:2, :] = slot1
    slot = iota((SLOTS, TOK), 0)
    pick = ((slot == slot0).astype(F32) + (slot == slot1).astype(F32)).astype(BF)
    pick_ref[...] = pick
    rows_ref[...] = dot(pick, x_ref[...], 1, 0).astype(BF)


def local_kernel(
    q_ref, slot_ref, w_ref, pick_ref, oc_ref, qry_ref, k_ref, v_ref, g_ref,
    rows_ref, tile_ref, cum_ref, dec_ref,
):
    slot = iota((SLOTS, TOK), 0)
    at0, at1 = slot == slot_ref[0:1, :], slot == slot_ref[1:2, :]
    weight = jnp.sum(
        jnp.where(at0, w_ref[0:1, :], 0.0) + jnp.where(at1, w_ref[1:2, :], 0.0),
        axis=1,
        keepdims=True,
    )
    rows_ref[...] = (dot(pick_ref[...], oc_ref[...], 1, 0) * weight).astype(BF)
    g = g_ref[...]
    cum = cumulative_sum(g)
    cum_ref[...] = cum
    dec_ref[...] = qry_ref[...].astype(F32) * jnp.exp(cum)
    to_end = k_ref[...].astype(F32) * jnp.exp(cum[TOK - 1 : TOK, :] - cum)
    state = dot(to_end.T, v_ref[...].astype(F32), 1, 0, HI)
    factor = jnp.exp(jnp.sum(g.T, axis=1, keepdims=True))
    high = rounded(factor)
    fill = jnp.where(iota((DK, LANES), 1) < 96, high, factor - high)
    tile_ref[...] = tiles_of(state, fill).astype(BF)


def gate_kernel(q_ref, x0_ref, x1_ref, x2_ref, x3_ref, wg_ref, wu_ref, g_ref, u_ref):
    g = u = None
    for n, ref in enumerate((x0_ref, x1_ref, x2_ref, x3_ref)):
        rows = quarter_rows(q_ref[n])
        x = ref[...]
        g1, u1 = dot(x, wg_ref[rows, :], 1, 0), dot(x, wu_ref[rows, :], 1, 0)
        g, u = (g1, u1) if g is None else (g + g1, u + u1)
    g_ref[...] = g
    u_ref[...] = u


def near_kernel(q_ref, y0_ref, y1_ref, y2_ref, wd_ref, h_ref):
    h = None
    for n, ref in enumerate((y0_ref, y1_ref, y2_ref)):
        h1 = dot(ref[...], wd_ref[:, quarter_rows(q_ref[n])], 1, 1)
        h = h1 if h is None else h + h1
    h_ref[...] = h


def far_kernel(
    q_ref, g_ref, u_ref, h_ref, top_ref, bot_ref, wg_ref, wu_ref, wd_ref,
    far_ref, right_ref, left_ref, own_ref, hid_ref, gu_ref,
):
    dy = jnp.concatenate([top_ref[...], bot_ref[...]], axis=0)
    g, u = g_ref[...], u_ref[...]
    h = h_ref[...] + dot(dy, wd_ref[:, quarter_rows(q_ref[3])], 1, 1)
    sig = jax.nn.sigmoid(g)
    hid_ref[...] = (g * sig * u).astype(BF)
    gate_cot = (h * u * sig * (1.0 + g * (1.0 - sig))).astype(BF)
    up_cot = (h * g * sig).astype(BF)
    gu_ref[:, :FF] = gate_cot
    gu_ref[:, FF:] = up_cot
    for n, ref in ((3, far_ref), (2, right_ref), (1, left_ref), (0, own_ref)):
        rows = quarter_rows(q_ref[n])
        part = dot(gate_cot, wg_ref[rows, :], 1, 1) + dot(up_cot, wu_ref[rows, :], 1, 1)
        ref[...] = part.astype(BF)


def weight_kernel(
    q_ref, x0_ref, x1_ref, x2_ref, x3_ref, y0_ref, y1_ref, y2_ref, top_ref, bot_ref,
    hid_ref, gu_ref, gg_ref, gup_ref, gd_ref,
):
    hid_t = hid_ref[...].T
    gu = gu_ref[...]
    far = jnp.concatenate([top_ref[...], bot_ref[...]], axis=0)
    cots = (y0_ref[...], y1_ref[...], y2_ref[...], far)
    for n, ref in enumerate((x0_ref, x1_ref, x2_ref, x3_ref)):
        rows = quarter_rows(q_ref[n])
        both = dot(ref[...].T, gu, 1, 0)
        gg_ref[rows, :] = both[:, :FF]
        gup_ref[rows, :] = both[:, FF:]
        gd_ref[:, rows] = dot(hid_t, cots[n], 1, 0)


def sum_kernel(q_ref, p0_ref, p1_ref, p2_ref, p3_ref, out_ref):
    total = p0_ref[...].astype(F32) + p1_ref[...].astype(F32)
    out_ref[...] = (total + p2_ref[...].astype(F32) + p3_ref[...].astype(F32)).astype(BF)


def combine_kernel(q_ref, rows_ref, pick_ref, oc_ref, out_ref):
    routed = dot(pick_ref[...].T, rows_ref[...], 1, 0)
    out_ref[...] = (oc_ref[...].astype(F32) + routed).astype(BF)


def head_kernel(
    q_ref, m0_ref, m1_ref, m2_ref, m3_ref, w_ref, dec_ref, tile_ref, h_ref, pay_ref
):
    head = None
    for n, ref in enumerate((m0_ref, m1_ref, m2_ref, m3_ref)):
        part = dot(ref[...], w_ref[quarter_rows(q_ref[n]), :], 1, 0)
        head = part if head is None else head + part
    h_ref[...] = head
    pay_ref[:, :LANES] = tiles_of(dot(dec_ref[...].T, head, 1, 0, HI)).astype(BF)
    pay_ref[:, LANES:] = tile_ref[...]


def out_proj_kernel(q_ref, m0_ref, m1_ref, m2_ref, m3_ref, mixed_ref, keep_ref, give_ref):
    mixed = mixed_ref[...]
    first = q_ref[4] == 0
    for n, ref in enumerate((m0_ref, m1_ref, m2_ref, m3_ref)):
        part = dot(ref[...].T, mixed, 1, 0).reshape(16, 32, DV)
        low = part[:, :16, :].reshape(256, DV)
        high = part[:, 16:, :].reshape(256, DV)
        rows = pl.ds(pl.multiple_of(q_ref[n] * 256, 256), 256)
        keep_ref[rows, :] = jnp.where(first, low, high).astype(BF)
        give_ref[rows, :] = jnp.where(first, high, low).astype(BF)


def split_kernel(q_ref, keep_ref, got_ref, o0_ref, o1_ref, o2_ref, o3_ref):
    total = (keep_ref[...].astype(F32) + got_ref[...].astype(F32)).reshape(64, 16, DV)
    tile = [
        total[:, 8 * (n // 2) : 8 * (n // 2) + 8, LANES * (n % 2) : LANES * (n % 2) + LANES]
        for n in range(4)
    ]
    tile = [t.reshape(SLOTS, LANES) for t in tile]
    y = q_ref[5]
    for k, ref in enumerate((o0_ref, o1_ref, o2_ref, o3_ref)):
        out = tile[k]
        for n in range(1, 4):
            out = jnp.where(y == n, tile[(n + k) % 4], out)
        ref[...] = out.astype(BF)


def scan_kernel(
    q_ref, in_ref, o_ref, r1_ref, r2_ref, r3_ref, out_ref, factor_ref, pre_ref, suf_ref
):
    pull = in_ref[:, :LANES].astype(F32)
    suf_ref[...] = pull + pltpu.roll(pull, HALF, 1)
    tile = in_ref[:, LANES:].astype(F32)
    pre_ref[...] = pltpu.roll(tile, HALF, 1)
    factor_ref[...] = jnp.broadcast_to(tile[:, 64:65] + tile[:, 96:97], tile.shape)
    before = after = jnp.zeros((8, LANES), F32)
    for s in range(EXPERTS):
        rows = slice(8 * s, 8 * s + 8)
        now = pre_ref[rows, :]
        pre_ref[rows, :] = before
        before = before * factor_ref[rows, :] + now
        e = EXPERTS - 1 - s
        rows = slice(8 * e, 8 * e + 8)
        now = suf_ref[rows, :]
        suf_ref[rows, :] = after
        after = after * factor_ref[rows, :] + now
    suf = suf_ref[...]
    out_ref[:, :LANES] = jnp.where(lower_lanes(suf.shape), suf, pre_ref[...]).astype(BF)
    total = o_ref[...].astype(F32) + r1_ref[...].astype(F32)
    out_ref[:, LANES:] = (total + r2_ref[...].astype(F32) + r3_ref[...].astype(F32)).astype(BF)


def inside_kernel(
    q_ref, k_ref, v_ref, cum_ref, dec_ref, h_ref, dq_ref, dk_ref, dv_ref
):
    k, v, q_dec, head = k_ref[...].astype(F32), v_ref[...].astype(F32), dec_ref[...], h_ref[...]
    k_grown = k * jnp.exp(-cum_ref[...])
    causal = iota((TOK, TOK), 0) >= iota((TOK, TOK), 1)
    score = jnp.where(causal, dot(q_dec, k_grown, 1, 1, HI), 0.0)
    d_score = jnp.where(causal, dot(head, v, 1, 1, HI), 0.0)
    dq_ref[...] = dot(d_score, k_grown, 1, 0, HI)
    dk_ref[...] = dot(d_score.T, q_dec, 1, 0, HI)
    dv_ref[...] = dot(score.T, head, 1, 0, HI)


def last_kernel(
    q_ref, k_ref, v_ref, cum_ref, dec_ref, h_ref, dq_ref, dk_ref, dv_ref, in_ref,
    gq_ref, gk_ref, gv_ref, gg_ref, go_ref,
):
    tiles = in_ref[:, :LANES].astype(F32)
    cot, state = state_of(tiles, False), state_of(tiles, True)
    k, v, head, cum = k_ref[...].astype(F32), v_ref[...].astype(F32), h_ref[...], cum_ref[...]
    last = cum[TOK - 1 : TOK, :]
    shrink, to_end = jnp.exp(-cum), jnp.exp(last - cum)
    k_end = k * to_end
    d_q = dq_ref[...] + dot(head, state, 1, 1, HI)
    d_kg = dk_ref[...]
    d_ke = dot(v, cot, 1, 1, HI)
    gq_ref[...] = (d_q * jnp.exp(cum)).astype(BF)
    gk_ref[...] = (d_kg * shrink + d_ke * to_end).astype(BF)
    gv_ref[...] = (dv_ref[...] + dot(k_end, cot, 1, 0, HI)).astype(BF)
    end = d_ke * k_end
    d_cum = d_q * dec_ref[...] - d_kg * (k * shrink) - end
    carried = jnp.sum((state * cot).T, axis=0, keepdims=True)
    d_last = jnp.sum(end, axis=0, keepdims=True) + jnp.exp(last) * carried
    upper = (iota((TOK, TOK), 0) <= iota((TOK, TOK), 1)).astype(F32)
    gg_ref[...] = dot(upper, d_cum, 1, 0, HI) + d_last
    parts = jnp.sum(in_ref[:, LANES:].astype(F32).reshape(8, EXPERTS, LANES), axis=0)
    for y in range(4):
        for core in range(2):
            n = 8 * (2 * y + core)
            rows = 16 * core + 8 * (y // 2)
            lanes = LANES * (y % 2)
            go_ref[rows : rows + 8, lanes : lanes + LANES] = parts[n : n + 8, :]


def per_device(
    expert_in, out_cot, route_ids, route_weights, w_gate, w_up, w_down, w_out,
    mixed_heads, queries, keys, values, log_decay,
):
    me, sp = lax.axis_index("tp"), lax.axis_index("sp")
    table = [
        [i, (i + 3) % 4, (i + 1) % 4, (i + 2) % 4, s % 2, s // 2] for s in range(8) for i in range(4)
    ]
    place = lax.rem(sp, 8) * 4 + me
    order = lax.dynamic_slice(jnp.array(table, jnp.int32).reshape(-1), (place * 6,), (6,))
    to_right = [(i, (i + 1) % 4) for i in range(4)]
    to_left = [(i, (i + 3) % 4) for i in range(4)]
    across = [(i, (i + 2) % 4) for i in range(4)]
    other_core = [(i, i ^ 1) for i in range(64)]

    def along_y(k):
        return [(i, i // 8 * 8 + (i + 2 * k) % 8) for i in range(64)]

    wg, wu, wd = w_gate[0], w_up[0], w_down[0]
    run = functools.partial(call, index=order)

    def exchange(rows):
        width = rows.shape[1]
        got = lax.all_to_all(rows.reshape(EXPERTS, CAP, width), "sp", 0, 0, tiled=True)
        return got.reshape(SLOTS, width)

    def quarter_block():
        return pl.BlockSpec((TOK, QUART), lambda i, q: (0, q[0]))

    rows_type = sds((SLOTS, QUART), BF)
    tile_type = sds((SLOTS, LANES), BF)
    x_rows, pick, slots = run(
        pick_kernel,
        (rows_type, sds((SLOTS, TOK), BF), sds((2, TOK), jnp.int32)),
        (route_ids.T, in_hbm(expert_in)),
        in_specs=[None, quarter_block()],
        flops=1e8,
    )
    y_rows, state_tile, cum, q_dec = run(
        local_kernel,
        (rows_type, tile_type, sds((TOK, DK), F32), sds((TOK, DK), F32)),
        (
            slots, route_weights.T, pick, in_hbm(out_cot), in_hbm(queries), in_hbm(keys),
            in_hbm(values), in_hbm(log_decay),
        ),
        in_specs=[None, None, None, quarter_block(), None, None, None, None],
        flops=3e8,
    )
    x0 = exchange(x_rows)
    x0, y_rows = lax.optimization_barrier((x0, y_rows))
    x3 = lax.ppermute(x0, "tp", across)
    x1 = lax.ppermute(x0, "tp", to_right)
    x2 = lax.ppermute(x0, "tp", to_left)
    y0 = exchange(y_rows)
    y1 = lax.ppermute(y0, "tp", to_right)
    y2 = lax.ppermute(y0, "tp", to_left)
    far_top = lax.ppermute(y1[: SLOTS // 2], "tp", to_right)
    far_bottom = lax.ppermute(y2[SLOTS // 2 :], "tp", to_left)
    g, u = run(
        gate_kernel, (sds((SLOTS, FF), F32),) * 2, (x0, x1, x2, x3, wg, wu), flops=1.1e9
    )
    h = run(near_kernel, sds((SLOTS, FF), F32), (y0, y1, y2, wd), flops=4e8)
    p_far, p_right, p_left, p_own, hidden, gate_up = run(
        far_kernel,
        (rows_type,) * 4 + (sds((SLOTS, FF), BF), sds((SLOTS, 2 * FF), BF)),
        (g, u, h, far_top, far_bottom, wg, wu, wd),
        flops=1.3e9,
    )
    r_far = lax.ppermute(p_far, "tp", across)
    r_left = lax.ppermute(p_right, "tp", to_right)
    r_right = lax.ppermute(p_left, "tp", to_left)
    grads = run(
        weight_kernel,
        (sds((WIDTH, FF), F32), sds((WIDTH, FF), F32), sds((FF, WIDTH), F32)),
        (x0, x1, x2, x3, y0, y1, y2, far_top, far_bottom, hidden, gate_up),
        flops=1.6e9,
    )
    p_own, grads = lax.optimization_barrier((p_own, grads))
    grad_gate, grad_up, grad_down = grads
    total = run(sum_kernel, rows_type, (p_own, r_far, r_left, r_right), flops=1e6)
    back = exchange(total)
    mid = run(
        combine_kernel,
        sds((TOK, QUART), BF),
        (back, pick, out_cot),
        in_specs=[None, None, quarter_block()],
        flops=7e7,
    )
    m_far = lax.ppermute(mid, "tp", across)
    m_left = lax.ppermute(mid, "tp", to_right)
    m_right = lax.ppermute(mid, "tp", to_left)
    mids = (mid, m_left, m_right, m_far)
    head, pay = run(
        head_kernel,
        (sds((TOK, DV), F32), sds((SLOTS, 2 * LANES), BF)),
        (*mids, w_out, q_dec, state_tile),
        flops=2e8,
    )
    pulled = exchange(pay)
    keep, give = run(out_proj_kernel, (sds((1024, DV), BF),) * 2, (*mids, mixed_heads), flops=1.4e8)
    got = lax.ppermute(give, "sp", other_core)
    tiles = run(split_kernel, (tile_type,) * 4, (keep, got), flops=1e6)
    adds = [lax.ppermute(tiles[k], "sp", along_y(k)) for k in (2, 1, 3)]
    pay = run(
        scan_kernel,
        sds((SLOTS, 2 * LANES), BF),
        (pulled, tiles[0], *adds),
        flops=1e8,
        scratch=[pltpu.VMEM((SLOTS, LANES), F32)] * 3,
    )
    back_states = exchange(pay)
    d_in = run(
        inside_kernel,
        (sds((TOK, DK), F32), sds((TOK, DK), F32), sds((TOK, DV), F32)),
        (keys, values, cum, q_dec, head),
        flops=3e8,
    )
    grad_queries, grad_keys, grad_values, grad_decay, grad_out_proj = run(
        last_kernel,
        (
            sds((TOK, DK), BF),
            sds((TOK, DK), BF),
            sds((TOK, DV), BF),
            sds((TOK, DK), F32),
            sds((32, DV), F32),
        ),
        (keys, values, cum, q_dec, head, *d_in, back_states),
        flops=3e8,
    )
    return (
        grad_gate[None],
        grad_up[None],
        grad_down[None],
        grad_out_proj,
        grad_queries,
        grad_keys,
        grad_values,
        grad_decay,
    )


def solution(mesh):
    return jax.shard_map(
        per_device,
        mesh=mesh,
        in_specs=(
            P("sp", None),
            P("sp", None),
            P("sp", None),
            P("sp", None),
            P("sp", None, "tp"),
            P("sp", None, "tp"),
            P("sp", "tp", None),
            P(None, "tp"),
            P("sp", "tp"),
            P("sp", "tp"),
            P("sp", "tp"),
            P("sp", "tp"),
            P("sp", "tp"),
        ),
        out_specs=(
            P("sp", None, "tp"),
            P("sp", None, "tp"),
            P("sp", "tp", None),
            P("sp", "tp"),
            P("sp", "tp"),
            P("sp", "tp"),
            P("sp", "tp"),
            P("sp", "tp"),
        ),
        check_vma=False,
    )
```

time: 234 us -> 214 us (0.915)
  blocking collectives: 89.4 us -> 46.2 us
  starting transfers between devices: 23.6 us -> 60.6 us
  local copies, waits for them, and re-layouts: 14.6 us -> 2.18 us
  Pallas kernels: 21.2 us -> 25.6 us
  waiting for transfers between devices: 78.2 us -> 75.4 us
  other arithmetic: 2.68 us -> 0 us
    all_to_all x3 -> x2, blocking collectives: 89.4 us -> 46.2 us  [exchange(): lax.all_to_all(rows.reshape(EXPERTS, CAP, width), 'sp', 0, 0, tiled=True)]
    all_to_all x1 -> x3, waiting for transfers between devices: 5.42 us -> 31.7 us  [exchange(): lax.all_to_all(rows.reshape(EXPERTS, CAP, width), 'sp', 0, 0, tiled=True)]
    ppermute x4 -> x11, starting transfers between devices: 3.94 us -> 25.7 us  [the longest x1 11.2 us: per_device(): far_bottom = lax.ppermute(y2[SLOTS // 2:], 'tp', to_left)]
    all_to_all x1 -> x3, starting transfers between devices: 5.43 us -> 26.3 us  [exchange(): lax.all_to_all(rows.reshape(EXPERTS, CAP, width), 'sp', 0, 0, tiled=True)]
    all_to_all x1 -> x0, waiting for transfers between devices: 15.9 us -> none  [per_device(): parts = lax.all_to_all(part.reshape(64, 32, DV), 'sp', 0, 0, tiled=True)]
    unnamed x72 -> x20, local copies, waits for them, and re-layouts: 14.4 us -> 1.39 us
    ppermute x4 -> x11, waiting for transfers between devices: 32.8 us -> 21.4 us  [the longest x1 9.86 us: per_device(): x2 = lax.ppermute(x0, 'tp', to_left)]
    pallas_call x9 -> x14, Pallas kernels: 19.5 us -> 25.6 us  [call(): pl.pallas_call(kernel, out_shape=out_shape, grid_spec=pltpu.PrefetchScala...]
  transfers between devices with their start and end apart: 12 -> 20, of which waited for: 11 -> 14; matrix products, arithmetic and copies ran while one was open for 0% -> 0% of each run, Pallas kernels for 6% -> 7%
where the time goes in v2:
time: 214 us; the launch traced here: 211 us
  waiting for transfers between devices  75.4 us (35%)
  starting transfers between devices  60.6 us (28%)
  blocking collectives  46.2 us (22%)
  Pallas kernels  25.6 us (12%)
  local copies, waits for them, and re-layouts  2.18 us (1%)
    all_to_all x2, blocking collectives, exchange(): lax.all_to_all(rows.reshape(EXPERTS, CAP, width), 'sp', 0, 0, tiled=True)  46.2 us
    all_to_all x3, waiting for transfers between devices, exchange(): lax.all_to_all(rows.reshape(EXPERTS, CAP, width), 'sp', 0, 0, tiled=True)  31.7 us
    all_to_all x3, starting transfers between devices, exchange(): lax.all_to_all(rows.reshape(EXPERTS, CAP, width), 'sp', 0, 0, tiled=True)  26.3 us
    pallas_call x14, Pallas kernels, call(): pl.pallas_call(kernel, out_shape=out_shape, grid_spec=pltpu.PrefetchScala...  25.6 us
    ppermute x1, starting transfers between devices, per_device(): far_bottom = lax.ppermute(y2[SLOTS // 2:], 'tp', to_left)  11.2 us
    ppermute x1, waiting for transfers between devices, per_device(): x2 = lax.ppermute(x0, 'tp', to_left)  9.86 us
    ppermute x1, waiting for transfers between devices, per_device(): r_left = lax.ppermute(p_right, 'tp', to_right)  8.91 us
    ppermute x1, waiting for transfers between devices, per_device(): y2 = lax.ppermute(y0, 'tp', to_left)  8.18 us
  transfers between devices with their start and end apart: 20, of which 14 were waited for; matrix products, arithmetic and copies ran while one was open for 0% of the time, Pallas kernels for 7%

profile of v2, /device:TPU:2, one launch (start us, length us, event | category | flops | bytes accessed | tf_op | source)
XLA Modules:
  0.0 210.8 jit_solution(749929428366128164)
XLA Ops:
  2.1 2.7 %shard_map.197 = (bf16[512,512]{1,0:T(8,128)(2,1)}, bf16[512,128]{1,0:T(8,128)(2,1)S(1)}, s32[2,128]{1,0:T(2,128)S(1)}) custom-call(s32[6]{0:T(128)S(1)} %dynamic_slice.3.q_ref, s32[2,128]{1,0:T(2,128)S(1)} %bitcast.38, bf16[128,2048]{1,0:T(8,128)(2,1)} %x_ref.1), custom_call_target="tpu_custom_call" | custom-call | flops 100000000 | bytes 1181696 | tf_op jit(solution)/shard_map/pallas_call | solution.py:55
  4.8 12.2 %all-to-all-start = ((bf16[64,8,512]{2,1,0:T(8,128)(2,1)}), bf16[64,8,512]{2,1,0:T(8,128)(2,1)S(1)}, u32[]{:S(2)}, u32[]{:S(2)}) async-start(bf16[64,8,512]{2,1,0:T(8,128)(2,1)} %bitcast.1), calls=%async_computation | async-start | bytes 1048576 | tf_op jit(solution)/shard_map/all_to_all | solution.py:352
  17.7 2.4 %shard_map.198 = (bf16[512,512]{1,0:T(8,128)(2,1)S(1)}, bf16[512,128]{1,0:T(8,128)(2,1)S(1)}, f32[128,128]{1,0:T(8,128)S(1)}, f32[128,128]{1,0:T(8,128)S(1)}) custom-call(s32[6]{0:T(128)S(1)} %dynamic_slice.3.q_ref, s32[2,128]{1,0:T(2,128)S(1)} %get-tuple-element.49.slot_ref, f32[2,128]{1,0:T(2,128)S(1)} %bitcast.39, ...), custom_call_target="tpu_custom_call" | custom-call | flops 300000000 | bytes 1640448 | tf_op jit(solution)/shard_map/pallas_call | solution.py:55
  20.1 14.5 %all-to-all-done = bf16[64,8,512]{2,1,0:T(8,128)(2,1)S(1)} async-done(((bf16[64,8,512]{2,1,0:T(8,128)(2,1)}), bf16[64,8,512]{2,1,0:T(8,128)(2,1)S(1)}, u32[]{:S(2)}, u32[]{:S(2)}) %all-to-all-start) | async-done | bytes 524320 | tf_op jit(solution)/shard_map/all_to_all | solution.py:352
  34.6 23.2 %all_to_all.25 = bf16[64,8,512]{2,1,0:T(8,128)(2,1)S(1)} all-to-all(bf16[64,8,512]{2,1,0:T(8,128)(2,1)S(1)} %bitcast.36), channel_id=1, replica_groups=mesh['sp'=64,'tp'=4] {'sp'}, dimensions={0} | all-to-all | bytes 1048576 | tf_op jit(solution)/shard_map/all_to_all | solution.py:352
  58.3 1.5 collective-permute-start.3
  59.8 3.3 %collective-permute-start.2 = (bf16[512,512]{1,0:T(8,128)(2,1)S(1)}, bf16[512,512]{1,0:T(8,128)(2,1)S(1)}, u32[]{:S(2)}, u32[]{:S(2)}) collective-permute-start(bf16[512,512]{1,0:T(8,128)(2,1)S(1)} %bitcast.24), channel_id=1, source_target_pairs={{0,2},{1,3},{2,0},{3,1},{4,6},{5,7},{6,4},{7,5},{8,10},{9,11},{10,... | collective-permute-start | bytes 1572872 | tf_op jit(solution)/shard_map/ppermute | solution.py:379
  63.4 1.8 collective-permute-start
  65.2 8.2 %collective-permute-done.4.y2_ref = bf16[512,512]{1,0:T(8,128)(2,1)S(1)} collective-permute-done((bf16[512,512]{1,0:T(8,128)(2,1)S(1)}, bf16[512,512]{1,0:T(8,128)(2,1)S(1)}, u32[]{:S(2)}, u32[]{:S(2)}) %collective-permute-start.4) | collective-permute-done | bytes 524320 | tf_op jit(solution)/shard_map/ppermute | solution.py:384
  73.4 11.2 %collective-permute-start.6 = (bf16[256,512]{1,0:T(8,128)(2,1)S(1)}, bf16[256,512]{1,0:T(8,128)(2,1)S(1)}, u32[]{:S(2)}, u32[]{:S(2)}) collective-permute-start(bf16[256,512]{1,0:T(8,128)(2,1)S(1)} %slice.9), channel_id=1, source_target_pairs={{0,3},{1,0},{2,1},{3,2},{4,7},{5,4},{6,5},{7,6},{8,11},{9,8},{10,9... | collective-permute-start | bytes 786440 | tf_op jit(solution)/shard_map/ppermute | solution.py:386
  85.2 9.9 %collective-permute-done.1.x2_ref = bf16[512,512]{1,0:T(8,128)(2,1)S(1)} collective-permute-done((bf16[512,512]{1,0:T(8,128)(2,1)S(1)}, bf16[512,512]{1,0:T(8,128)(2,1)S(1)}, u32[]{:S(2)}, u32[]{:S(2)}) %collective-permute-start.1) | collective-permute-done | bytes 524320 | tf_op jit(solution)/shard_map/ppermute | solution.py:381
  96.4 1.8 shard_map.199
  101.1 2.1 shard_map.201
  103.3 2.1 %collective-permute-start.7 = (bf16[512,512]{1,0:T(8,128)(2,1)S(1)}, bf16[512,512]{1,0:T(8,128)(2,1)S(1)}, u32[]{:S(2)}, u32[]{:S(2)}) collective-permute-start(bf16[512,512]{1,0:T(8,128)(2,1)S(1)} %get-tuple-element.68), channel_id=1, source_target_pairs={{0,2},{1,3},{2,0},{3,1},{4,6},{5,7},{6,4},{7,5},{8,10},{9,11},{10,... | collective-permute-start | bytes 1572872 | tf_op jit(solution)/shard_map/ppermute | solution.py:397
  105.4 2.3 %collective-permute-start.8 = (bf16[512,512]{1,0:T(8,128)(2,1)S(1)}, bf16[512,512]{1,0:T(8,128)(2,1)S(1)}, u32[]{:S(2)}, u32[]{:S(2)}) collective-permute-start(bf16[512,512]{1,0:T(8,128)(2,1)S(1)} %get-tuple-element.69), channel_id=1, source_target_pairs={{0,1},{1,2},{2,3},{3,0},{4,5},{5,6},{6,7},{7,4},{8,9},{9,10},{10,1... | collective-permute-start | bytes 1572872 | tf_op jit(solution)/shard_map/ppermute | solution.py:398
  107.7 4.9 %shard_map.202 = (f32[2048,256]{1,0:T(8,128)}, f32[2048,256]{1,0:T(8,128)}, f32[256,2048]{1,0:T(8,128)}) custom-call(s32[6]{0:T(128)S(1)} %dynamic_slice.3.q_ref, bf16[512,512]{1,0:T(8,128)(2,1)S(1)} %bitcast.28, bf16[512,512]{1,0:T(8,128)(2,1)S(1)} %collective-permute-done.x1_ref, bf16[512,512]{1,0:T(8,128)(2,1)S(1)} %collective-permute-done.1.x2_ref, ...), custom_call_target="tpu_custom_call" | custom-call | flops 1600000000 | bytes 11272192 | tf_op jit(solution)/shard_map/pallas_call | solution.py:55
  112.7 7.0 %collective-permute-done.7.p1_ref = bf16[512,512]{1,0:T(8,128)(2,1)S(1)} collective-permute-done((bf16[512,512]{1,0:T(8,128)(2,1)S(1)}, bf16[512,512]{1,0:T(8,128)(2,1)S(1)}, u32[]{:S(2)}, u32[]{:S(2)}) %collective-permute-start.7) | collective-permute-done | bytes 524320 | tf_op jit(solution)/shard_map/ppermute | solution.py:397
  119.7 8.9 %collective-permute-done.8.p2_ref = bf16[512,512]{1,0:T(8,128)(2,1)S(1)} collective-permute-done((bf16[512,512]{1,0:T(8,128)(2,1)S(1)}, bf16[512,512]{1,0:T(8,128)(2,1)S(1)}, u32[]{:S(2)}, u32[]{:S(2)}) %collective-permute-start.8) | collective-permute-done | bytes 524320 | tf_op jit(solution)/shard_map/ppermute | solution.py:398
  130.0 23.0 %all_to_all.26 = bf16[64,8,512]{2,1,0:T(8,128)(2,1)S(1)} all-to-all(bf16[64,8,512]{2,1,0:T(8,128)(2,1)S(1)} %bitcast.34), channel_id=1, replica_groups=mesh['sp'=64,'tp'=4] {'sp'}, dimensions={0} | all-to-all | bytes 1048576 | tf_op jit(solution)/shard_map/all_to_all | solution.py:352
  153.8 2.2 %collective-permute-start.12 = (bf16[128,512]{1,0:T(8,128)(2,1)S(1)}, bf16[128,512]{1,0:T(8,128)(2,1)S(1)}, u32[]{:S(2)}, u32[]{:S(2)}) collective-permute-start(bf16[128,512]{1,0:T(8,128)(2,1)S(1)} %shard_map.204.m0_ref), channel_id=1, source_target_pairs={{0,2},{1,3},{2,0},{3,1},{4,6},{5,7},{6,4},{7,5},{8,10},{9,11},{10,... | collective-permute-start | bytes 393224 | tf_op jit(solution)/shard_map/ppermute | solution.py:417
  158.0 3.8 %collective-permute-done.12.m3_ref = bf16[128,512]{1,0:T(8,128)(2,1)S(1)} collective-permute-done((bf16[128,512]{1,0:T(8,128)(2,1)S(1)}, bf16[128,512]{1,0:T(8,128)(2,1)S(1)}, u32[]{:S(2)}, u32[]{:S(2)}) %collective-permute-start.12) | collective-permute-done | bytes 131104 | tf_op jit(solution)/shard_map/ppermute | solution.py:417
  161.8 1.9 collective-permute-done.11.m2_ref
  164.9 2.0 shard_map.205
  167.0 5.5 %all-to-all-start.3 = ((bf16[64,8,256]{2,1,0:T(8,128)(2,1)}), bf16[64,8,256]{2,1,0:T(8,128)(2,1)S(1)}, u32[]{:S(2)}, u32[]{:S(2)}) async-start(bf16[64,8,256]{2,1,0:T(8,128)(2,1)} %bitcast.14), calls=%async_computation.3 | async-start | bytes 524288 | tf_op jit(solution)/shard_map/all_to_all | solution.py:352
  173.3 3.2 %collective-permute-start.14 = (bf16[512,128]{1,0:T(8,128)(2,1)S(1)}, bf16[512,128]{1,0:T(8,128)(2,1)S(1)}, u32[]{:S(2)}, u32[]{:S(2)}) collective-permute-start(bf16[512,128]{1,0:T(8,128)(2,1)S(1)} %get-tuple-element.80), channel_id=1, source_target_pairs={{0,16},{4,20},{8,24},{12,28},{16,0},{20,4},{24,8},{28,12},{32,48},... | collective-permute-start | bytes 393224 | tf_op jit(solution)/shard_map/ppermute | solution.py:431
  177.0 2.7 %collective-permute-start.16 = (bf16[512,128]{1,0:T(8,128)(2,1)S(1)}, bf16[512,128]{1,0:T(8,128)(2,1)S(1)}, u32[]{:S(2)}, u32[]{:S(2)}) collective-permute-start(bf16[512,128]{1,0:T(8,128)(2,1)S(1)} %get-tuple-element.82), channel_id=1, source_target_pairs={{0,24},{4,28},{8,0},{12,4},{16,8},{20,12},{24,16},{28,20},{32,56},... | collective-permute-start | bytes 393224 | tf_op jit(solution)/shard_map/ppermute | solution.py:431
  179.7 5.7 %all-to-all-done.3 = bf16[64,8,256]{2,1,0:T(8,128)(2,1)S(1)} async-done(((bf16[64,8,256]{2,1,0:T(8,128)(2,1)}), bf16[64,8,256]{2,1,0:T(8,128)(2,1)S(1)}, u32[]{:S(2)}, u32[]{:S(2)}) %all-to-all-start.3) | async-done | bytes 262176 | tf_op jit(solution)/shard_map/all_to_all | solution.py:352
  185.6 1.7 shard_map.209
  187.3 8.6 %all-to-all-start.4 = ((bf16[64,8,256]{2,1,0:T(8,128)(2,1)}), bf16[64,8,256]{2,1,0:T(8,128)(2,1)S(1)}, u32[]{:S(2)}, u32[]{:S(2)}) async-start(bf16[64,8,256]{2,1,0:T(8,128)(2,1)} %bitcast.16), calls=%async_computation.4 | async-start | bytes 524288 | tf_op jit(solution)/shard_map/all_to_all | solution.py:352
  196.0 1.4 shard_map.206
  197.3 11.5 %all-to-all-done.4 = bf16[64,8,256]{2,1,0:T(8,128)(2,1)S(1)} async-done(((bf16[64,8,256]{2,1,0:T(8,128)(2,1)}), bf16[64,8,256]{2,1,0:T(8,128)(2,1)S(1)}, u32[]{:S(2)}, u32[]{:S(2)}) %all-to-all-start.4) | async-done | bytes 262176 | tf_op jit(solution)/shard_map/all_to_all | solution.py:352
  208.8 1.9 shard_map.210
  (47 shorter events, 14.8 us)
Async XLA Ops:
  1.4 0.7 copy-start.6
  4.8 91.6 %copy-start = (bf16[1,2048,256]{2,1,0:T(8,128)(2,1)S(1)}, bf16[1,2048,256]{2,1,0:T(8,128)(2,1)}, u32[]{:S(2)}) copy-start(bf16[1,2048,256]{2,1,0:T(8,128)(2,1)} %param.18) | copy-start | bytes 3145732
  4.8 91.6 %copy-start.1 = (bf16[1,2048,256]{2,1,0:T(8,128)(2,1)S(1)}, bf16[1,2048,256]{2,1,0:T(8,128)(2,1)}, u32[]{:S(2)}) copy-start(bf16[1,2048,256]{2,1,0:T(8,128)(2,1)} %param.19) | copy-start | bytes 3145732
  4.8 29.9 %all-to-all-start = ((bf16[64,8,512]{2,1,0:T(8,128)(2,1)}), bf16[64,8,512]{2,1,0:T(8,128)(2,1)S(1)}, u32[]{:S(2)}, u32[]{:S(2)}) async-start(bf16[64,8,512]{2,1,0:T(8,128)(2,1)} %bitcast.1), calls=%async_computation | async-start | bytes 1048576 | tf_op jit(solution)/shard_map/all_to_all | solution.py:352
  17.0 0.7 copy-start.9
  57.8 15.6 %collective-permute-start.4 = (bf16[512,512]{1,0:T(8,128)(2,1)S(1)}, bf16[512,512]{1,0:T(8,128)(2,1)S(1)}, u32[]{:S(2)}, u32[]{:S(2)}) collective-permute-start(bf16[512,512]{1,0:T(8,128)(2,1)S(1)} %bitcast.30), channel_id=1, source_target_pairs={{0,3},{1,0},{2,1},{3,2},{4,7},{5,4},{6,5},{7,6},{8,11},{9,8},{10,9... | collective-permute-start | bytes 1572872 | tf_op jit(solution)/shard_map/ppermute | solution.py:384
  58.3 26.3 %collective-permute-start.3 = (bf16[512,512]{1,0:T(8,128)(2,1)S(1)}, bf16[512,512]{1,0:T(8,128)(2,1)S(1)}, u32[]{:S(2)}, u32[]{:S(2)}) collective-permute-start(bf16[512,512]{1,0:T(8,128)(2,1)S(1)} %bitcast.31), channel_id=1, source_target_pairs={{0,1},{1,2},{2,3},{3,0},{4,5},{5,6},{6,7},{7,4},{8,9},{9,10},{10,1... | collective-permute-start | bytes 1572872 | tf_op jit(solution)/shard_map/ppermute | solution.py:383
  59.8 25.4 %collective-permute-start.2 = (bf16[512,512]{1,0:T(8,128)(2,1)S(1)}, bf16[512,512]{1,0:T(8,128)(2,1)S(1)}, u32[]{:S(2)}, u32[]{:S(2)}) collective-permute-start(bf16[512,512]{1,0:T(8,128)(2,1)S(1)} %bitcast.24), channel_id=1, source_target_pairs={{0,2},{1,3},{2,0},{3,1},{4,6},{5,7},{6,4},{7,5},{8,10},{9,11},{10,... | collective-permute-start | bytes 1572872 | tf_op jit(solution)/shard_map/ppermute | solution.py:379
  63.2 31.9 %collective-permute-start.1 = (bf16[512,512]{1,0:T(8,128)(2,1)S(1)}, bf16[512,512]{1,0:T(8,128)(2,1)S(1)}, u32[]{:S(2)}, u32[]{:S(2)}) collective-permute-start(bf16[512,512]{1,0:T(8,128)(2,1)S(1)} %bitcast.25), channel_id=1, source_target_pairs={{0,3},{1,0},{2,1},{3,2},{4,7},{5,4},{6,5},{7,6},{8,11},{9,8},{10,9... | collective-permute-start | bytes 1572872 | tf_op jit(solution)/shard_map/ppermute | solution.py:381
  63.4 33.0 %collective-permute-start = (bf16[512,512]{1,0:T(8,128)(2,1)S(1)}, bf16[512,512]{1,0:T(8,128)(2,1)S(1)}, u32[]{:S(2)}, u32[]{:S(2)}) collective-permute-start(bf16[512,512]{1,0:T(8,128)(2,1)S(1)} %bitcast.26), channel_id=1, source_target_pairs={{0,1},{1,2},{2,3},{3,0},{4,5},{5,6},{6,7},{7,4},{8,9},{9,10},{10,1... | collective-permute-start | bytes 1572872 | tf_op jit(solution)/shard_map/ppermute | solution.py:380
  73.4 26.4 %collective-permute-start.6 = (bf16[256,512]{1,0:T(8,128)(2,1)S(1)}, bf16[256,512]{1,0:T(8,128)(2,1)S(1)}, u32[]{:S(2)}, u32[]{:S(2)}) collective-permute-start(bf16[256,512]{1,0:T(8,128)(2,1)S(1)} %slice.9), channel_id=1, source_target_pairs={{0,3},{1,0},{2,1},{3,2},{4,7},{5,4},{6,5},{7,6},{8,11},{9,8},{10,9... | collective-permute-start | bytes 786440 | tf_op jit(solution)/shard_map/ppermute | solution.py:386
  84.6 16.5 %collective-permute-start.5 = (bf16[256,512]{1,0:T(8,128)(2,1)S(1)}, bf16[256,512]{1,0:T(8,128)(2,1)S(1)}, u32[]{:S(2)}, u32[]{:S(2)}) collective-permute-start(bf16[256,512]{1,0:T(8,128)(2,1)S(1)} %slice.8), channel_id=1, source_target_pairs={{0,1},{1,2},{2,3},{3,0},{4,5},{5,6},{6,7},{7,4},{8,9},{9,10},{10,1... | collective-permute-start | bytes 786440 | tf_op jit(solution)/shard_map/ppermute | solution.py:385
  96.4 1.8 copy-start.2
  103.3 16.4 %collective-permute-start.7 = (bf16[512,512]{1,0:T(8,128)(2,1)S(1)}, bf16[512,512]{1,0:T(8,128)(2,1)S(1)}, u32[]{:S(2)}, u32[]{:S(2)}) collective-permute-start(bf16[512,512]{1,0:T(8,128)(2,1)S(1)} %get-tuple-element.68), channel_id=1, source_target_pairs={{0,2},{1,3},{2,0},{3,1},{4,6},{5,7},{6,4},{7,5},{8,10},{9,11},{10,... | collective-permute-start | bytes 1572872 | tf_op jit(solution)/shard_map/ppermute | solution.py:397
  105.4 23.2 %collective-permute-start.8 = (bf16[512,512]{1,0:T(8,128)(2,1)S(1)}, bf16[512,512]{1,0:T(8,128)(2,1)S(1)}, u32[]{:S(2)}, u32[]{:S(2)}) collective-permute-start(bf16[512,512]{1,0:T(8,128)(2,1)S(1)} %get-tuple-element.69), channel_id=1, source_target_pairs={{0,1},{1,2},{2,3},{3,0},{4,5},{5,6},{6,7},{7,4},{8,9},{9,10},{10,1... | collective-permute-start | bytes 1572872 | tf_op jit(solution)/shard_map/ppermute | solution.py:398
  107.7 21.4 %collective-permute-start.9 = (bf16[512,512]{1,0:T(8,128)(2,1)S(1)}, bf16[512,512]{1,0:T(8,128)(2,1)S(1)}, u32[]{:S(2)}, u32[]{:S(2)}) collective-permute-start(bf16[512,512]{1,0:T(8,128)(2,1)S(1)} %get-tuple-element.70), channel_id=1, source_target_pairs={{0,3},{1,0},{2,1},{3,2},{4,7},{5,4},{6,5},{7,6},{8,11},{9,8},{10,9... | collective-permute-start | bytes 1572872 | tf_op jit(solution)/shard_map/ppermute | solution.py:399
  112.7 40.3 %copy-start.4 = (bf16[128,2048]{1,0:T(8,128)(2,1)S(1)}, bf16[128,2048]{1,0:T(8,128)(2,1)}, u32[]{:S(2)}) copy-start(bf16[128,2048]{1,0:T(8,128)(2,1)} %oc_ref.3) | copy-start | bytes 1572868
  112.7 51.1 %copy-start.5 = (bf16[128,256]{1,0:T(8,128)(2,1)S(1)}, bf16[128,256]{1,0:T(8,128)(2,1)}, u32[]{:S(2)}) copy-start(bf16[128,256]{1,0:T(8,128)(2,1)} %mixed_ref.1) | copy-start | bytes 196612
  130.0 34.9 %copy-start.3 = (bf16[2048,256]{1,0:T(8,128)(2,1)S(1)}, bf16[2048,256]{1,0:T(8,128)(2,1)}, u32[]{:S(2)}) copy-start(bf16[2048,256]{1,0:T(8,128)(2,1)} %w_ref.1) | copy-start | bytes 3145732
  153.8 8.0 %collective-permute-start.12 = (bf16[128,512]{1,0:T(8,128)(2,1)S(1)}, bf16[128,512]{1,0:T(8,128)(2,1)S(1)}, u32[]{:S(2)}, u32[]{:S(2)}) collective-permute-start(bf16[128,512]{1,0:T(8,128)(2,1)S(1)} %shard_map.204.m0_ref), channel_id=1, source_target_pairs={{0,2},{1,3},{2,0},{3,1},{4,6},{5,7},{6,4},{7,5},{8,10},{9,11},{10,... | collective-permute-start | bytes 393224 | tf_op jit(solution)/shard_map/ppermute | solution.py:417
  156.0 7.8 %collective-permute-start.11 = (bf16[128,512]{1,0:T(8,128)(2,1)S(1)}, bf16[128,512]{1,0:T(8,128)(2,1)S(1)}, u32[]{:S(2)}, u32[]{:S(2)}) collective-permute-start(bf16[128,512]{1,0:T(8,128)(2,1)S(1)} %shard_map.204.m0_ref), channel_id=1, source_target_pairs={{0,3},{1,0},{2,1},{3,2},{4,7},{5,4},{6,5},{7,6},{8,11},{9,8},{10,9... | collective-permute-start | bytes 393224 | tf_op jit(solution)/shard_map/ppermute | solution.py:419
  156.8 6.9 %collective-permute-start.10 = (bf16[128,512]{1,0:T(8,128)(2,1)S(1)}, bf16[128,512]{1,0:T(8,128)(2,1)S(1)}, u32[]{:S(2)}, u32[]{:S(2)}) collective-permute-start(bf16[128,512]{1,0:T(8,128)(2,1)S(1)} %shard_map.204.m0_ref), channel_id=1, source_target_pairs={{0,1},{1,2},{2,3},{3,0},{4,5},{5,6},{6,7},{7,4},{8,9},{9,10},{10,1... | collective-permute-start | bytes 393224 | tf_op jit(solution)/shard_map/ppermute | solution.py:418
  164.8 7.7 %collective-permute-start.13 = (bf16[1024,256]{1,0:T(8,128)(2,1)S(1)}, bf16[1024,256]{1,0:T(8,128)(2,1)S(1)}, u32[]{:S(2)}, u32[]{:S(2)}) collective-permute-start(bf16[1024,256]{1,0:T(8,128)(2,1)S(1)} %get-tuple-element.78), channel_id=1, source_target_pairs={{0,4},{4,0},{8,12},{12,8},{16,20},{20,16},{24,28},{28,24},{32,36},... | collective-permute-start | bytes 1572872 | tf_op jit(solution)/shard_map/ppermute | solution.py:429
  164.9 31.0 %copy-start.7 = (bf16[128,256]{1,0:T(8,128)(2,1)S(1)}, bf16[128,256]{1,0:T(8,128)(2,1)}, u32[]{:S(2)}) copy-start(bf16[128,256]{1,0:T(8,128)(2,1)} %v_ref.5) | copy-start | bytes 196612
  164.9 31.0 %copy-start.8 = (bf16[128,128]{1,0:T(8,128)(2,1)S(1)}, bf16[128,128]{1,0:T(8,128)(2,1)}, u32[]{:S(2)}) copy-start(bf16[128,128]{1,0:T(8,128)(2,1)} %k_ref.5) | copy-start | bytes 98308
  167.0 18.4 %all-to-all-start.3 = ((bf16[64,8,256]{2,1,0:T(8,128)(2,1)}), bf16[64,8,256]{2,1,0:T(8,128)(2,1)S(1)}, u32[]{:S(2)}, u32[]{:S(2)}) async-start(bf16[64,8,256]{2,1,0:T(8,128)(2,1)} %bitcast.14), calls=%async_computation.3 | async-start | bytes 524288 | tf_op jit(solution)/shard_map/all_to_all | solution.py:352
  173.3 12.1 %collective-permute-start.14 = (bf16[512,128]{1,0:T(8,128)(2,1)S(1)}, bf16[512,128]{1,0:T(8,128)(2,1)S(1)}, u32[]{:S(2)}, u32[]{:S(2)}) collective-permute-start(bf16[512,128]{1,0:T(8,128)(2,1)S(1)} %get-tuple-element.80), channel_id=1, source_target_pairs={{0,16},{4,20},{8,24},{12,28},{16,0},{20,4},{24,8},{28,12},{32,48},... | collective-permute-start | bytes 393224 | tf_op jit(solution)/shard_map/ppermute | solution.py:431
  176.4 9.2 %collective-permute-start.15 = (bf16[512,128]{1,0:T(8,128)(2,1)S(1)}, bf16[512,128]{1,0:T(8,128)(2,1)S(1)}, u32[]{:S(2)}, u32[]{:S(2)}) collective-permute-start(bf16[512,128]{1,0:T(8,128)(2,1)S(1)} %get-tuple-element.81), channel_id=1, source_target_pairs={{0,8},{4,12},{8,16},{12,20},{16,24},{20,28},{24,0},{28,4},{32,40},... | collective-permute-start | bytes 393224 | tf_op jit(solution)/shard_map/ppermute | solution.py:431
  177.0 8.6 %collective-permute-start.16 = (bf16[512,128]{1,0:T(8,128)(2,1)S(1)}, bf16[512,128]{1,0:T(8,128)(2,1)S(1)}, u32[]{:S(2)}, u32[]{:S(2)}) collective-permute-start(bf16[512,128]{1,0:T(8,128)(2,1)S(1)} %get-tuple-element.82), channel_id=1, source_target_pairs={{0,24},{4,28},{8,0},{12,4},{16,8},{20,12},{24,16},{28,20},{32,56},... | collective-permute-start | bytes 393224 | tf_op jit(solution)/shard_map/ppermute | solution.py:431
  187.3 21.5 %all-to-all-start.4 = ((bf16[64,8,256]{2,1,0:T(8,128)(2,1)}), bf16[64,8,256]{2,1,0:T(8,128)(2,1)S(1)}, u32[]{:S(2)}, u32[]{:S(2)}) async-start(bf16[64,8,256]{2,1,0:T(8,128)(2,1)} %bitcast.16), calls=%async_computation.4 | async-start | bytes 524288 | tf_op jit(solution)/shard_map/all_to_all | solution.py:352

commit v3 on v2

--- a/solution.py
+++ b/solution.py
@@ -154,9 +154,9 @@
     tile_ref[...] = tiles_of(state, fill).astype(BF)
 
 
-def gate_kernel(q_ref, x0_ref, x1_ref, x2_ref, x3_ref, wg_ref, wu_ref, g_ref, u_ref):
+def gate_near_kernel(q_ref, x0_ref, x1_ref, x2_ref, wg_ref, wu_ref, g_ref, u_ref):
     g = u = None
-    for n, ref in enumerate((x0_ref, x1_ref, x2_ref, x3_ref)):
+    for n, ref in enumerate((x0_ref, x1_ref, x2_ref)):
         rows = quarter_rows(q_ref[n])
         x = ref[...]
         g1, u1 = dot(x, wg_ref[rows, :], 1, 0), dot(x, wu_ref[rows, :], 1, 0)
@@ -165,52 +165,84 @@
     u_ref[...] = u
 
 
-def near_kernel(q_ref, y0_ref, y1_ref, y2_ref, wd_ref, h_ref):
-    h = None
-    for n, ref in enumerate((y0_ref, y1_ref, y2_ref)):
-        h1 = dot(ref[...], wd_ref[:, quarter_rows(q_ref[n])], 1, 1)
-        h = h1 if h is None else h + h1
-    h_ref[...] = h
+def gate_far_kernel(
+    q_ref, g_ref, u_ref, t3_ref, b3_ref, wg_ref, wu_ref, hid_ref, to_gate_ref, to_up_ref
+):
+    rows = quarter_rows(q_ref[3])
+    x = jnp.concatenate([t3_ref[...], b3_ref[...]], axis=0)
+    g = g_ref[...] + dot(x, wg_ref[rows, :], 1, 0)
+    u = u_ref[...] + dot(x, wu_ref[rows, :], 1, 0)
+    sig = jax.nn.sigmoid(g)
+    silu = g * sig
+    hid_ref[...] = (silu * u).astype(BF)
+    to_gate_ref[...] = u * sig * (1.0 + g * (1.0 - sig))
+    to_up_ref[...] = silu
+
+
+TOP, BOTTOM = slice(0, SLOTS // 2), slice(SLOTS // 2, SLOTS)
+
+
+def near_kernel(q_ref, y0_ref, t1_ref, b1_ref, t2_ref, b2_ref, wd_ref, h_ref):
+    w0, w1, w2 = (wd_ref[:, quarter_rows(q_ref[n])] for n in range(3))
+    h = dot(y0_ref[...], w0, 1, 1)
+    h_ref[TOP, :] = h[TOP] + dot(t1_ref[...], w1, 1, 1) + dot(t2_ref[...], w2, 1, 1)
+    h_ref[BOTTOM, :] = h[BOTTOM] + dot(b1_ref[...], w1, 1, 1) + dot(b2_ref[...], w2, 1, 1)
+
+
+def back_rows(gu_ref, wg_ref, wu_ref, rows):
+    part = dot(gu_ref[:, :FF], wg_ref[rows, :], 1, 1) + dot(gu_ref[:, FF:], wu_ref[rows, :], 1, 1)
+    return part.astype(BF)
 
 
 def far_kernel(
-    q_ref, g_ref, u_ref, h_ref, top_ref, bot_ref, wg_ref, wu_ref, wd_ref,
-    far_ref, right_ref, left_ref, own_ref, hid_ref, gu_ref,
-):
-    dy = jnp.concatenate([top_ref[...], bot_ref[...]], axis=0)
-    g, u = g_ref[...], u_ref[...]
-    h = h_ref[...] + dot(dy, wd_ref[:, quarter_rows(q_ref[3])], 1, 1)
-    sig = jax.nn.sigmoid(g)
-    hid_ref[...] = (g * sig * u).astype(BF)
-    gate_cot = (h * u * sig * (1.0 + g * (1.0 - sig))).astype(BF)
-    up_cot = (h * g * sig).astype(BF)
-    gu_ref[:, :FF] = gate_cot
-    gu_ref[:, FF:] = up_cot
-    for n, ref in ((3, far_ref), (2, right_ref), (1, left_ref), (0, own_ref)):
-        rows = quarter_rows(q_ref[n])
-        part = dot(gate_cot, wg_ref[rows, :], 1, 1) + dot(up_cot, wu_ref[rows, :], 1, 1)
-        ref[...] = part.astype(BF)
+    q_ref, h_ref, t3_ref, b3_ref, to_gate_ref, to_up_ref, wg_ref, wu_ref, wd_ref,
+    gu_ref, top_ref, bottom_ref,
+):
+    w3 = wd_ref[:, quarter_rows(q_ref[3])]
+    for rows, ref in ((TOP, t3_ref), (BOTTOM, b3_ref)):
+        h = h_ref[rows, :] + dot(ref[...], w3, 1, 1)
+        gu_ref[rows, :FF] = (h * to_gate_ref[rows, :]).astype(BF)
+        gu_ref[rows, FF:] = (h * to_up_ref[rows, :]).astype(BF)
+    far = back_rows(gu_ref, wg_ref, wu_ref, quarter_rows(q_ref[3]))
+    top_ref[...] = far[TOP]
+    bottom_ref[...] = far[BOTTOM]
+
+
+def sides_kernel(q_ref, gu_ref, wg_ref, wu_ref, rt_ref, rb_ref, lt_ref, lb_ref):
+    for n, top_ref, bottom_ref in ((2, rt_ref, rb_ref), (1, lt_ref, lb_ref)):
+        part = back_rows(gu_ref, wg_ref, wu_ref, quarter_rows(q_ref[n]))
+        top_ref[...] = part[TOP]
+        bottom_ref[...] = part[BOTTOM]
+
+
+def merge_kernel(q_ref, rt_ref, lb_ref, from_left_ref, from_right_ref, t_ref, b_ref):
+    t_ref[...] = (rt_ref[...].astype(F32) + from_left_ref[...].astype(F32)).astype(BF)
+    b_ref[...] = (lb_ref[...].astype(F32) + from_right_ref[...].astype(F32)).astype(BF)
 
 
 def weight_kernel(
-    q_ref, x0_ref, x1_ref, x2_ref, x3_ref, y0_ref, y1_ref, y2_ref, top_ref, bot_ref,
-    hid_ref, gu_ref, gg_ref, gup_ref, gd_ref,
-):
+    q_ref, x0_ref, x1_ref, x2_ref, xt_ref, xb_ref,
+    y0_ref, t1_ref, b1_ref, t2_ref, b2_ref, t3_ref, b3_ref,
+    hid_ref, gu_ref, wg_ref, wu_ref, gg_ref, gup_ref, gd_ref, own_ref,
+):
+    own_ref[...] = back_rows(gu_ref, wg_ref, wu_ref, quarter_rows(q_ref[0]))
     hid_t = hid_ref[...].T
     gu = gu_ref[...]
-    far = jnp.concatenate([top_ref[...], bot_ref[...]], axis=0)
-    cots = (y0_ref[...], y1_ref[...], y2_ref[...], far)
-    for n, ref in enumerate((x0_ref, x1_ref, x2_ref, x3_ref)):
+    pairs = ((t1_ref, b1_ref), (t2_ref, b2_ref), (t3_ref, b3_ref))
+    cots = [y0_ref[...]] + [jnp.concatenate([t[...], b[...]], axis=0) for t, b in pairs]
+    far = jnp.concatenate([xt_ref[...], xb_ref[...]], axis=0)
+    for n, x in enumerate((x0_ref[...], x1_ref[...], x2_ref[...], far)):
         rows = quarter_rows(q_ref[n])
-        both = dot(ref[...].T, gu, 1, 0)
+        both = dot(x.T, gu, 1, 0)
         gg_ref[rows, :] = both[:, :FF]
         gup_ref[rows, :] = both[:, FF:]
         gd_ref[:, rows] = dot(hid_t, cots[n], 1, 0)
 
 
-def sum_kernel(q_ref, p0_ref, p1_ref, p2_ref, p3_ref, out_ref):
-    total = p0_ref[...].astype(F32) + p1_ref[...].astype(F32)
-    out_ref[...] = (total + p2_ref[...].astype(F32) + p3_ref[...].astype(F32)).astype(BF)
+def sum_kernel(q_ref, own_ref, tl_ref, tr_ref, bl_ref, br_ref, out_ref):
+    for rows, a_ref, b_ref in ((TOP, tl_ref, tr_ref), (BOTTOM, bl_ref, br_ref)):
+        got = a_ref[...].astype(F32) + b_ref[...].astype(F32)
+        out_ref[rows, :] = (own_ref[rows, :].astype(F32) + got).astype(BF)
 
 
 def combine_kernel(q_ref, rows_ref, pick_ref, oc_ref, out_ref):
@@ -360,7 +392,7 @@
     x_rows, pick, slots = run(
         pick_kernel,
         (rows_type, sds((SLOTS, TOK), BF), sds((2, TOK), jnp.int32)),
-        (route_ids.T, in_hbm(expert_in)),
+        (in_hbm(route_ids.T), in_hbm(expert_in)),
         in_specs=[None, quarter_block()],
         flops=1e8,
     )
@@ -368,7 +400,7 @@
         local_kernel,
         (rows_type, tile_type, sds((TOK, DK), F32), sds((TOK, DK), F32)),
         (
-            slots, route_weights.T, pick, in_hbm(out_cot), in_hbm(queries), in_hbm(keys),
+            slots, in_hbm(route_weights.T), pick, in_hbm(out_cot), in_hbm(queries), in_hbm(keys),
             in_hbm(values), in_hbm(log_decay),
         ),
         in_specs=[None, None, None, quarter_block(), None, None, None, None],
@@ -376,36 +408,52 @@
     )
     x0 = exchange(x_rows)
     x0, y_rows = lax.optimization_barrier((x0, y_rows))
-    x3 = lax.ppermute(x0, "tp", across)
     x1 = lax.ppermute(x0, "tp", to_right)
     x2 = lax.ppermute(x0, "tp", to_left)
+    xt3 = lax.ppermute(x1[TOP], "tp", to_right)
+    xb3 = lax.ppermute(x2[BOTTOM], "tp", to_left)
     y0 = exchange(y_rows)
-    y1 = lax.ppermute(y0, "tp", to_right)
-    y2 = lax.ppermute(y0, "tp", to_left)
-    far_top = lax.ppermute(y1[: SLOTS // 2], "tp", to_right)
-    far_bottom = lax.ppermute(y2[SLOTS // 2 :], "tp", to_left)
-    g, u = run(
-        gate_kernel, (sds((SLOTS, FF), F32),) * 2, (x0, x1, x2, x3, wg, wu), flops=1.1e9
-    )
-    h = run(near_kernel, sds((SLOTS, FF), F32), (y0, y1, y2, wd), flops=4e8)
-    p_far, p_right, p_left, p_own, hidden, gate_up = run(
+    y_top, y_bottom = y0[TOP], y0[BOTTOM]
+    t1 = lax.ppermute(y_top, "tp", to_right)
+    b2 = lax.ppermute(y_bottom, "tp", to_left)
+    b1 = lax.ppermute(y_bottom, "tp", to_right)
+    t2 = lax.ppermute(y_top, "tp", to_left)
+    t3 = lax.ppermute(t1, "tp", to_right)
+    b3 = lax.ppermute(b2, "tp", to_left)
+    half_type = sds((SLOTS, FF), F32)
+    part_type = sds((SLOTS // 2, QUART), BF)
+    g, u = run(gate_near_kernel, (half_type,) * 2, (x0, x1, x2, wg, wu), flops=8e8)
+    hidden, to_gate, to_up = run(
+        gate_far_kernel,
+        (sds((SLOTS, FF), BF), half_type, half_type),
+        (g, u, xt3, xb3, wg, wu),
+        flops=3e8,
+    )
+    h = run(near_kernel, half_type, (y0, t1, b1, t2, b2, wd), flops=4e8)
+    gate_up, p_top, p_bottom = run(
         far_kernel,
-        (rows_type,) * 4 + (sds((SLOTS, FF), BF), sds((SLOTS, 2 * FF), BF)),
-        (g, u, h, far_top, far_bottom, wg, wu, wd),
-        flops=1.3e9,
-    )
-    r_far = lax.ppermute(p_far, "tp", across)
-    r_left = lax.ppermute(p_right, "tp", to_right)
-    r_right = lax.ppermute(p_left, "tp", to_left)
-    grads = run(
+        (sds((SLOTS, 2 * FF), BF), part_type, part_type),
+        (h, t3, b3, to_gate, to_up, wg, wu, wd),
+        flops=4e8,
+    )
+    far_top = lax.ppermute(p_top, "tp", to_right)
+    far_bottom = lax.ppermute(p_bottom, "tp", to_left)
+    p_rt, p_rb, p_lt, p_lb = run(sides_kernel, (part_type,) * 4, (gate_up, wg, wu), flops=5e8)
+    bl = lax.ppermute(p_rb, "tp", to_right)
+    tr = lax.ppermute(p_lt, "tp", to_left)
+    p_t, p_b = run(merge_kernel, (part_type,) * 2, (p_rt, p_lb, far_top, far_bottom), flops=1e6)
+    tl = lax.ppermute(p_t, "tp", to_right)
+    br = lax.ppermute(p_b, "tp", to_left)
+    *grads, p_own = run(
         weight_kernel,
-        (sds((WIDTH, FF), F32), sds((WIDTH, FF), F32), sds((FF, WIDTH), F32)),
-        (x0, x1, x2, x3, y0, y1, y2, far_top, far_bottom, hidden, gate_up),
-        flops=1.6e9,
-    )
-    p_own, grads = lax.optimization_barrier((p_own, grads))
+        (sds((WIDTH, FF), F32), sds((WIDTH, FF), F32), sds((FF, WIDTH), F32), rows_type),
+        (
+            x0, x1, x2, xt3, xb3, y0, t1, b1, t2, b2, t3, b3, hidden, gate_up, wg, wu,
+        ),
+        flops=1.9e9,
+    )
     grad_gate, grad_up, grad_down = grads
-    total = run(sum_kernel, rows_type, (p_own, r_far, r_left, r_right), flops=1e6)
+    total = run(sum_kernel, rows_type, (p_own, tl, tr, bl, br), flops=1e6)
     back = exchange(total)
     mid = run(
         combine_kernel,

time: 214 us -> 192 us (0.90)
  blocking collectives: 46.2 us -> 25.5 us
  waiting for transfers between devices: 75.4 us -> 63.5 us
  local copies, waits for them, and re-layouts: 2.18 us -> 6.45 us
  Pallas kernels: 25.6 us -> 29.8 us
  starting transfers between devices: 60.6 us -> 63.1 us
    all_to_all x2 -> x1, blocking collectives: 46.2 us -> 25.5 us  [exchange(): lax.all_to_all(rows.reshape(EXPERTS, CAP, width), 'sp', 0, 0, tiled=True)]
    ppermute x8 -> x14, waiting for transfers between devices: 26.5 us -> 14.5 us  [the longest x1 3.32 us: per_device(): b3 = lax.ppermute(b2, 'tp', to_left)]
    ppermute x1, waiting for transfers between devices: 1.31 us -> 11.9 us  [per_device(): x1 = lax.ppermute(x0, 'tp', to_right)]
    ppermute x1, waiting for transfers between devices: 9.86 us -> 0.01 us  [per_device(): x2 = lax.ppermute(x0, 'tp', to_left)]
    all_to_all x3 -> x4, starting transfers between devices: 26.3 us -> 31.9 us  [exchange(): lax.all_to_all(rows.reshape(EXPERTS, CAP, width), 'sp', 0, 0, tiled=True)]
    pallas_call x14 -> x17, Pallas kernels: 25.6 us -> 29.8 us  [call(): pl.pallas_call(kernel, out_shape=out_shape, grid_spec=pltpu.PrefetchScala...]
    ppermute x8 -> x14, starting transfers between devices: 21.6 us -> 17.9 us  [the longest x1 2.95 us: per_device(): t2 = lax.ppermute(y_top, 'tp', to_left)]
    unnamed x20 -> x36, local copies, waits for them, and re-layouts: 1.39 us -> 3.94 us
  transfers between devices with their start and end apart: 20 -> 27, of which waited for: 14 -> 15; matrix products, arithmetic and copies ran while one was open for 0% -> 1% of each run, Pallas kernels for 7% -> 10%
where the time goes in v3:
time: 192 us; the launch traced here: 189 us
  waiting for transfers between devices  63.5 us (33%)
  starting transfers between devices  63.1 us (33%)
  Pallas kernels  29.8 us (16%)
  blocking collectives  25.5 us (13%)
  local copies, waits for them, and re-layouts  6.45 us (3%)
    all_to_all x4, starting transfers between devices, exchange(): lax.all_to_all(rows.reshape(EXPERTS, CAP, width), 'sp', 0, 0, tiled=True)  31.9 us
    all_to_all x4, waiting for transfers between devices, exchange(): lax.all_to_all(rows.reshape(EXPERTS, CAP, width), 'sp', 0, 0, tiled=True)  30.8 us
    pallas_call x17, Pallas kernels, call(): pl.pallas_call(kernel, out_shape=out_shape, grid_spec=pltpu.PrefetchScala...  29.8 us
    all_to_all x1, blocking collectives, exchange(): lax.all_to_all(rows.reshape(EXPERTS, CAP, width), 'sp', 0, 0, tiled=True)  25.5 us
    ppermute x1, waiting for transfers between devices, per_device(): x1 = lax.ppermute(x0, 'tp', to_right)  11.9 us
    ppermute x3, starting transfers between devices, per_device(): adds = [lax.ppermute(tiles[k], 'sp', along_y(k)) for k in (2, 1, 3)]  6.4 us
    unnamed x36, local copies, waits for them, and re-layouts  3.94 us
  transfers between devices with their start and end apart: 27, of which 15 were waited for; matrix products, arithmetic and copies ran while one was open for 1% of the time, Pallas kernels for 10%

profile of v3, /device:TPU:2, one launch (start us, length us, event | category | flops | bytes accessed | tf_op | source)
XLA Modules:
  0.0 189.4 jit_solution(15816780483067491599)
XLA Ops:
  1.4 2.7 %shard_map.197 = (bf16[512,512]{1,0:T(8,128)(2,1)}, bf16[512,128]{1,0:T(8,128)(2,1)S(1)}, s32[2,128]{1,0:T(2,128)S(1)}) custom-call(s32[6]{0:T(128)S(1)} %dynamic_slice.3.q_ref, s32[2,128]{1,0:T(2,128)} %bitcast.45, bf16[128,2048]{1,0:T(8,128)(2,1)} %x_ref.1), custom_call_target="tpu_custom_call" | custom-call | flops 100000000 | bytes 1181696 | tf_op jit(solution)/shard_map/pallas_call | solution.py:55
  4.1 12.1 %all-to-all-start = ((bf16[64,8,512]{2,1,0:T(8,128)(2,1)}), bf16[64,8,512]{2,1,0:T(8,128)(2,1)S(1)}, u32[]{:S(2)}, u32[]{:S(2)}) async-start(bf16[64,8,512]{2,1,0:T(8,128)(2,1)} %bitcast.1), calls=%async_computation | async-start | bytes 1048576 | tf_op jit(solution)/shard_map/all_to_all | solution.py:384
  16.2 2.5 %shard_map.198 = (bf16[512,512]{1,0:T(8,128)(2,1)S(1)}, bf16[512,128]{1,0:T(8,128)(2,1)S(1)}, f32[128,128]{1,0:T(8,128)S(1)}, f32[128,128]{1,0:T(8,128)S(1)}) custom-call(s32[6]{0:T(128)S(1)} %dynamic_slice.3.q_ref, s32[2,128]{1,0:T(2,128)S(1)} %get-tuple-element.52.slot_ref, f32[2,128]{1,0:T(2,128)} %bitcast.49, ...), custom_call_target="tpu_custom_call" | custom-call | flops 300000000 | bytes 1640448 | tf_op jit(solution)/shard_map/pallas_call | solution.py:55
  21.4 12.4 %all-to-all-done = bf16[64,8,512]{2,1,0:T(8,128)(2,1)S(1)} async-done(((bf16[64,8,512]{2,1,0:T(8,128)(2,1)}), bf16[64,8,512]{2,1,0:T(8,128)(2,1)S(1)}, u32[]{:S(2)}, u32[]{:S(2)}) %all-to-all-start) | async-done | bytes 524320 | tf_op jit(solution)/shard_map/all_to_all | solution.py:384
  33.8 5.8 %all-to-all-start.1 = ((bf16[64,8,512]{2,1,0:T(8,128)(2,1)}), bf16[64,8,512]{2,1,0:T(8,128)(2,1)S(1)}, u32[]{:S(2)}, u32[]{:S(2)}) async-start(bf16[64,8,512]{2,1,0:T(8,128)(2,1)} %bitcast.43), calls=%async_computation.1 | async-start | bytes 1048576 | tf_op jit(solution)/shard_map/all_to_all | solution.py:384
  39.6 1.6 collective-permute-start
  41.7 11.9 %collective-permute-done.x1_ref = bf16[512,512]{1,0:T(8,128)(2,1)S(1)} collective-permute-done((bf16[512,512]{1,0:T(8,128)(2,1)S(1)}, bf16[512,512]{1,0:T(8,128)(2,1)S(1)}, u32[]{:S(2)}, u32[]{:S(2)}) %collective-permute-start) | collective-permute-done | bytes 524320 | tf_op jit(solution)/shard_map/ppermute | solution.py:411
  57.3 1.6 collective-permute-start.4
  60.3 1.8 collective-permute-start.3
  63.8 3.0 %collective-permute-start.6 = (bf16[256,512]{1,0:T(8,128)(2,1)S(1)}, bf16[256,512]{1,0:T(8,128)(2,1)S(1)}, u32[]{:S(2)}, u32[]{:S(2)}) collective-permute-start(bf16[256,512]{1,0:T(8,128)(2,1)S(1)} %get-tuple-element.95), channel_id=1, source_target_pairs={{0,3},{1,0},{2,1},{3,2},{4,7},{5,4},{6,5},{7,6},{8,11},{9,8},{10,9... | collective-permute-start | bytes 786440 | tf_op jit(solution)/shard_map/ppermute | solution.py:420
  66.8 2.7 %collective-permute-done.4.t1_ref = bf16[256,512]{1,0:T(8,128)(2,1)S(1)} collective-permute-done((bf16[256,512]{1,0:T(8,128)(2,1)S(1)}, bf16[256,512]{1,0:T(8,128)(2,1)S(1)}, u32[]{:S(2)}, u32[]{:S(2)}) %collective-permute-start.4) | collective-permute-done | bytes 262176 | tf_op jit(solution)/shard_map/ppermute | solution.py:417
  73.4 2.6 %shard_map.199 = (f32[512,256]{1,0:T(8,128)S(1)}, f32[512,256]{1,0:T(8,128)S(1)}) custom-call(s32[6]{0:T(128)S(1)} %dynamic_slice.3.q_ref, bf16[512,512]{1,0:T(8,128)(2,1)S(1)} %bitcast.36, bf16[512,512]{1,0:T(8,128)(2,1)S(1)} %copy-done.4, bf16[512,512]{1,0:T(8,128)(2,1)} %collective-permute-done.1.x2_ref, bf16[2048,256]{1,0:T(8,128)(2,1)S(1)} %bitcast.22, ...), custom_call_target="tpu_custom_call" | custom-call | flops 800000000 | bytes 4718592 | tf_op jit(solution)/shard_map/pallas_call | solution.py:55
  77.1 2.1 %collective-permute-done.6.t2_ref = bf16[256,512]{1,0:T(8,128)(2,1)S(1)} collective-permute-done((bf16[256,512]{1,0:T(8,128)(2,1)S(1)}, bf16[256,512]{1,0:T(8,128)(2,1)S(1)}, u32[]{:S(2)}, u32[]{:S(2)}) %collective-permute-start.6) | collective-permute-done | bytes 262176 | tf_op jit(solution)/shard_map/ppermute | solution.py:420
  80.4 3.3 %collective-permute-done.9.b3_ref = bf16[256,512]{1,0:T(8,128)(2,1)S(1)} collective-permute-done((bf16[256,512]{1,0:T(8,128)(2,1)S(1)}, bf16[256,512]{1,0:T(8,128)(2,1)S(1)}, u32[]{:S(2)}, u32[]{:S(2)}) %collective-permute-start.9) | collective-permute-done | bytes 262176 | tf_op jit(solution)/shard_map/ppermute | solution.py:422
  88.4 1.8 collective-permute-start.13
  90.5 3.0 %collective-permute-done.10.from_left_ref = bf16[256,512]{1,0:T(8,128)(2,1)S(1)} collective-permute-done((bf16[256,512]{1,0:T(8,128)(2,1)S(1)}, bf16[256,512]{1,0:T(8,128)(2,1)S(1)}, u32[]{:S(2)}, u32[]{:S(2)}) %collective-permute-start.10) | collective-permute-done | bytes 262176 | tf_op jit(solution)/shard_map/ppermute | solution.py:439
  93.5 2.0 %collective-permute-done.11.from_right_ref = bf16[256,512]{1,0:T(8,128)(2,1)S(1)} collective-permute-done((bf16[256,512]{1,0:T(8,128)(2,1)S(1)}, bf16[256,512]{1,0:T(8,128)(2,1)S(1)}, u32[]{:S(2)}, u32[]{:S(2)}) %collective-permute-start.11) | collective-permute-done | bytes 262176 | tf_op jit(solution)/shard_map/ppermute | solution.py:440
  96.1 1.7 collective-permute-start.12
  98.2 6.2 %shard_map.203 = (f32[2048,256]{1,0:T(8,128)}, f32[2048,256]{1,0:T(8,128)}, f32[256,2048]{1,0:T(8,128)}, bf16[512,512]{1,0:T(8,128)(2,1)S(1)}) custom-call(s32[6]{0:T(128)S(1)} %dynamic_slice.3.q_ref, bf16[512,512]{1,0:T(8,128)(2,1)S(1)} %bitcast.37, bf16[512,512]{1,0:T(8,128)(2,1)S(1)} %copy-done.5, bf16[512,512]{1,0:T(8,128)(2,1)} %collective-permute-done.1.x2_ref, ...), custom_call_target="tpu_custom_call" | custom-call | flops 1900000000 | bytes 13893632 | tf_op jit(solution)/shard_map/pallas_call | solution.py:55
  105.3 25.5 %all_to_all.25 = bf16[64,8,512]{2,1,0:T(8,128)(2,1)S(1)} all-to-all(bf16[64,8,512]{2,1,0:T(8,128)(2,1)S(1)} %bitcast.40), channel_id=1, replica_groups=mesh['sp'=64,'tp'=4] {'sp'}, dimensions={0} | all-to-all | bytes 1048576 | tf_op jit(solution)/shard_map/all_to_all | solution.py:384
  131.6 1.7 collective-permute-start.16
  133.7 2.5 %collective-permute-start.18 = (bf16[128,512]{1,0:T(8,128)(2,1)S(1)}, bf16[128,512]{1,0:T(8,128)(2,1)S(1)}, u32[]{:S(2)}, u32[]{:S(2)}) collective-permute-start(bf16[128,512]{1,0:T(8,128)(2,1)S(1)} %shard_map.207.m0_ref), channel_id=1, source_target_pairs={{0,2},{1,3},{2,0},{3,1},{4,6},{5,7},{6,4},{7,5},{8,10},{9,11},{10,... | collective-permute-start | bytes 393224 | tf_op jit(solution)/shard_map/ppermute | solution.py:465
  138.8 3.5 %collective-permute-done.18.m3_ref = bf16[128,512]{1,0:T(8,128)(2,1)S(1)} collective-permute-done((bf16[128,512]{1,0:T(8,128)(2,1)S(1)}, bf16[128,512]{1,0:T(8,128)(2,1)S(1)}, u32[]{:S(2)}, u32[]{:S(2)}) %collective-permute-start.18) | collective-permute-done | bytes 131104 | tf_op jit(solution)/shard_map/ppermute | solution.py:465
  143.5 2.1 %shard_map.208 = (f32[128,256]{1,0:T(8,128)S(1)}, bf16[512,256]{1,0:T(8,128)(2,1)}) custom-call(s32[6]{0:T(128)S(1)} %dynamic_slice.3.q_ref, bf16[128,512]{1,0:T(8,128)(2,1)S(1)} %shard_map.207.m0_ref, bf16[128,512]{1,0:T(8,128)(2,1)S(1)} %collective-permute-done.16.m1_ref, bf16[128,512]{1,0:T(8,128)(2,1)S(1)} %collective-permute-done.17.m2_ref, ...), custom_call_target="tpu_custom_call" | custom-call | flops 200000000 | bytes 2162688 | tf_op jit(solution)/shard_map/pallas_call | solution.py:55
  145.6 5.5 %all-to-all-start.3 = ((bf16[64,8,256]{2,1,0:T(8,128)(2,1)}), bf16[64,8,256]{2,1,0:T(8,128)(2,1)S(1)}, u32[]{:S(2)}, u32[]{:S(2)}) async-start(bf16[64,8,256]{2,1,0:T(8,128)(2,1)} %bitcast.16), calls=%async_computation.3 | async-start | bytes 524288 | tf_op jit(solution)/shard_map/all_to_all | solution.py:384
  151.9 3.2 %collective-permute-start.20 = (bf16[512,128]{1,0:T(8,128)(2,1)S(1)}, bf16[512,128]{1,0:T(8,128)(2,1)S(1)}, u32[]{:S(2)}, u32[]{:S(2)}) collective-permute-start(bf16[512,128]{1,0:T(8,128)(2,1)S(1)} %get-tuple-element.86), channel_id=1, source_target_pairs={{0,16},{4,20},{8,24},{12,28},{16,0},{20,4},{24,8},{28,12},{32,48},... | collective-permute-start | bytes 393224 | tf_op jit(solution)/shard_map/ppermute | solution.py:479
  155.6 2.7 %collective-permute-start.22 = (bf16[512,128]{1,0:T(8,128)(2,1)S(1)}, bf16[512,128]{1,0:T(8,128)(2,1)S(1)}, u32[]{:S(2)}, u32[]{:S(2)}) collective-permute-start(bf16[512,128]{1,0:T(8,128)(2,1)S(1)} %get-tuple-element.88), channel_id=1, source_target_pairs={{0,24},{4,28},{8,0},{12,4},{16,8},{20,12},{24,16},{28,20},{32,56},... | collective-permute-start | bytes 393224 | tf_op jit(solution)/shard_map/ppermute | solution.py:479
  158.3 5.7 %all-to-all-done.3 = bf16[64,8,256]{2,1,0:T(8,128)(2,1)S(1)} async-done(((bf16[64,8,256]{2,1,0:T(8,128)(2,1)}), bf16[64,8,256]{2,1,0:T(8,128)(2,1)S(1)}, u32[]{:S(2)}, u32[]{:S(2)}) %all-to-all-start.3) | async-done | bytes 262176 | tf_op jit(solution)/shard_map/all_to_all | solution.py:384
  164.2 1.7 shard_map.212
  166.0 8.6 %all-to-all-start.4 = ((bf16[64,8,256]{2,1,0:T(8,128)(2,1)}), bf16[64,8,256]{2,1,0:T(8,128)(2,1)S(1)}, u32[]{:S(2)}, u32[]{:S(2)}) async-start(bf16[64,8,256]{2,1,0:T(8,128)(2,1)} %bitcast.18), calls=%async_computation.4 | async-start | bytes 524288 | tf_op jit(solution)/shard_map/all_to_all | solution.py:384
  176.0 11.5 %all-to-all-done.4 = bf16[64,8,256]{2,1,0:T(8,128)(2,1)S(1)} async-done(((bf16[64,8,256]{2,1,0:T(8,128)(2,1)}), bf16[64,8,256]{2,1,0:T(8,128)(2,1)S(1)}, u32[]{:S(2)}, u32[]{:S(2)}) %all-to-all-start.4) | async-done | bytes 262176 | tf_op jit(solution)/shard_map/all_to_all | solution.py:384
  187.5 1.9 %shard_map.213 = (bf16[128,128]{1,0:T(8,128)(2,1)}, bf16[128,128]{1,0:T(8,128)(2,1)}, bf16[128,256]{1,0:T(8,128)(2,1)}, f32[128,128]{1,0:T(8,128)}, f32[32,256]{1,0:T(8,128)}) custom-call(s32[6]{0:T(128)S(1)} %dynamic_slice.3.q_ref, bf16[128,128]{1,0:T(8,128)(2,1)S(1)} %copy-done.15, bf16[128,256]{1,0:T(8,128)(2,1)S(1)} %copy-done.14, ...), custom_call_target="tpu_custom_call" | custom-call | flops 300000000 | bytes 1114112 | tf_op jit(solution)/shard_map/pallas_call | solution.py:55
  (80 shorter events, 31.7 us)
Async XLA Ops:
  4.1 29.7 %all-to-all-start = ((bf16[64,8,512]{2,1,0:T(8,128)(2,1)}), bf16[64,8,512]{2,1,0:T(8,128)(2,1)S(1)}, u32[]{:S(2)}, u32[]{:S(2)}) async-start(bf16[64,8,512]{2,1,0:T(8,128)(2,1)} %bitcast.1), calls=%async_computation | async-start | bytes 1048576 | tf_op jit(solution)/shard_map/all_to_all | solution.py:384
  16.2 56.2 %copy-start = (bf16[1,2048,256]{2,1,0:T(8,128)(2,1)S(1)}, bf16[1,2048,256]{2,1,0:T(8,128)(2,1)}, u32[]{:S(2)}) copy-start(bf16[1,2048,256]{2,1,0:T(8,128)(2,1)} %param.18) | copy-start | bytes 3145732
  16.2 56.2 %copy-start.1 = (bf16[1,2048,256]{2,1,0:T(8,128)(2,1)S(1)}, bf16[1,2048,256]{2,1,0:T(8,128)(2,1)}, u32[]{:S(2)}) copy-start(bf16[1,2048,256]{2,1,0:T(8,128)(2,1)} %param.19) | copy-start | bytes 3145732
  33.8 23.4 %all-to-all-start.1 = ((bf16[64,8,512]{2,1,0:T(8,128)(2,1)}), bf16[64,8,512]{2,1,0:T(8,128)(2,1)S(1)}, u32[]{:S(2)}, u32[]{:S(2)}) async-start(bf16[64,8,512]{2,1,0:T(8,128)(2,1)} %bitcast.43), calls=%async_computation.1 | async-start | bytes 1048576 | tf_op jit(solution)/shard_map/all_to_all | solution.py:384
  39.6 14.0 %collective-permute-start = (bf16[512,512]{1,0:T(8,128)(2,1)S(1)}, bf16[512,512]{1,0:T(8,128)(2,1)S(1)}, u32[]{:S(2)}, u32[]{:S(2)}) collective-permute-start(bf16[512,512]{1,0:T(8,128)(2,1)S(1)} %bitcast.34), channel_id=1, source_target_pairs={{0,1},{1,2},{2,3},{3,0},{4,5},{5,6},{6,7},{7,4},{8,9},{9,10},{10,1... | collective-permute-start | bytes 1572872 | tf_op jit(solution)/shard_map/ppermute | solution.py:411
  41.2 18.2 %collective-permute-start.1 = (bf16[512,512]{1,0:T(8,128)(2,1)S(1)}, bf16[512,512]{1,0:T(8,128)(2,1)}, u32[]{:S(2)}, u32[]{:S(2)}) collective-permute-start(bf16[512,512]{1,0:T(8,128)(2,1)S(1)} %bitcast.35), channel_id=1, source_target_pairs={{0,3},{1,0},{2,1},{3,2},{4,7},{5,4},{6,5},{7,6},{8,11},{9,8},{10,9... | collective-permute-start | bytes 1572872 | tf_op jit(solution)/shard_map/ppermute | solution.py:412
  54.4 9.4 %collective-permute-start.2 = (bf16[256,512]{1,0:T(8,128)(2,1)}, bf16[256,512]{1,0:T(8,128)(2,1)S(1)}, u32[]{:S(2)}, u32[]{:S(2)}) collective-permute-start(bf16[256,512]{1,0:T(8,128)(2,1)} %slice.24), channel_id=1, source_target_pairs={{0,1},{1,2},{2,3},{3,0},{4,5},{5,6},{6,7},{7,4},{8,9},{9,10},{10,1... | collective-permute-start | bytes 786440 | tf_op jit(solution)/shard_map/ppermute | solution.py:413
  57.3 12.2 %collective-permute-start.4 = (bf16[256,512]{1,0:T(8,128)(2,1)S(1)}, bf16[256,512]{1,0:T(8,128)(2,1)S(1)}, u32[]{:S(2)}, u32[]{:S(2)}) collective-permute-start(bf16[256,512]{1,0:T(8,128)(2,1)S(1)} %get-tuple-element.95), channel_id=1, source_target_pairs={{0,1},{1,2},{2,3},{3,0},{4,5},{5,6},{6,7},{7,4},{8,9},{9,10},{10,1... | collective-permute-start | bytes 786440 | tf_op jit(solution)/shard_map/ppermute | solution.py:417
  58.8 12.1 %collective-permute-start.7 = (bf16[256,512]{1,0:T(8,128)(2,1)S(1)}, bf16[256,512]{1,0:T(8,128)(2,1)S(1)}, u32[]{:S(2)}, u32[]{:S(2)}) collective-permute-start(bf16[256,512]{1,0:T(8,128)(2,1)S(1)} %get-tuple-element.94), channel_id=1, source_target_pairs={{0,3},{1,0},{2,1},{3,2},{4,7},{5,4},{6,5},{7,6},{8,11},{9,8},{10,9... | collective-permute-start | bytes 786440 | tf_op jit(solution)/shard_map/ppermute | solution.py:418
  60.3 15.7 %collective-permute-start.3 = (bf16[256,512]{1,0:T(8,128)(2,1)S(1)}, bf16[256,512]{1,0:T(8,128)(2,1)S(1)}, u32[]{:S(2)}, u32[]{:S(2)}) collective-permute-start(bf16[256,512]{1,0:T(8,128)(2,1)S(1)} %slice.25), channel_id=1, source_target_pairs={{0,3},{1,0},{2,1},{3,2},{4,7},{5,4},{6,5},{7,6},{8,11},{9,8},{10,9... | collective-permute-start | bytes 786440 | tf_op jit(solution)/shard_map/ppermute | solution.py:414
  62.2 15.0 %collective-permute-start.5 = (bf16[256,512]{1,0:T(8,128)(2,1)S(1)}, bf16[256,512]{1,0:T(8,128)(2,1)S(1)}, u32[]{:S(2)}, u32[]{:S(2)}) collective-permute-start(bf16[256,512]{1,0:T(8,128)(2,1)S(1)} %get-tuple-element.94), channel_id=1, source_target_pairs={{0,1},{1,2},{2,3},{3,0},{4,5},{5,6},{6,7},{7,4},{8,9},{9,10},{10,1... | collective-permute-start | bytes 786440 | tf_op jit(solution)/shard_map/ppermute | solution.py:419
  63.8 15.4 %collective-permute-start.6 = (bf16[256,512]{1,0:T(8,128)(2,1)S(1)}, bf16[256,512]{1,0:T(8,128)(2,1)S(1)}, u32[]{:S(2)}, u32[]{:S(2)}) collective-permute-start(bf16[256,512]{1,0:T(8,128)(2,1)S(1)} %get-tuple-element.95), channel_id=1, source_target_pairs={{0,3},{1,0},{2,1},{3,2},{4,7},{5,4},{6,5},{7,6},{8,11},{9,8},{10,9... | collective-permute-start | bytes 786440 | tf_op jit(solution)/shard_map/ppermute | solution.py:420
  69.4 11.0 %collective-permute-start.8 = (bf16[256,512]{1,0:T(8,128)(2,1)S(1)}, bf16[256,512]{1,0:T(8,128)(2,1)S(1)}, u32[]{:S(2)}, u32[]{:S(2)}) collective-permute-start(bf16[256,512]{1,0:T(8,128)(2,1)S(1)} %collective-permute-done.4.t1_ref), channel_id=1, source_target_pairs={{0,1},{1,2},{2,3},{3,0},{4,5},{5,6},{6,7},{7,4},{8,9},{9,10},{10,1... | collective-permute-start | bytes 786440 | tf_op jit(solution)/shard_map/ppermute | solution.py:421
  70.9 12.8 %collective-permute-start.9 = (bf16[256,512]{1,0:T(8,128)(2,1)S(1)}, bf16[256,512]{1,0:T(8,128)(2,1)S(1)}, u32[]{:S(2)}, u32[]{:S(2)}) collective-permute-start(bf16[256,512]{1,0:T(8,128)(2,1)S(1)} %collective-permute-done.7.b2_ref), channel_id=1, source_target_pairs={{0,3},{1,0},{2,1},{3,2},{4,7},{5,4},{6,5},{7,6},{8,11},{9,8},{10,9... | collective-permute-start | bytes 786440 | tf_op jit(solution)/shard_map/ppermute | solution.py:422
  85.0 8.5 %collective-permute-start.10 = (bf16[256,512]{1,0:T(8,128)(2,1)S(1)}, bf16[256,512]{1,0:T(8,128)(2,1)S(1)}, u32[]{:S(2)}, u32[]{:S(2)}) collective-permute-start(bf16[256,512]{1,0:T(8,128)(2,1)S(1)} %get-tuple-element.71), channel_id=1, source_target_pairs={{0,1},{1,2},{2,3},{3,0},{4,5},{5,6},{6,7},{7,4},{8,9},{9,10},{10,1... | collective-permute-start | bytes 786440 | tf_op jit(solution)/shard_map/ppermute | solution.py:439
  86.3 9.2 %collective-permute-start.11 = (bf16[256,512]{1,0:T(8,128)(2,1)S(1)}, bf16[256,512]{1,0:T(8,128)(2,1)S(1)}, u32[]{:S(2)}, u32[]{:S(2)}) collective-permute-start(bf16[256,512]{1,0:T(8,128)(2,1)S(1)} %get-tuple-element.72), channel_id=1, source_target_pairs={{0,3},{1,0},{2,1},{3,2},{4,7},{5,4},{6,5},{7,6},{8,11},{9,8},{10,9... | collective-permute-start | bytes 786440 | tf_op jit(solution)/shard_map/ppermute | solution.py:440
  88.4 16.1 %collective-permute-start.13 = (bf16[256,512]{1,0:T(8,128)(2,1)S(1)}, bf16[256,512]{1,0:T(8,128)(2,1)S(1)}, u32[]{:S(2)}, u32[]{:S(2)}) collective-permute-start(bf16[256,512]{1,0:T(8,128)(2,1)S(1)} %get-tuple-element.74), channel_id=1, source_target_pairs={{0,3},{1,0},{2,1},{3,2},{4,7},{5,4},{6,5},{7,6},{8,11},{9,8},{10,9... | collective-permute-start | bytes 786440 | tf_op jit(solution)/shard_map/ppermute | solution.py:443
  90.2 14.3 %collective-permute-start.14 = (bf16[256,512]{1,0:T(8,128)(2,1)S(1)}, bf16[256,512]{1,0:T(8,128)(2,1)S(1)}, u32[]{:S(2)}, u32[]{:S(2)}) collective-permute-start(bf16[256,512]{1,0:T(8,128)(2,1)S(1)} %get-tuple-element.75), channel_id=1, source_target_pairs={{0,1},{1,2},{2,3},{3,0},{4,5},{5,6},{6,7},{7,4},{8,9},{9,10},{10,1... | collective-permute-start | bytes 786440 | tf_op jit(solution)/shard_map/ppermute | solution.py:442
  96.1 8.4 %collective-permute-start.12 = (bf16[256,512]{1,0:T(8,128)(2,1)S(1)}, bf16[256,512]{1,0:T(8,128)(2,1)S(1)}, u32[]{:S(2)}, u32[]{:S(2)}) collective-permute-start(bf16[256,512]{1,0:T(8,128)(2,1)S(1)} %get-tuple-element.73), channel_id=1, source_target_pairs={{0,1},{1,2},{2,3},{3,0},{4,5},{5,6},{6,7},{7,4},{8,9},{9,10},{10,1... | collective-permute-start | bytes 786440 | tf_op jit(solution)/shard_map/ppermute | solution.py:445
  97.9 6.6 %collective-permute-start.15 = (bf16[256,512]{1,0:T(8,128)(2,1)S(1)}, bf16[256,512]{1,0:T(8,128)(2,1)S(1)}, u32[]{:S(2)}, u32[]{:S(2)}) collective-permute-start(bf16[256,512]{1,0:T(8,128)(2,1)S(1)} %get-tuple-element.76), channel_id=1, source_target_pairs={{0,3},{1,0},{2,1},{3,2},{4,7},{5,4},{6,5},{7,6},{8,11},{9,8},{10,9... | collective-permute-start | bytes 786440 | tf_op jit(solution)/shard_map/ppermute | solution.py:446
  104.5 38.9 %copy-start.6 = (bf16[2048,256]{1,0:T(8,128)(2,1)S(1)}, bf16[2048,256]{1,0:T(8,128)(2,1)}, u32[]{:S(2)}) copy-start(bf16[2048,256]{1,0:T(8,128)(2,1)} %w_ref.1) | copy-start | bytes 3145732
  104.5 38.9 %copy-start.10 = (bf16[512,128]{1,0:T(8,128)(2,1)S(1)}, bf16[512,128]{1,0:T(8,128)(2,1)}, u32[]{:S(2)}) copy-start(bf16[512,128]{1,0:T(8,128)(2,1)} %copy-done.9) | copy-start | bytes 393220
  104.5 38.9 %copy-start.13 = (f32[128,128]{1,0:T(8,128)S(1)}, f32[128,128]{1,0:T(8,128)}, u32[]{:S(2)}) copy-start(f32[128,128]{1,0:T(8,128)} %copy-done.12) | copy-start | bytes 196612
  131.6 5.6 %collective-permute-start.16 = (bf16[128,512]{1,0:T(8,128)(2,1)S(1)}, bf16[128,512]{1,0:T(8,128)(2,1)S(1)}, u32[]{:S(2)}, u32[]{:S(2)}) collective-permute-start(bf16[128,512]{1,0:T(8,128)(2,1)S(1)} %shard_map.207.m0_ref), channel_id=1, source_target_pairs={{0,1},{1,2},{2,3},{3,0},{4,5},{5,6},{6,7},{7,4},{8,9},{9,10},{10,1... | collective-permute-start | bytes 393224 | tf_op jit(solution)/shard_map/ppermute | solution.py:466
  133.3 5.4 %collective-permute-start.17 = (bf16[128,512]{1,0:T(8,128)(2,1)S(1)}, bf16[128,512]{1,0:T(8,128)(2,1)S(1)}, u32[]{:S(2)}, u32[]{:S(2)}) collective-permute-start(bf16[128,512]{1,0:T(8,128)(2,1)S(1)} %shard_map.207.m0_ref), channel_id=1, source_target_pairs={{0,3},{1,0},{2,1},{3,2},{4,7},{5,4},{6,5},{7,6},{8,11},{9,8},{10,9... | collective-permute-start | bytes 393224 | tf_op jit(solution)/shard_map/ppermute | solution.py:467
  133.7 8.6 %collective-permute-start.18 = (bf16[128,512]{1,0:T(8,128)(2,1)S(1)}, bf16[128,512]{1,0:T(8,128)(2,1)S(1)}, u32[]{:S(2)}, u32[]{:S(2)}) collective-permute-start(bf16[128,512]{1,0:T(8,128)(2,1)S(1)} %shard_map.207.m0_ref), channel_id=1, source_target_pairs={{0,2},{1,3},{2,0},{3,1},{4,6},{5,7},{6,4},{7,5},{8,10},{9,11},{10,... | collective-permute-start | bytes 393224 | tf_op jit(solution)/shard_map/ppermute | solution.py:465
  143.3 7.7 %collective-permute-start.19 = (bf16[1024,256]{1,0:T(8,128)(2,1)S(1)}, bf16[1024,256]{1,0:T(8,128)(2,1)S(1)}, u32[]{:S(2)}, u32[]{:S(2)}) collective-permute-start(bf16[1024,256]{1,0:T(8,128)(2,1)S(1)} %get-tuple-element.84), channel_id=1, source_target_pairs={{0,4},{4,0},{8,12},{12,8},{16,20},{20,16},{24,28},{28,24},{32,36},... | collective-permute-start | bytes 1572872 | tf_op jit(solution)/shard_map/ppermute | solution.py:477
  145.6 18.4 %all-to-all-start.3 = ((bf16[64,8,256]{2,1,0:T(8,128)(2,1)}), bf16[64,8,256]{2,1,0:T(8,128)(2,1)S(1)}, u32[]{:S(2)}, u32[]{:S(2)}) async-start(bf16[64,8,256]{2,1,0:T(8,128)(2,1)} %bitcast.16), calls=%async_computation.3 | async-start | bytes 524288 | tf_op jit(solution)/shard_map/all_to_all | solution.py:384
  151.9 12.1 %collective-permute-start.20 = (bf16[512,128]{1,0:T(8,128)(2,1)S(1)}, bf16[512,128]{1,0:T(8,128)(2,1)S(1)}, u32[]{:S(2)}, u32[]{:S(2)}) collective-permute-start(bf16[512,128]{1,0:T(8,128)(2,1)S(1)} %get-tuple-element.86), channel_id=1, source_target_pairs={{0,16},{4,20},{8,24},{12,28},{16,0},{20,4},{24,8},{28,12},{32,48},... | collective-permute-start | bytes 393224 | tf_op jit(solution)/shard_map/ppermute | solution.py:479
  155.0 9.2 %collective-permute-start.21 = (bf16[512,128]{1,0:T(8,128)(2,1)S(1)}, bf16[512,128]{1,0:T(8,128)(2,1)S(1)}, u32[]{:S(2)}, u32[]{:S(2)}) collective-permute-start(bf16[512,128]{1,0:T(8,128)(2,1)S(1)} %get-tuple-element.87), channel_id=1, source_target_pairs={{0,8},{4,12},{8,16},{12,20},{16,24},{20,28},{24,0},{28,4},{32,40},... | collective-permute-start | bytes 393224 | tf_op jit(solution)/shard_map/ppermute | solution.py:479
  155.6 8.6 %collective-permute-start.22 = (bf16[512,128]{1,0:T(8,128)(2,1)S(1)}, bf16[512,128]{1,0:T(8,128)(2,1)S(1)}, u32[]{:S(2)}, u32[]{:S(2)}) collective-permute-start(bf16[512,128]{1,0:T(8,128)(2,1)S(1)} %get-tuple-element.88), channel_id=1, source_target_pairs={{0,24},{4,28},{8,0},{12,4},{16,8},{20,12},{24,16},{28,20},{32,56},... | collective-permute-start | bytes 393224 | tf_op jit(solution)/shard_map/ppermute | solution.py:479
  166.0 21.5 %all-to-all-start.4 = ((bf16[64,8,256]{2,1,0:T(8,128)(2,1)}), bf16[64,8,256]{2,1,0:T(8,128)(2,1)S(1)}, u32[]{:S(2)}, u32[]{:S(2)}) async-start(bf16[64,8,256]{2,1,0:T(8,128)(2,1)} %bitcast.18), calls=%async_computation.4 | async-start | bytes 524288 | tf_op jit(solution)/shard_map/all_to_all | solution.py:384
  (13 other events, 178.6 us)

commit v4 on v3

--- a/solution.py
+++ b/solution.py
@@ -16,6 +16,8 @@
 EXPERTS = 64
 CAP = 8
 SLOTS = EXPERTS * CAP
+SIDE = SLOTS // 2
+CHIPS = EXPERTS // 2
 WIDTH = 2048
 QUART = 512
 FF = 256
@@ -111,7 +113,11 @@
     return jnp.concatenate(halves, axis=1)
 
 
-def pick_kernel(q_ref, ids_ref, x_ref, rows_ref, pick_ref, slot_ref):
+def pick_kernel(ids_ref, x_ref, keep_ref, give_ref, pick_ref, slot_ref, own_ref, sem):
+    start = pl.multiple_of(lax.axis_index("tp") * QUART, QUART)
+    copy = pltpu.make_async_copy(x_ref.at[:, pl.ds(start, QUART)], own_ref, sem)
+    copy.start()
+    core = lax.rem(lax.axis_index("sp"), 2)
     expert = iota((EXPERTS, TOK), 0)
     id0, id1 = ids_ref[0:1, :], ids_ref[1:2, :]
     hit0, hit1 = expert == id0, expert == id1
@@ -120,19 +126,32 @@
     count = dot(named, before, 1, 0)
     rank0 = jnp.sum(jnp.where(hit0, count, 0.0), axis=0, keepdims=True)
     rank1 = jnp.sum(jnp.where(hit1, count, 0.0), axis=0, keepdims=True)
-    slot0 = id0 * CAP + rank0.astype(jnp.int32)
-    slot1 = id1 * CAP + rank1.astype(jnp.int32)
+
+    def slot_of(expert_id, rank):
+        side = jnp.bitwise_xor(jnp.bitwise_and(expert_id, 1), core)
+        return side * SIDE + (expert_id // 2) * CAP + rank.astype(jnp.int32)
+
+    slot0, slot1 = slot_of(id0, rank0), slot_of(id1, rank1)
     slot_ref[0:1, :] = slot0
     slot_ref[1:2, :] = slot1
     slot = iota((SLOTS, TOK), 0)
     pick = ((slot == slot0).astype(F32) + (slot == slot1).astype(F32)).astype(BF)
     pick_ref[...] = pick
-    rows_ref[...] = dot(pick, x_ref[...], 1, 0).astype(BF)
+    copy.wait()
+    rows = dot(pick, own_ref[...], 1, 0).astype(BF)
+    keep_ref[...] = rows[:SIDE]
+    give_ref[...] = rows[SIDE:]
+
+
+def weave_kernel(q_ref, keep_ref, got_ref, out_ref):
+    keep = keep_ref[...].astype(F32).reshape(CHIPS, CAP, QUART)
+    got = got_ref[...].astype(F32).reshape(CHIPS, CAP, QUART)
+    out_ref[...] = jnp.concatenate([keep, got], axis=1).reshape(SLOTS, QUART).astype(BF)
 
 
 def local_kernel(
     q_ref, slot_ref, w_ref, pick_ref, oc_ref, qry_ref, k_ref, v_ref, g_ref,
-    rows_ref, tile_ref, cum_ref, dec_ref,
+    keep_ref, give_ref, tile_ref, cum_ref, dec_ref,
 ):
     slot = iota((SLOTS, TOK), 0)
     at0, at1 = slot == slot_ref[0:1, :], slot == slot_ref[1:2, :]
@@ -141,7 +160,9 @@
         axis=1,
         keepdims=True,
     )
-    rows_ref[...] = (dot(pick_ref[...], oc_ref[...], 1, 0) * weight).astype(BF)
+    rows = (dot(pick_ref[...], oc_ref[...], 1, 0) * weight).astype(BF)
+    keep_ref[...] = rows[:SIDE]
+    give_ref[...] = rows[SIDE:]
     g = g_ref[...]
     cum = cumulative_sum(g)
     cum_ref[...] = cum
@@ -220,23 +241,28 @@
     b_ref[...] = (lb_ref[...].astype(F32) + from_right_ref[...].astype(F32)).astype(BF)
 
 
-def weight_kernel(
-    q_ref, x0_ref, x1_ref, x2_ref, xt_ref, xb_ref,
-    y0_ref, t1_ref, b1_ref, t2_ref, b2_ref, t3_ref, b3_ref,
-    hid_ref, gu_ref, wg_ref, wu_ref, gg_ref, gup_ref, gd_ref, own_ref,
+def down_kernel(
+    q_ref, y0_ref, t1_ref, b1_ref, t2_ref, b2_ref, t3_ref, b3_ref, hid_ref, gu_ref, wg_ref, wu_ref,
+    gd_ref, own_ref,
 ):
     own_ref[...] = back_rows(gu_ref, wg_ref, wu_ref, quarter_rows(q_ref[0]))
     hid_t = hid_ref[...].T
-    gu = gu_ref[...]
     pairs = ((t1_ref, b1_ref), (t2_ref, b2_ref), (t3_ref, b3_ref))
     cots = [y0_ref[...]] + [jnp.concatenate([t[...], b[...]], axis=0) for t, b in pairs]
+    for n, dy in enumerate(cots):
+        gd_ref[:, quarter_rows(q_ref[n])] = dot(hid_t, dy, 1, 0)
+
+
+def weight_kernel(
+    q_ref, x0_ref, x1_ref, x2_ref, xt_ref, xb_ref, gu_ref, gg_ref, gup_ref
+):
+    gu = gu_ref[...]
     far = jnp.concatenate([xt_ref[...], xb_ref[...]], axis=0)
     for n, x in enumerate((x0_ref[...], x1_ref[...], x2_ref[...], far)):
         rows = quarter_rows(q_ref[n])
         both = dot(x.T, gu, 1, 0)
         gg_ref[rows, :] = both[:, :FF]
         gup_ref[rows, :] = both[:, FF:]
-        gd_ref[:, rows] = dot(hid_t, cots[n], 1, 0)
 
 
 def sum_kernel(q_ref, own_ref, tl_ref, tr_ref, bl_ref, br_ref, out_ref):
@@ -245,8 +271,11 @@
         out_ref[rows, :] = (own_ref[rows, :].astype(F32) + got).astype(BF)
 
 
-def combine_kernel(q_ref, rows_ref, pick_ref, oc_ref, out_ref):
-    routed = dot(pick_ref[...].T, rows_ref[...], 1, 0)
+def combine_kernel(q_ref, rows_ref, got_ref, pick_ref, oc_ref, out_ref):
+    keep = rows_ref[...].astype(F32).reshape(CHIPS, 2 * CAP, QUART)[:, :CAP, :]
+    keep = keep.reshape(SIDE, QUART).astype(BF)
+    pick = pick_ref[...].T
+    routed = dot(pick[:, :SIDE], keep, 1, 0) + dot(pick[:, SIDE:], got_ref[...], 1, 0)
     out_ref[...] = (oc_ref[...].astype(F32) + routed).astype(BF)
 
 
@@ -389,16 +418,34 @@
 
     rows_type = sds((SLOTS, QUART), BF)
     tile_type = sds((SLOTS, LANES), BF)
-    x_rows, pick, slots = run(
+    side_type = sds((SIDE, QUART), BF)
+
+    def between_chips(rows):
+        groups = [list(range(core, 64, 2)) for core in range(2)]
+        got = lax.all_to_all(
+            rows.reshape(CHIPS, 2 * CAP, QUART), "sp", 0, 0, tiled=True, axis_index_groups=groups
+        )
+        return got.reshape(SLOTS, QUART)
+
+    x_keep, x_give, pick, slots = pl.pallas_call(
         pick_kernel,
-        (rows_type, sds((SLOTS, TOK), BF), sds((2, TOK), jnp.int32)),
-        (in_hbm(route_ids.T), in_hbm(expert_in)),
-        in_specs=[None, quarter_block()],
-        flops=1e8,
-    )
-    y_rows, state_tile, cum, q_dec = run(
+        out_shape=(side_type, side_type, sds((SLOTS, TOK), BF), sds((2, TOK), jnp.int32)),
+        in_specs=[
+            pl.BlockSpec(memory_space=pltpu.VMEM),
+            pl.BlockSpec(memory_space=pltpu.HBM),
+        ],
+        out_specs=(pl.BlockSpec(memory_space=pltpu.VMEM),) * 4,
+        scratch_shapes=[pltpu.VMEM((TOK, QUART), BF), pltpu.SemaphoreType.DMA],
+        compiler_params=pltpu.CompilerParams(vmem_limit_bytes=24 * 2**20),
+        cost_estimate=pl.CostEstimate(
+            flops=10**8, bytes_accessed=2 * 10**6, transcendentals=0
+        ),
+    )(in_hbm(route_ids.T), expert_in)
+    x_got = lax.ppermute(x_give, "sp", other_core)
+    x_rows = run(weave_kernel, rows_type, (x_keep, x_got), flops=1e6)
+    y_keep, y_give, state_tile, cum, q_dec = run(
         local_kernel,
-        (rows_type, tile_type, sds((TOK, DK), F32), sds((TOK, DK), F32)),
+        (side_type, side_type, tile_type, sds((TOK, DK), F32), sds((TOK, DK), F32)),
         (
             slots, in_hbm(route_weights.T), pick, in_hbm(out_cot), in_hbm(queries), in_hbm(keys),
             in_hbm(values), in_hbm(log_decay),
@@ -406,13 +453,15 @@
         in_specs=[None, None, None, quarter_block(), None, None, None, None],
         flops=3e8,
     )
-    x0 = exchange(x_rows)
+    y_got = lax.ppermute(y_give, "sp", other_core)
+    y_rows = run(weave_kernel, rows_type, (y_keep, y_got), flops=1e6)
+    x0 = between_chips(x_rows)
     x0, y_rows = lax.optimization_barrier((x0, y_rows))
     x1 = lax.ppermute(x0, "tp", to_right)
     x2 = lax.ppermute(x0, "tp", to_left)
     xt3 = lax.ppermute(x1[TOP], "tp", to_right)
     xb3 = lax.ppermute(x2[BOTTOM], "tp", to_left)
-    y0 = exchange(y_rows)
+    y0 = between_chips(y_rows)
     y_top, y_bottom = y0[TOP], y0[BOTTOM]
     t1 = lax.ppermute(y_top, "tp", to_right)
     b2 = lax.ppermute(y_bottom, "tp", to_left)
@@ -441,25 +490,33 @@
     p_rt, p_rb, p_lt, p_lb = run(sides_kernel, (part_type,) * 4, (gate_up, wg, wu), flops=5e8)
     bl = lax.ppermute(p_rb, "tp", to_right)
     tr = lax.ppermute(p_lt, "tp", to_left)
+    grad_down, p_own = run(
+        down_kernel,
+        (sds((FF, WIDTH), F32), rows_type),
+        (y0, t1, b1, t2, b2, t3, b3, hidden, gate_up, wg, wu),
+        flops=8e8,
+    )
+    far_top, p_own = lax.optimization_barrier((far_top, p_own))
     p_t, p_b = run(merge_kernel, (part_type,) * 2, (p_rt, p_lb, far_top, far_bottom), flops=1e6)
     tl = lax.ppermute(p_t, "tp", to_right)
     br = lax.ppermute(p_b, "tp", to_left)
-    *grads, p_own = run(
+    grads = run(
         weight_kernel,
-        (sds((WIDTH, FF), F32), sds((WIDTH, FF), F32), sds((FF, WIDTH), F32), rows_type),
-        (
-            x0, x1, x2, xt3, xb3, y0, t1, b1, t2, b2, t3, b3, hidden, gate_up, wg, wu,
-        ),
-        flops=1.9e9,
-    )
-    grad_gate, grad_up, grad_down = grads
+        (sds((WIDTH, FF), F32), sds((WIDTH, FF), F32)),
+        (x0, x1, x2, xt3, xb3, gate_up),
+        flops=1.1e9,
+    )
+    p_own, grads = lax.optimization_barrier((p_own, grads))
+    grad_gate, grad_up = grads
     total = run(sum_kernel, rows_type, (p_own, tl, tr, bl, br), flops=1e6)
-    back = exchange(total)
+    back = between_chips(total)
+    give = back.reshape(CHIPS, 2 * CAP, QUART)[:, CAP:, :].reshape(SIDE, QUART)
+    got = lax.ppermute(give, "sp", other_core)
     mid = run(
         combine_kernel,
         sds((TOK, QUART), BF),
-        (back, pick, out_cot),
-        in_specs=[None, None, quarter_block()],
+        (back, got, pick, out_cot),
+        in_specs=[None, None, None, quarter_block()],
         flops=7e7,
     )
     m_far = lax.ppermute(mid, "tp", across)

time: 192 us -> 187 us (0.974)
  waiting for transfers between devices: 63.5 us -> 59.1 us
  blocking collectives: 25.5 us -> 22.6 us
  Pallas kernels: 29.8 us -> 32.6 us
    all_to_all x4 -> x2, starting transfers between devices: 31.9 us -> 13.7 us  [exchange(): lax.all_to_all(rows.reshape(EXPERTS, CAP, width), 'sp', 0, 0, tiled=True)]
    all_to_all x0 -> x2, starting transfers between devices: none -> 16.1 us  [between_chips(): lax.all_to_all(rows.reshape(CHIPS, 2 * CAP, QUART), 'sp', 0, 0, tiled=Tru...]
    all_to_all x4 -> x2, waiting for transfers between devices: 30.8 us -> 17.1 us  [exchange(): lax.all_to_all(rows.reshape(EXPERTS, CAP, width), 'sp', 0, 0, tiled=True)]
    all_to_all x0 -> x2, waiting for transfers between devices: none -> 13.5 us  [between_chips(): lax.all_to_all(rows.reshape(CHIPS, 2 * CAP, QUART), 'sp', 0, 0, tiled=Tru...]
    all_to_all x1, blocking collectives: 25.5 us -> 22.6 us  [between_chips(): lax.all_to_all(rows.reshape(CHIPS, 2 * CAP, QUART), 'sp', 0, 0, tiled=Tru...]
    ppermute x0 -> x2, waiting for transfers between devices: none -> 2.28 us  [the longest x1 1.53 us: per_device(): y_got = lax.ppermute(y_give, 'sp', other_core)]
    ppermute x1, waiting for transfers between devices: 3 us -> 0.87 us  [per_device(): far_top = lax.ppermute(p_top, 'tp', to_right)]
    ppermute x1, waiting for transfers between devices: 1.97 us -> 0.01 us  [per_device(): far_bottom = lax.ppermute(p_bottom, 'tp', to_left)]
  transfers between devices with their start and end apart: 27 -> 30, of which waited for: 15 -> 18; matrix products, arithmetic and copies ran while one was open for 1% -> 1% of each run, Pallas kernels for 10% -> 12%
where the time goes in v4:
time: 187 us; the launch traced here: 184 us
  starting transfers between devices  62.8 us (34%)
  waiting for transfers between devices  59.1 us (32%)
  Pallas kernels  32.6 us (17%)
  blocking collectives  22.6 us (12%)
  local copies, waits for them, and re-layouts  6.08 us (3%)
    pallas_call x19, Pallas kernels, call(): pl.pallas_call(kernel, out_shape=out_shape, grid_spec=pltpu.PrefetchScala...  31.4 us
    all_to_all x1, blocking collectives, between_chips(): lax.all_to_all(rows.reshape(CHIPS, 2 * CAP, QUART), 'sp', 0, 0, tiled=Tru...  22.6 us
    all_to_all x2, waiting for transfers between devices, exchange(): lax.all_to_all(rows.reshape(EXPERTS, CAP, width), 'sp', 0, 0, tiled=True)  17.1 us
    all_to_all x2, starting transfers between devices, between_chips(): lax.all_to_all(rows.reshape(CHIPS, 2 * CAP, QUART), 'sp', 0, 0, tiled=Tru...  16.1 us
    all_to_all x2, starting transfers between devices, exchange(): lax.all_to_all(rows.reshape(EXPERTS, CAP, width), 'sp', 0, 0, tiled=True)  13.7 us
    all_to_all x2, waiting for transfers between devices, between_chips(): lax.all_to_all(rows.reshape(CHIPS, 2 * CAP, QUART), 'sp', 0, 0, tiled=Tru...  13.5 us
    ppermute x1, waiting for transfers between devices, per_device(): x1 = lax.ppermute(x0, 'tp', to_right)  10.5 us
    ppermute x3, starting transfers between devices, per_device(): adds = [lax.ppermute(tiles[k], 'sp', along_y(k)) for k in (2, 1, 3)]  6.4 us
  transfers between devices with their start and end apart: 30, of which 18 were waited for; matrix products, arithmetic and copies ran while one was open for 1% of the time, Pallas kernels for 12%

profile of v4, /device:TPU:2, one launch (start us, length us, event | category | flops | bytes accessed | tf_op | source)
XLA Modules:
  0.0 184.2 jit_solution(15381207933626674913)
XLA Ops:
  5.9 11.5 %all-to-all-start = ((bf16[32,16,512]{2,1,0:T(8,128)(2,1)}), bf16[32,16,512]{2,1,0:T(8,128)(2,1)S(1)}, u32[]{:S(2)}, u32[]{:S(2)}) async-start(bf16[32,16,512]{2,1,0:T(8,128)(2,1)} %bitcast.1), calls=%async_computation | async-start | bytes 1048576 | tf_op jit(solution)/shard_map/all_to_all | solution.py:425
  17.4 2.4 %shard_map.199 = (bf16[256,512]{1,0:T(8,128)(2,1)S(1)}, bf16[256,512]{1,0:T(8,128)(2,1)S(1)}, bf16[512,128]{1,0:T(8,128)(2,1)S(1)}, f32[128,128]{1,0:T(8,128)S(1)}, f32[128,128]{1,0:T(8,128)S(1)}) custom-call(s32[6]{0:T(128)S(1)} %dynamic_slice.3.q_ref, s32[2,128]{1,0:T(2,128)S(1)} %get-tuple-element.60.slot_ref, f32[2,128]{1,0:T(2,128)} %bitcast.50, ...), custom_call_target="tpu_custom_call" | custom-call | flops 300000000 | bytes 1640448 | tf_op jit(solution)/shard_map/pallas_call | solution.py:57
  21.2 1.5 collective-permute-done.1.got_ref
  24.1 11.4 %all-to-all-done = bf16[32,16,512]{2,1,0:T(8,128)(2,1)S(1)} async-done(((bf16[32,16,512]{2,1,0:T(8,128)(2,1)}), bf16[32,16,512]{2,1,0:T(8,128)(2,1)S(1)}, u32[]{:S(2)}, u32[]{:S(2)}) %all-to-all-start) | async-done | bytes 524320 | tf_op jit(solution)/shard_map/all_to_all | solution.py:425
  35.5 4.6 %all-to-all-start.1 = ((bf16[32,16,512]{2,1,0:T(8,128)(2,1)}), bf16[32,16,512]{2,1,0:T(8,128)(2,1)S(1)}, u32[]{:S(2)}, u32[]{:S(2)}) async-start(bf16[32,16,512]{2,1,0:T(8,128)(2,1)} %bitcast.4), calls=%async_computation.1 | async-start | bytes 1048576 | tf_op jit(solution)/shard_map/all_to_all | solution.py:425
  40.1 1.6 collective-permute-start.8
  42.2 10.5 %collective-permute-done.8.x1_ref = bf16[512,512]{1,0:T(8,128)(2,1)S(1)} collective-permute-done((bf16[512,512]{1,0:T(8,128)(2,1)S(1)}, bf16[512,512]{1,0:T(8,128)(2,1)S(1)}, u32[]{:S(2)}, u32[]{:S(2)}) %collective-permute-start.8) | collective-permute-done | bytes 524320 | tf_op jit(solution)/shard_map/ppermute | solution.py:460
  55.1 2.0 %all-to-all-done.1 = bf16[32,16,512]{2,1,0:T(8,128)(2,1)S(1)} async-done(((bf16[32,16,512]{2,1,0:T(8,128)(2,1)}), bf16[32,16,512]{2,1,0:T(8,128)(2,1)S(1)}, u32[]{:S(2)}, u32[]{:S(2)}) %all-to-all-start.1) | async-done | bytes 524320 | tf_op jit(solution)/shard_map/all_to_all | solution.py:425
  57.2 1.6 collective-permute-start.2
  60.2 1.8 collective-permute-start.11
  63.0 3.0 %collective-permute-start.4 = (bf16[256,512]{1,0:T(8,128)(2,1)S(1)}, bf16[256,512]{1,0:T(8,128)(2,1)S(1)}, u32[]{:S(2)}, u32[]{:S(2)}) collective-permute-start(bf16[256,512]{1,0:T(8,128)(2,1)S(1)} %bitcast.45), channel_id=1, source_target_pairs={{0,3},{1,0},{2,1},{3,2},{4,7},{5,4},{6,5},{7,6},{8,11},{9,8},{10,9... | collective-permute-start | bytes 786440 | tf_op jit(solution)/shard_map/ppermute | solution.py:469
  66.0 2.7 %collective-permute-done.2.t1_ref = bf16[256,512]{1,0:T(8,128)(2,1)S(1)} collective-permute-done((bf16[256,512]{1,0:T(8,128)(2,1)S(1)}, bf16[256,512]{1,0:T(8,128)(2,1)S(1)}, u32[]{:S(2)}, u32[]{:S(2)}) %collective-permute-start.2) | collective-permute-done | bytes 262176 | tf_op jit(solution)/shard_map/ppermute | solution.py:466
  72.6 2.6 %shard_map.202 = (f32[512,256]{1,0:T(8,128)S(1)}, f32[512,256]{1,0:T(8,128)S(1)}) custom-call(s32[6]{0:T(128)S(1)} %dynamic_slice.3.q_ref, bf16[512,512]{1,0:T(8,128)(2,1)S(1)} %bitcast.40, bf16[512,512]{1,0:T(8,128)(2,1)S(1)} %copy-done.4, bf16[512,512]{1,0:T(8,128)(2,1)} %collective-permute-done.9.x2_ref, bf16[2048,256]{1,0:T(8,128)(2,1)S(1)} %bitcast.22, ...), custom_call_target="tpu_custom_call" | custom-call | flops 800000000 | bytes 4718592 | tf_op jit(solution)/shard_map/pallas_call | solution.py:57
  78.8 1.6 collective-permute-done.7.b3_ref
  85.1 1.8 collective-permute-start.15
  87.2 2.9 %shard_map.205 = (f32[256,2048]{1,0:T(8,128)}, bf16[512,512]{1,0:T(8,128)(2,1)S(1)}) custom-call(s32[6]{0:T(128)S(1)} %dynamic_slice.3.q_ref, bf16[512,512]{1,0:T(8,128)(2,1)S(1)} %bitcast.33, bf16[256,512]{1,0:T(8,128)(2,1)S(1)} %collective-permute-done.2.t1_ref, bf16[256,512]{1,0:T(8,128)(2,1)S(1)} %collective-permute-done.3.b1_ref, ...), custom_call_target="tpu_custom_call" | custom-call | flops 800000000 | bytes 7602176 | tf_op jit(solution)/shard_map/pallas_call | solution.py:57
  93.7 4.9 %shard_map.206 = (f32[2048,256]{1,0:T(8,128)}, f32[2048,256]{1,0:T(8,128)}) custom-call(s32[6]{0:T(128)S(1)} %dynamic_slice.3.q_ref, bf16[512,512]{1,0:T(8,128)(2,1)S(1)} %bitcast.41, bf16[512,512]{1,0:T(8,128)(2,1)S(1)} %copy-done.5, bf16[512,512]{1,0:T(8,128)(2,1)} %collective-permute-done.9.x2_ref, ...), custom_call_target="tpu_custom_call" | custom-call | flops 1100000000 | bytes 6815744 | tf_op jit(solution)/shard_map/pallas_call | solution.py:57
  100.1 22.6 %all_to_all.25 = bf16[32,16,512]{2,1,0:T(8,128)(2,1)S(1)} all-to-all(bf16[32,16,512]{2,1,0:T(8,128)(2,1)S(1)} %bitcast.37), channel_id=1, replica_groups={{0,8,16,24,32,40,48,56,64,72,80,88,96,104,112,120,128,136,144,152,160,1..., dimensions={0} | all-to-all | bytes 1048576 | tf_op jit(solution)/shard_map/all_to_all | solution.py:425
  122.8 1.5 collective-permute-done.18.got_ref
  125.2 1.9 %collective-permute-start.19 = (bf16[128,512]{1,0:T(8,128)(2,1)S(1)}, bf16[128,512]{1,0:T(8,128)(2,1)S(1)}, u32[]{:S(2)}, u32[]{:S(2)}) collective-permute-start(bf16[128,512]{1,0:T(8,128)(2,1)S(1)} %shard_map.210.m0_ref), channel_id=1, source_target_pairs={{0,1},{1,2},{2,3},{3,0},{4,5},{5,6},{6,7},{7,4},{8,9},{9,10},{10,1... | collective-permute-start | bytes 393224 | tf_op jit(solution)/shard_map/ppermute | solution.py:523
  128.3 3.2 %collective-permute-start.21 = (bf16[128,512]{1,0:T(8,128)(2,1)S(1)}, bf16[128,512]{1,0:T(8,128)(2,1)S(1)}, u32[]{:S(2)}, u32[]{:S(2)}) collective-permute-start(bf16[128,512]{1,0:T(8,128)(2,1)S(1)} %shard_map.210.m0_ref), channel_id=1, source_target_pairs={{0,2},{1,3},{2,0},{3,1},{4,6},{5,7},{6,4},{7,5},{8,10},{9,11},{10,... | collective-permute-start | bytes 393224 | tf_op jit(solution)/shard_map/ppermute | solution.py:522
  132.0 1.6 collective-permute-done.20.m2_ref
  133.6 4.0 %collective-permute-done.21.m3_ref = bf16[128,512]{1,0:T(8,128)(2,1)S(1)} collective-permute-done((bf16[128,512]{1,0:T(8,128)(2,1)S(1)}, bf16[128,512]{1,0:T(8,128)(2,1)S(1)}, u32[]{:S(2)}, u32[]{:S(2)}) %collective-permute-start.21) | collective-permute-done | bytes 131104 | tf_op jit(solution)/shard_map/ppermute | solution.py:522
  138.8 2.1 %shard_map.211 = (f32[128,256]{1,0:T(8,128)S(1)}, bf16[512,256]{1,0:T(8,128)(2,1)}) custom-call(s32[6]{0:T(128)S(1)} %dynamic_slice.3.q_ref, bf16[128,512]{1,0:T(8,128)(2,1)S(1)} %shard_map.210.m0_ref, bf16[128,512]{1,0:T(8,128)(2,1)S(1)} %collective-permute-done.19.m1_ref, bf16[128,512]{1,0:T(8,128)(2,1)S(1)} %collective-permute-done.20.m2_ref, ...), custom_call_target="tpu_custom_call" | custom-call | flops 200000000 | bytes 2162688 | tf_op jit(solution)/shard_map/pallas_call | solution.py:57
  140.9 5.1 %all-to-all-start.3 = ((bf16[64,8,256]{2,1,0:T(8,128)(2,1)}), bf16[64,8,256]{2,1,0:T(8,128)(2,1)S(1)}, u32[]{:S(2)}, u32[]{:S(2)}) async-start(bf16[64,8,256]{2,1,0:T(8,128)(2,1)} %bitcast.17), calls=%async_computation.3 | async-start | bytes 524288 | tf_op jit(solution)/shard_map/all_to_all | solution.py:413
  146.7 3.2 %collective-permute-start.23 = (bf16[512,128]{1,0:T(8,128)(2,1)S(1)}, bf16[512,128]{1,0:T(8,128)(2,1)S(1)}, u32[]{:S(2)}, u32[]{:S(2)}) collective-permute-start(bf16[512,128]{1,0:T(8,128)(2,1)S(1)} %get-tuple-element.100), channel_id=1, source_target_pairs={{0,16},{4,20},{8,24},{12,28},{16,0},{20,4},{24,8},{28,12},{32,48},... | collective-permute-start | bytes 393224 | tf_op jit(solution)/shard_map/ppermute | solution.py:536
  150.5 2.7 %collective-permute-start.25 = (bf16[512,128]{1,0:T(8,128)(2,1)S(1)}, bf16[512,128]{1,0:T(8,128)(2,1)S(1)}, u32[]{:S(2)}, u32[]{:S(2)}) collective-permute-start(bf16[512,128]{1,0:T(8,128)(2,1)S(1)} %get-tuple-element.102), channel_id=1, source_target_pairs={{0,24},{4,28},{8,0},{12,4},{16,8},{20,12},{24,16},{28,20},{32,56},... | collective-permute-start | bytes 393224 | tf_op jit(solution)/shard_map/ppermute | solution.py:536
  153.1 5.7 %all-to-all-done.3 = bf16[64,8,256]{2,1,0:T(8,128)(2,1)S(1)} async-done(((bf16[64,8,256]{2,1,0:T(8,128)(2,1)}), bf16[64,8,256]{2,1,0:T(8,128)(2,1)S(1)}, u32[]{:S(2)}, u32[]{:S(2)}) %all-to-all-start.3) | async-done | bytes 262176 | tf_op jit(solution)/shard_map/all_to_all | solution.py:413
  159.1 1.7 shard_map.215
  160.8 8.6 %all-to-all-start.4 = ((bf16[64,8,256]{2,1,0:T(8,128)(2,1)}), bf16[64,8,256]{2,1,0:T(8,128)(2,1)S(1)}, u32[]{:S(2)}, u32[]{:S(2)}) async-start(bf16[64,8,256]{2,1,0:T(8,128)(2,1)} %bitcast.19), calls=%async_computation.4 | async-start | bytes 524288 | tf_op jit(solution)/shard_map/all_to_all | solution.py:413
  170.8 11.5 %all-to-all-done.4 = bf16[64,8,256]{2,1,0:T(8,128)(2,1)S(1)} async-done(((bf16[64,8,256]{2,1,0:T(8,128)(2,1)}), bf16[64,8,256]{2,1,0:T(8,128)(2,1)S(1)}, u32[]{:S(2)}, u32[]{:S(2)}) %all-to-all-start.4) | async-done | bytes 262176 | tf_op jit(solution)/shard_map/all_to_all | solution.py:413
  182.3 1.9 %shard_map.216 = (bf16[128,128]{1,0:T(8,128)(2,1)}, bf16[128,128]{1,0:T(8,128)(2,1)}, bf16[128,256]{1,0:T(8,128)(2,1)}, f32[128,128]{1,0:T(8,128)}, f32[32,256]{1,0:T(8,128)}) custom-call(s32[6]{0:T(128)S(1)} %dynamic_slice.3.q_ref, bf16[128,128]{1,0:T(8,128)(2,1)S(1)} %copy-done.15, bf16[128,256]{1,0:T(8,128)(2,1)S(1)} %copy-done.14, ...), custom_call_target="tpu_custom_call" | custom-call | flops 300000000 | bytes 1114112 | tf_op jit(solution)/shard_map/pallas_call | solution.py:57
  (90 shorter events, 37.7 us)
Async XLA Ops:
  2.9 1.6 collective-permute-start
  5.9 29.6 %all-to-all-start = ((bf16[32,16,512]{2,1,0:T(8,128)(2,1)}), bf16[32,16,512]{2,1,0:T(8,128)(2,1)S(1)}, u32[]{:S(2)}, u32[]{:S(2)}) async-start(bf16[32,16,512]{2,1,0:T(8,128)(2,1)} %bitcast.1), calls=%async_computation | async-start | bytes 1048576 | tf_op jit(solution)/shard_map/all_to_all | solution.py:425
  21.1 1.5 collective-permute-start.1
  22.7 48.9 %copy-start = (bf16[1,2048,256]{2,1,0:T(8,128)(2,1)S(1)}, bf16[1,2048,256]{2,1,0:T(8,128)(2,1)}, u32[]{:S(2)}) copy-start(bf16[1,2048,256]{2,1,0:T(8,128)(2,1)} %param.18) | copy-start | bytes 3145732
  22.7 48.9 %copy-start.1 = (bf16[1,2048,256]{2,1,0:T(8,128)(2,1)S(1)}, bf16[1,2048,256]{2,1,0:T(8,128)(2,1)}, u32[]{:S(2)}) copy-start(bf16[1,2048,256]{2,1,0:T(8,128)(2,1)} %param.19) | copy-start | bytes 3145732
  35.5 21.6 %all-to-all-start.1 = ((bf16[32,16,512]{2,1,0:T(8,128)(2,1)}), bf16[32,16,512]{2,1,0:T(8,128)(2,1)S(1)}, u32[]{:S(2)}, u32[]{:S(2)}) async-start(bf16[32,16,512]{2,1,0:T(8,128)(2,1)} %bitcast.4), calls=%async_computation.1 | async-start | bytes 1048576 | tf_op jit(solution)/shard_map/all_to_all | solution.py:425
  40.1 12.6 %collective-permute-start.8 = (bf16[512,512]{1,0:T(8,128)(2,1)S(1)}, bf16[512,512]{1,0:T(8,128)(2,1)S(1)}, u32[]{:S(2)}, u32[]{:S(2)}) collective-permute-start(bf16[512,512]{1,0:T(8,128)(2,1)S(1)} %bitcast.38), channel_id=1, source_target_pairs={{0,1},{1,2},{2,3},{3,0},{4,5},{5,6},{6,7},{7,4},{8,9},{9,10},{10,1... | collective-permute-start | bytes 1572872 | tf_op jit(solution)/shard_map/ppermute | solution.py:460
  41.7 17.6 %collective-permute-start.9 = (bf16[512,512]{1,0:T(8,128)(2,1)S(1)}, bf16[512,512]{1,0:T(8,128)(2,1)}, u32[]{:S(2)}, u32[]{:S(2)}) collective-permute-start(bf16[512,512]{1,0:T(8,128)(2,1)S(1)} %bitcast.39), channel_id=1, source_target_pairs={{0,3},{1,0},{2,1},{3,2},{4,7},{5,4},{6,5},{7,6},{8,11},{9,8},{10,9... | collective-permute-start | bytes 1572872 | tf_op jit(solution)/shard_map/ppermute | solution.py:461
  53.6 9.4 %collective-permute-start.10 = (bf16[256,512]{1,0:T(8,128)(2,1)}, bf16[256,512]{1,0:T(8,128)(2,1)S(1)}, u32[]{:S(2)}, u32[]{:S(2)}) collective-permute-start(bf16[256,512]{1,0:T(8,128)(2,1)} %slice.30), channel_id=1, source_target_pairs={{0,1},{1,2},{2,3},{3,0},{4,5},{5,6},{6,7},{7,4},{8,9},{9,10},{10,1... | collective-permute-start | bytes 786440 | tf_op jit(solution)/shard_map/ppermute | solution.py:462
  57.2 11.5 %collective-permute-start.2 = (bf16[256,512]{1,0:T(8,128)(2,1)S(1)}, bf16[256,512]{1,0:T(8,128)(2,1)S(1)}, u32[]{:S(2)}, u32[]{:S(2)}) collective-permute-start(bf16[256,512]{1,0:T(8,128)(2,1)S(1)} %bitcast.44), channel_id=1, source_target_pairs={{0,1},{1,2},{2,3},{3,0},{4,5},{5,6},{6,7},{7,4},{8,9},{9,10},{10,1... | collective-permute-start | bytes 786440 | tf_op jit(solution)/shard_map/ppermute | solution.py:466
  58.7 11.4 %collective-permute-start.5 = (bf16[256,512]{1,0:T(8,128)(2,1)S(1)}, bf16[256,512]{1,0:T(8,128)(2,1)S(1)}, u32[]{:S(2)}, u32[]{:S(2)}) collective-permute-start(bf16[256,512]{1,0:T(8,128)(2,1)S(1)} %bitcast.46), channel_id=1, source_target_pairs={{0,3},{1,0},{2,1},{3,2},{4,7},{5,4},{6,5},{7,6},{8,11},{9,8},{10,9... | collective-permute-start | bytes 786440 | tf_op jit(solution)/shard_map/ppermute | solution.py:467
  60.2 15.0 %collective-permute-start.11 = (bf16[256,512]{1,0:T(8,128)(2,1)S(1)}, bf16[256,512]{1,0:T(8,128)(2,1)S(1)}, u32[]{:S(2)}, u32[]{:S(2)}) collective-permute-start(bf16[256,512]{1,0:T(8,128)(2,1)S(1)} %slice.31), channel_id=1, source_target_pairs={{0,3},{1,0},{2,1},{3,2},{4,7},{5,4},{6,5},{7,6},{8,11},{9,8},{10,9... | collective-permute-start | bytes 786440 | tf_op jit(solution)/shard_map/ppermute | solution.py:463
  62.1 14.2 %collective-permute-start.3 = (bf16[256,512]{1,0:T(8,128)(2,1)S(1)}, bf16[256,512]{1,0:T(8,128)(2,1)S(1)}, u32[]{:S(2)}, u32[]{:S(2)}) collective-permute-start(bf16[256,512]{1,0:T(8,128)(2,1)S(1)} %bitcast.47), channel_id=1, source_target_pairs={{0,1},{1,2},{2,3},{3,0},{4,5},{5,6},{6,7},{7,4},{8,9},{9,10},{10,1... | collective-permute-start | bytes 786440 | tf_op jit(solution)/shard_map/ppermute | solution.py:468
  63.0 14.6 %collective-permute-start.4 = (bf16[256,512]{1,0:T(8,128)(2,1)S(1)}, bf16[256,512]{1,0:T(8,128)(2,1)S(1)}, u32[]{:S(2)}, u32[]{:S(2)}) collective-permute-start(bf16[256,512]{1,0:T(8,128)(2,1)S(1)} %bitcast.45), channel_id=1, source_target_pairs={{0,3},{1,0},{2,1},{3,2},{4,7},{5,4},{6,5},{7,6},{8,11},{9,8},{10,9... | collective-permute-start | bytes 786440 | tf_op jit(solution)/shard_map/ppermute | solution.py:469
  68.6 10.2 %collective-permute-start.6 = (bf16[256,512]{1,0:T(8,128)(2,1)S(1)}, bf16[256,512]{1,0:T(8,128)(2,1)S(1)}, u32[]{:S(2)}, u32[]{:S(2)}) collective-permute-start(bf16[256,512]{1,0:T(8,128)(2,1)S(1)} %collective-permute-done.2.t1_ref), channel_id=1, source_target_pairs={{0,1},{1,2},{2,3},{3,0},{4,5},{5,6},{6,7},{7,4},{8,9},{9,10},{10,1... | collective-permute-start | bytes 786440 | tf_op jit(solution)/shard_map/ppermute | solution.py:470
  70.1 10.3 %collective-permute-start.7 = (bf16[256,512]{1,0:T(8,128)(2,1)S(1)}, bf16[256,512]{1,0:T(8,128)(2,1)S(1)}, u32[]{:S(2)}, u32[]{:S(2)}) collective-permute-start(bf16[256,512]{1,0:T(8,128)(2,1)S(1)} %collective-permute-done.5.b2_ref), channel_id=1, source_target_pairs={{0,3},{1,0},{2,1},{3,2},{4,7},{5,4},{6,5},{7,6},{8,11},{9,8},{10,9... | collective-permute-start | bytes 786440 | tf_op jit(solution)/shard_map/ppermute | solution.py:471
  81.7 9.3 %collective-permute-start.12 = (bf16[256,512]{1,0:T(8,128)(2,1)S(1)}, bf16[256,512]{1,0:T(8,128)(2,1)S(1)}, u32[]{:S(2)}, u32[]{:S(2)}) collective-permute-start(bf16[256,512]{1,0:T(8,128)(2,1)S(1)} %get-tuple-element.70), channel_id=1, source_target_pairs={{0,1},{1,2},{2,3},{3,0},{4,5},{5,6},{6,7},{7,4},{8,9},{9,10},{10,1... | collective-permute-start | bytes 786440 | tf_op jit(solution)/shard_map/ppermute | solution.py:488
  83.0 8.0 %collective-permute-start.13 = (bf16[256,512]{1,0:T(8,128)(2,1)S(1)}, bf16[256,512]{1,0:T(8,128)(2,1)S(1)}, u32[]{:S(2)}, u32[]{:S(2)}) collective-permute-start(bf16[256,512]{1,0:T(8,128)(2,1)S(1)} %get-tuple-element.86), channel_id=1, source_target_pairs={{0,3},{1,0},{2,1},{3,2},{4,7},{5,4},{6,5},{7,6},{8,11},{9,8},{10,9... | collective-permute-start | bytes 786440 | tf_op jit(solution)/shard_map/ppermute | solution.py:489
  85.1 13.5 %collective-permute-start.15 = (bf16[256,512]{1,0:T(8,128)(2,1)S(1)}, bf16[256,512]{1,0:T(8,128)(2,1)S(1)}, u32[]{:S(2)}, u32[]{:S(2)}) collective-permute-start(bf16[256,512]{1,0:T(8,128)(2,1)S(1)} %get-tuple-element.88), channel_id=1, source_target_pairs={{0,3},{1,0},{2,1},{3,2},{4,7},{5,4},{6,5},{7,6},{8,11},{9,8},{10,9... | collective-permute-start | bytes 786440 | tf_op jit(solution)/shard_map/ppermute | solution.py:492
  86.9 11.7 %collective-permute-start.16 = (bf16[256,512]{1,0:T(8,128)(2,1)S(1)}, bf16[256,512]{1,0:T(8,128)(2,1)S(1)}, u32[]{:S(2)}, u32[]{:S(2)}) collective-permute-start(bf16[256,512]{1,0:T(8,128)(2,1)S(1)} %get-tuple-element.89), channel_id=1, source_target_pairs={{0,1},{1,2},{2,3},{3,0},{4,5},{5,6},{6,7},{7,4},{8,9},{9,10},{10,1... | collective-permute-start | bytes 786440 | tf_op jit(solution)/shard_map/ppermute | solution.py:491
  91.6 7.0 %collective-permute-start.14 = (bf16[256,512]{1,0:T(8,128)(2,1)S(1)}, bf16[256,512]{1,0:T(8,128)(2,1)S(1)}, u32[]{:S(2)}, u32[]{:S(2)}) collective-permute-start(bf16[256,512]{1,0:T(8,128)(2,1)S(1)} %get-tuple-element.87), channel_id=1, source_target_pairs={{0,1},{1,2},{2,3},{3,0},{4,5},{5,6},{6,7},{7,4},{8,9},{9,10},{10,1... | collective-permute-start | bytes 786440 | tf_op jit(solution)/shard_map/ppermute | solution.py:501
  92.3 6.9 %collective-permute-start.17 = (bf16[256,512]{1,0:T(8,128)(2,1)S(1)}, bf16[256,512]{1,0:T(8,128)(2,1)S(1)}, u32[]{:S(2)}, u32[]{:S(2)}) collective-permute-start(bf16[256,512]{1,0:T(8,128)(2,1)S(1)} %get-tuple-element.90), channel_id=1, source_target_pairs={{0,3},{1,0},{2,1},{3,2},{4,7},{5,4},{6,5},{7,6},{8,11},{9,8},{10,9... | collective-permute-start | bytes 786440 | tf_op jit(solution)/shard_map/ppermute | solution.py:502
  122.7 1.6 collective-permute-start.18
  125.2 6.9 %collective-permute-start.19 = (bf16[128,512]{1,0:T(8,128)(2,1)S(1)}, bf16[128,512]{1,0:T(8,128)(2,1)S(1)}, u32[]{:S(2)}, u32[]{:S(2)}) collective-permute-start(bf16[128,512]{1,0:T(8,128)(2,1)S(1)} %shard_map.210.m0_ref), channel_id=1, source_target_pairs={{0,1},{1,2},{2,3},{3,0},{4,5},{5,6},{6,7},{7,4},{8,9},{9,10},{10,1... | collective-permute-start | bytes 393224 | tf_op jit(solution)/shard_map/ppermute | solution.py:523
  127.0 6.6 %collective-permute-start.20 = (bf16[128,512]{1,0:T(8,128)(2,1)S(1)}, bf16[128,512]{1,0:T(8,128)(2,1)S(1)}, u32[]{:S(2)}, u32[]{:S(2)}) collective-permute-start(bf16[128,512]{1,0:T(8,128)(2,1)S(1)} %shard_map.210.m0_ref), channel_id=1, source_target_pairs={{0,3},{1,0},{2,1},{3,2},{4,7},{5,4},{6,5},{7,6},{8,11},{9,8},{10,9... | collective-permute-start | bytes 393224 | tf_op jit(solution)/shard_map/ppermute | solution.py:524
  128.3 9.3 %collective-permute-start.21 = (bf16[128,512]{1,0:T(8,128)(2,1)S(1)}, bf16[128,512]{1,0:T(8,128)(2,1)S(1)}, u32[]{:S(2)}, u32[]{:S(2)}) collective-permute-start(bf16[128,512]{1,0:T(8,128)(2,1)S(1)} %shard_map.210.m0_ref), channel_id=1, source_target_pairs={{0,2},{1,3},{2,0},{3,1},{4,6},{5,7},{6,4},{7,5},{8,10},{9,11},{10,... | collective-permute-start | bytes 393224 | tf_op jit(solution)/shard_map/ppermute | solution.py:522
  138.6 7.3 %collective-permute-start.22 = (bf16[1024,256]{1,0:T(8,128)(2,1)S(1)}, bf16[1024,256]{1,0:T(8,128)(2,1)S(1)}, u32[]{:S(2)}, u32[]{:S(2)}) collective-permute-start(bf16[1024,256]{1,0:T(8,128)(2,1)S(1)} %get-tuple-element.98), channel_id=1, source_target_pairs={{0,4},{4,0},{8,12},{12,8},{16,20},{20,16},{24,28},{28,24},{32,36},... | collective-permute-start | bytes 1572872 | tf_op jit(solution)/shard_map/ppermute | solution.py:534
  140.9 18.0 %all-to-all-start.3 = ((bf16[64,8,256]{2,1,0:T(8,128)(2,1)}), bf16[64,8,256]{2,1,0:T(8,128)(2,1)S(1)}, u32[]{:S(2)}, u32[]{:S(2)}) async-start(bf16[64,8,256]{2,1,0:T(8,128)(2,1)} %bitcast.17), calls=%async_computation.3 | async-start | bytes 524288 | tf_op jit(solution)/shard_map/all_to_all | solution.py:413
  146.7 12.1 %collective-permute-start.23 = (bf16[512,128]{1,0:T(8,128)(2,1)S(1)}, bf16[512,128]{1,0:T(8,128)(2,1)S(1)}, u32[]{:S(2)}, u32[]{:S(2)}) collective-permute-start(bf16[512,128]{1,0:T(8,128)(2,1)S(1)} %get-tuple-element.100), channel_id=1, source_target_pairs={{0,16},{4,20},{8,24},{12,28},{16,0},{20,4},{24,8},{28,12},{32,48},... | collective-permute-start | bytes 393224 | tf_op jit(solution)/shard_map/ppermute | solution.py:536
  149.9 9.2 %collective-permute-start.24 = (bf16[512,128]{1,0:T(8,128)(2,1)S(1)}, bf16[512,128]{1,0:T(8,128)(2,1)S(1)}, u32[]{:S(2)}, u32[]{:S(2)}) collective-permute-start(bf16[512,128]{1,0:T(8,128)(2,1)S(1)} %get-tuple-element.101), channel_id=1, source_target_pairs={{0,8},{4,12},{8,16},{12,20},{16,24},{20,28},{24,0},{28,4},{32,40},... | collective-permute-start | bytes 393224 | tf_op jit(solution)/shard_map/ppermute | solution.py:536
  150.5 8.6 %collective-permute-start.25 = (bf16[512,128]{1,0:T(8,128)(2,1)S(1)}, bf16[512,128]{1,0:T(8,128)(2,1)S(1)}, u32[]{:S(2)}, u32[]{:S(2)}) collective-permute-start(bf16[512,128]{1,0:T(8,128)(2,1)S(1)} %get-tuple-element.102), channel_id=1, source_target_pairs={{0,24},{4,28},{8,0},{12,4},{16,8},{20,12},{24,16},{28,20},{32,56},... | collective-permute-start | bytes 393224 | tf_op jit(solution)/shard_map/ppermute | solution.py:536
  160.8 21.5 %all-to-all-start.4 = ((bf16[64,8,256]{2,1,0:T(8,128)(2,1)}), bf16[64,8,256]{2,1,0:T(8,128)(2,1)S(1)}, u32[]{:S(2)}, u32[]{:S(2)}) async-start(bf16[64,8,256]{2,1,0:T(8,128)(2,1)} %bitcast.19), calls=%async_computation.4 | async-start | bytes 524288 | tf_op jit(solution)/shard_map/all_to_all | solution.py:413
  (16 other events, 316.2 us)

commit v5 on v4

--- a/solution.py
+++ b/solution.py
@@ -41,10 +41,6 @@
     return x.astype(BF).astype(F32)
 
 
-def lower_lanes(shape):
-    return iota(shape, len(shape) - 1) < HALF
-
-
 def call(kernel, out_shape, args, *, index, in_specs=None, flops=0, vmem=24, scratch=()):
     nbytes = sum(a.size * a.dtype.itemsize for a in args)
     nbytes += sum(o.size * o.dtype.itemsize for o in jax.tree.leaves(out_shape))
@@ -88,37 +84,22 @@
     return dot(lower, g, 1, 0, HI)
 
 
-def tiles_of(state, fill=None):
-    out = []
-    for b in range(4):
-        t = state[:, LANES * (b // 2) : LANES * (b // 2 + 1)]
-        r = pltpu.roll(t, HALF, 1)
-        low, up = (t, r) if b % 2 == 0 else (r, t)
-        upper = fill if fill is not None else up - rounded(up)
-        tile = jnp.where(lower_lanes(t.shape), rounded(low), upper)
-        out.append(tile.reshape(16, 8, LANES))
-    return jnp.concatenate(out, axis=1).reshape(SLOTS, LANES)
-
-
-def state_of(tiles, upper):
-    other = pltpu.roll(tiles, HALF, 1)
-    even, odd = (other, tiles) if upper else (tiles, other)
-    even, odd = even.reshape(16, 32, LANES), odd.reshape(16, 32, LANES)
-    low = lower_lanes((DK, LANES))
-    halves = []
-    for b in (0, 2):
-        first = even[:, 8 * b : 8 * b + 8, :].reshape(DK, LANES)
-        second = odd[:, 8 * b + 8 : 8 * b + 16, :].reshape(DK, LANES)
-        halves.append(jnp.where(low, first, second))
-    return jnp.concatenate(halves, axis=1)
-
-
-def pick_kernel(ids_ref, x_ref, keep_ref, give_ref, pick_ref, slot_ref, own_ref, sem):
+def dot_rounded(a, b, ca, cb):
+    high = a.astype(BF)
+    return dot(high, b, ca, cb) + dot((a - high.astype(F32)).astype(BF), b, ca, cb)
+
+
+def pick_kernel(
+    ids_hbm, x_ref, keep_ref, give_ref, pick_ref, slot_ref, ids_ref, own_ref, ids_sem, sem
+):
+    ids_copy = pltpu.make_async_copy(ids_hbm, ids_ref, ids_sem)
+    ids_copy.start()
     start = pl.multiple_of(lax.axis_index("tp") * QUART, QUART)
     copy = pltpu.make_async_copy(x_ref.at[:, pl.ds(start, QUART)], own_ref, sem)
     copy.start()
     core = lax.rem(lax.axis_index("sp"), 2)
     expert = iota((EXPERTS, TOK), 0)
+    ids_copy.wait()
     id0, id1 = ids_ref[0:1, :], ids_ref[1:2, :]
     hit0, hit1 = expert == id0, expert == id1
     named = (hit0.astype(F32) + hit1.astype(F32)).astype(BF)
@@ -171,8 +152,8 @@
     state = dot(to_end.T, v_ref[...].astype(F32), 1, 0, HI)
     factor = jnp.exp(jnp.sum(g.T, axis=1, keepdims=True))
     high = rounded(factor)
-    fill = jnp.where(iota((DK, LANES), 1) < 96, high, factor - high)
-    tile_ref[...] = tiles_of(state, fill).astype(BF)
+    tile_ref[:, :DV] = state.astype(BF)
+    tile_ref[:, DV:] = jnp.where(iota((DK, LANES), 1) < HALF, high, factor - high).astype(BF)
 
 
 def gate_near_kernel(q_ref, x0_ref, x1_ref, x2_ref, wg_ref, wu_ref, g_ref, u_ref):
@@ -287,60 +268,93 @@
         part = dot(ref[...], w_ref[quarter_rows(q_ref[n]), :], 1, 0)
         head = part if head is None else head + part
     h_ref[...] = head
-    pay_ref[:, :LANES] = tiles_of(dot(dec_ref[...].T, head, 1, 0, HI)).astype(BF)
-    pay_ref[:, LANES:] = tile_ref[...]
+    pay_ref[:, :DV] = dot(dec_ref[...].T, head, 1, 0, HI).astype(BF)
+    pay_ref[:, DV:] = tile_ref[...]
 
 
 def out_proj_kernel(q_ref, m0_ref, m1_ref, m2_ref, m3_ref, mixed_ref, keep_ref, give_ref):
     mixed = mixed_ref[...]
     first = q_ref[4] == 0
     for n, ref in enumerate((m0_ref, m1_ref, m2_ref, m3_ref)):
-        part = dot(ref[...].T, mixed, 1, 0).reshape(16, 32, DV)
-        low = part[:, :16, :].reshape(256, DV)
-        high = part[:, 16:, :].reshape(256, DV)
+        part = dot(ref[...].T, mixed, 1, 0).reshape(8, 64, DV)
+        low = part[:, :32, :].reshape(256, DV)
+        high = part[:, 32:, :].reshape(256, DV)
         rows = pl.ds(pl.multiple_of(q_ref[n] * 256, 256), 256)
         keep_ref[rows, :] = jnp.where(first, low, high).astype(BF)
         give_ref[rows, :] = jnp.where(first, high, low).astype(BF)
 
 
 def split_kernel(q_ref, keep_ref, got_ref, o0_ref, o1_ref, o2_ref, o3_ref):
-    total = (keep_ref[...].astype(F32) + got_ref[...].astype(F32)).reshape(64, 16, DV)
-    tile = [
-        total[:, 8 * (n // 2) : 8 * (n // 2) + 8, LANES * (n % 2) : LANES * (n % 2) + LANES]
-        for n in range(4)
-    ]
-    tile = [t.reshape(SLOTS, LANES) for t in tile]
+    total = (keep_ref[...].astype(F32) + got_ref[...].astype(F32)).reshape(8, 128, DV)
+    slab = []
+    for n in range(4):
+        block = total[:, 32 * n : 32 * n + 32, :]
+        wide = jnp.concatenate([block[:, :16, :], block[:, 16:, :]], axis=2)
+        slab.append(wide.reshape(TOK, 2 * DV))
     y = q_ref[5]
     for k, ref in enumerate((o0_ref, o1_ref, o2_ref, o3_ref)):
-        out = tile[k]
+        out = slab[k]
         for n in range(1, 4):
-            out = jnp.where(y == n, tile[(n + k) % 4], out)
+            out = jnp.where(y == n, slab[(n + k) % 4], out)
         ref[...] = out.astype(BF)
 
 
-def scan_kernel(
-    q_ref, in_ref, o_ref, r1_ref, r2_ref, r3_ref, out_ref, factor_ref, pre_ref, suf_ref
-):
-    pull = in_ref[:, :LANES].astype(F32)
-    suf_ref[...] = pull + pltpu.roll(pull, HALF, 1)
-    tile = in_ref[:, LANES:].astype(F32)
-    pre_ref[...] = pltpu.roll(tile, HALF, 1)
-    factor_ref[...] = jnp.broadcast_to(tile[:, 64:65] + tile[:, 96:97], tile.shape)
-    before = after = jnp.zeros((8, LANES), F32)
-    for s in range(EXPERTS):
-        rows = slice(8 * s, 8 * s + 8)
-        now = pre_ref[rows, :]
-        pre_ref[rows, :] = before
-        before = before * factor_ref[rows, :] + now
-        e = EXPERTS - 1 - s
-        rows = slice(8 * e, 8 * e + 8)
-        now = suf_ref[rows, :]
-        suf_ref[rows, :] = after
-        after = after * factor_ref[rows, :] + now
-    suf = suf_ref[...]
-    out_ref[:, :LANES] = jnp.where(lower_lanes(suf.shape), suf, pre_ref[...]).astype(BF)
+def block_of(n):
+    return slice(16 * n, 16 * n + 16)
+
+
+def factor_of(ref, lane):
+    high, low = ref[:, lane : lane + 1], ref[:, lane + HALF : lane + HALF + 1]
+    return jnp.broadcast_to(high.astype(F32) + low.astype(F32), (DK, DV))
+
+
+def plane_kernel(
+    q_ref, in_ref, o_ref, r1_ref, r2_ref, r3_ref, pay_ref, suf_ref, pre_ref, factor_ref
+):
+    factor_ref[...] = factor_of(in_ref, 2 * DV)
+    suf = pre = jnp.zeros((16, DV), F32)
+    whole = jnp.ones((16, DV), F32)
+    for n in range(8):
+        rows = block_of(n)
+        pre_ref[rows, :] = pre
+        pre = pre * factor_ref[rows, :] + in_ref[rows, DV : 2 * DV].astype(F32)
+        whole = whole * factor_ref[rows, :]
+        rows = block_of(7 - n)
+        suf_ref[rows, :] = suf
+        suf = suf * factor_ref[rows, :] + in_ref[rows, :DV].astype(F32)
+    part = whole[:, :LANES]
+    high = rounded(part)
+    part = jnp.where(iota(part.shape, 1) < HALF, high, part - high)
+    block = jnp.concatenate([suf, pre, part], axis=1)
+    pay_ref[:, : 2 * DV + LANES] = jnp.concatenate([block] * 8, axis=0).astype(BF)
     total = o_ref[...].astype(F32) + r1_ref[...].astype(F32)
-    out_ref[:, LANES:] = (total + r2_ref[...].astype(F32) + r3_ref[...].astype(F32)).astype(BF)
+    total = total + r2_ref[...].astype(F32) + r3_ref[...].astype(F32)
+    pay_ref[:, 2 * DV + LANES :] = total.astype(BF)
+
+
+def line_kernel(
+    q_ref, in_ref, suf_ref, pre_ref, factor_ref, pay_ref, go_ref, totals_ref
+):
+    totals_ref[...] = factor_of(in_ref, 2 * DV)
+    z = q_ref[6]
+    suf = pre = jnp.zeros((16, DV), F32)
+    for n in range(8):
+        rows = block_of(n)
+        step = pre * totals_ref[rows, :] + in_ref[rows, DV : 2 * DV].astype(F32)
+        pre = jnp.where(n < z, step, pre)
+        rows = block_of(7 - n)
+        step = suf * totals_ref[rows, :] + in_ref[rows, :DV].astype(F32)
+        suf = jnp.where(7 - n > z, step, suf)
+    for n in range(8):
+        rows = block_of(n)
+        pay_ref[rows, DV:] = (pre_ref[rows, :] + pre).astype(BF)
+        pre = pre * factor_ref[rows, :]
+        rows = block_of(7 - n)
+        pay_ref[rows, :DV] = (suf_ref[rows, :] + suf).astype(BF)
+        suf = suf * factor_ref[rows, :]
+    total = jnp.sum(in_ref[:, 2 * DV + LANES :].astype(F32).reshape(8, 16, 2 * DV), axis=0)
+    go_ref[:16, :] = total[:, :DV]
+    go_ref[16:, :] = total[:, DV:]
 
 
 def inside_kernel(
@@ -358,33 +372,25 @@
 
 def last_kernel(
     q_ref, k_ref, v_ref, cum_ref, dec_ref, h_ref, dq_ref, dk_ref, dv_ref, in_ref,
-    gq_ref, gk_ref, gv_ref, gg_ref, go_ref,
-):
-    tiles = in_ref[:, :LANES].astype(F32)
-    cot, state = state_of(tiles, False), state_of(tiles, True)
-    k, v, head, cum = k_ref[...].astype(F32), v_ref[...].astype(F32), h_ref[...], cum_ref[...]
+    gq_ref, gk_ref, gv_ref, gg_ref,
+):
+    cot, state = in_ref[:, :DV], in_ref[:, DV:]
+    k, cum = k_ref[...].astype(F32), cum_ref[...]
     last = cum[TOK - 1 : TOK, :]
     shrink, to_end = jnp.exp(-cum), jnp.exp(last - cum)
     k_end = k * to_end
-    d_q = dq_ref[...] + dot(head, state, 1, 1, HI)
+    d_q = dq_ref[...] + dot_rounded(h_ref[...], state, 1, 1)
     d_kg = dk_ref[...]
-    d_ke = dot(v, cot, 1, 1, HI)
+    d_ke = dot(v_ref[...], cot, 1, 1)
     gq_ref[...] = (d_q * jnp.exp(cum)).astype(BF)
     gk_ref[...] = (d_kg * shrink + d_ke * to_end).astype(BF)
-    gv_ref[...] = (dv_ref[...] + dot(k_end, cot, 1, 0, HI)).astype(BF)
+    gv_ref[...] = (dv_ref[...] + dot_rounded(k_end, cot, 1, 0)).astype(BF)
     end = d_ke * k_end
     d_cum = d_q * dec_ref[...] - d_kg * (k * shrink) - end
-    carried = jnp.sum((state * cot).T, axis=0, keepdims=True)
+    carried = jnp.sum((state.astype(F32) * cot.astype(F32)).T, axis=0, keepdims=True)
     d_last = jnp.sum(end, axis=0, keepdims=True) + jnp.exp(last) * carried
     upper = (iota((TOK, TOK), 0) <= iota((TOK, TOK), 1)).astype(F32)
     gg_ref[...] = dot(upper, d_cum, 1, 0, HI) + d_last
-    parts = jnp.sum(in_ref[:, LANES:].astype(F32).reshape(8, EXPERTS, LANES), axis=0)
-    for y in range(4):
-        for core in range(2):
-            n = 8 * (2 * y + core)
-            rows = 16 * core + 8 * (y // 2)
-            lanes = LANES * (y % 2)
-            go_ref[rows : rows + 8, lanes : lanes + LANES] = parts[n : n + 8, :]
 
 
 def per_device(
@@ -393,10 +399,12 @@
 ):
     me, sp = lax.axis_index("tp"), lax.axis_index("sp")
     table = [
-        [i, (i + 3) % 4, (i + 1) % 4, (i + 2) % 4, s % 2, s // 2] for s in range(8) for i in range(4)
+        [i, (i + 3) % 4, (i + 1) % 4, (i + 2) % 4, s % 2, s // 2 % 4, s // 8]
+        for s in range(64)
+        for i in range(4)
     ]
-    place = lax.rem(sp, 8) * 4 + me
-    order = lax.dynamic_slice(jnp.array(table, jnp.int32).reshape(-1), (place * 6,), (6,))
+    place = (sp * 4 + me) * 7
+    order = lax.dynamic_slice(jnp.array(table, jnp.int32).reshape(-1), (place,), (7,))
     to_right = [(i, (i + 1) % 4) for i in range(4)]
     to_left = [(i, (i + 3) % 4) for i in range(4)]
     across = [(i, (i + 2) % 4) for i in range(4)]
@@ -408,16 +416,21 @@
     wg, wu, wd = w_gate[0], w_up[0], w_down[0]
     run = functools.partial(call, index=order)
 
-    def exchange(rows):
+    def exchange(rows, groups):
         width = rows.shape[1]
-        got = lax.all_to_all(rows.reshape(EXPERTS, CAP, width), "sp", 0, 0, tiled=True)
-        return got.reshape(SLOTS, width)
+        got = lax.all_to_all(
+            rows.reshape(8, 16, width), "sp", 0, 0, tiled=True, axis_index_groups=groups
+        )
+        return got.reshape(DK, width)
+
+    in_plane = [[8 * z + n for n in range(8)] for z in range(8)]
+    along_z = [[8 * z + n for z in range(8)] for n in range(8)]
 
     def quarter_block():
         return pl.BlockSpec((TOK, QUART), lambda i, q: (0, q[0]))
 
     rows_type = sds((SLOTS, QUART), BF)
-    tile_type = sds((SLOTS, LANES), BF)
+    tile_type = sds((TOK, 2 * DV), BF)
     side_type = sds((SIDE, QUART), BF)
 
     def between_chips(rows):
@@ -430,22 +443,27 @@
     x_keep, x_give, pick, slots = pl.pallas_call(
         pick_kernel,
         out_shape=(side_type, side_type, sds((SLOTS, TOK), BF), sds((2, TOK), jnp.int32)),
-        in_specs=[
-            pl.BlockSpec(memory_space=pltpu.VMEM),
-            pl.BlockSpec(memory_space=pltpu.HBM),
+        in_specs=[pl.BlockSpec(memory_space=pltpu.HBM)] * 2,
+        out_specs=(pl.BlockSpec(memory_space=pltpu.VMEM),) * 4,
+        scratch_shapes=[
+            pltpu.VMEM((2, TOK), jnp.int32),
+            pltpu.VMEM((TOK, QUART), BF),
+            pltpu.SemaphoreType.DMA,
+            pltpu.SemaphoreType.DMA,
         ],
-        out_specs=(pl.BlockSpec(memory_space=pltpu.VMEM),) * 4,
-        scratch_shapes=[pltpu.VMEM((TOK, QUART), BF), pltpu.SemaphoreType.DMA],
         compiler_params=pltpu.CompilerParams(vmem_limit_bytes=24 * 2**20),
         cost_estimate=pl.CostEstimate(
             flops=10**8, bytes_accessed=2 * 10**6, transcendentals=0
         ),
-    )(in_hbm(route_ids.T), expert_in)
+    )(in_hbm(route_ids.T), in_hbm(expert_in))
     x_got = lax.ppermute(x_give, "sp", other_core)
     x_rows = run(weave_kernel, rows_type, (x_keep, x_got), flops=1e6)
     y_keep, y_give, state_tile, cum, q_dec = run(
         local_kernel,
-        (side_type, side_type, tile_type, sds((TOK, DK), F32), sds((TOK, DK), F32)),
+        (
+            side_type, side_type, sds((DK, DV + LANES), BF), sds((TOK, DK), F32),
+            sds((TOK, DK), F32),
+        ),
         (
             slots, in_hbm(route_weights.T), pick, in_hbm(out_cot), in_hbm(queries), in_hbm(keys),
             in_hbm(values), in_hbm(log_decay),
@@ -525,37 +543,44 @@
     mids = (mid, m_left, m_right, m_far)
     head, pay = run(
         head_kernel,
-        (sds((TOK, DV), F32), sds((SLOTS, 2 * LANES), BF)),
+        (sds((TOK, DV), F32), sds((DK, 2 * DV + LANES), BF)),
         (*mids, w_out, q_dec, state_tile),
         flops=2e8,
     )
-    pulled = exchange(pay)
+    pulled = exchange(pay, in_plane)
     keep, give = run(out_proj_kernel, (sds((1024, DV), BF),) * 2, (*mids, mixed_heads), flops=1.4e8)
     got = lax.ppermute(give, "sp", other_core)
     tiles = run(split_kernel, (tile_type,) * 4, (keep, got), flops=1e6)
     adds = [lax.ppermute(tiles[k], "sp", along_y(k)) for k in (2, 1, 3)]
-    pay = run(
-        scan_kernel,
-        sds((SLOTS, 2 * LANES), BF),
+    state_type = sds((DK, DV), F32)
+    pay, suf, pre, factor = run(
+        plane_kernel,
+        (sds((DK, 4 * DV + LANES), BF), state_type, state_type, state_type),
         (pulled, tiles[0], *adds),
-        flops=1e8,
-        scratch=[pltpu.VMEM((SLOTS, LANES), F32)] * 3,
-    )
-    back_states = exchange(pay)
+        flops=1e7,
+    )
+    totals = exchange(pay, along_z)
+    pay, grad_out_proj = run(
+        line_kernel,
+        (sds((DK, 2 * DV), BF), sds((32, DV), F32)),
+        (totals, suf, pre, factor),
+        flops=1e7,
+        scratch=[pltpu.VMEM((DK, DV), F32)],
+    )
+    back_states = exchange(pay, in_plane)
     d_in = run(
         inside_kernel,
         (sds((TOK, DK), F32), sds((TOK, DK), F32), sds((TOK, DV), F32)),
         (keys, values, cum, q_dec, head),
         flops=3e8,
     )
-    grad_queries, grad_keys, grad_values, grad_decay, grad_out_proj = run(
+    grad_queries, grad_keys, grad_values, grad_decay = run(
         last_kernel,
         (
             sds((TOK, DK), BF),
             sds((TOK, DK), BF),
             sds((TOK, DV), BF),
             sds((TOK, DK), F32),
-            sds((32, DV), F32),
         ),
         (keys, values, cum, q_dec, head, *d_in, back_states),
         flops=3e8,

time: 187 us -> 186 us (level)
  blocking collectives: 22.6 us -> 37.9 us
  waiting for transfers between devices: 59.1 us -> 50.7 us
  starting transfers between devices: 62.8 us -> 56.6 us
    all_to_all x0 -> x1, blocking collectives: none -> 15.3 us  [exchange(): lax.all_to_all(rows.reshape(8, 16, width), 'sp', 0, 0, tiled=True, axis_i...]
    all_to_all x2, waiting for transfers between devices: 17.1 us -> 4.61 us  [exchange(): lax.all_to_all(rows.reshape(8, 16, width), 'sp', 0, 0, tiled=True, axis_i...]
    all_to_all x2, starting transfers between devices: 13.7 us -> 6.95 us  [exchange(): lax.all_to_all(rows.reshape(8, 16, width), 'sp', 0, 0, tiled=True, axis_i...]
    ppermute x3, waiting for transfers between devices: 0.28 us -> 4.41 us  [per_device(): adds = [lax.ppermute(tiles[k], 'sp', along_y(k)) for k in (2, 1, 3)]]
    pallas_call x19 -> x20, Pallas kernels: 31.4 us -> 31.3 us  [call(): pl.pallas_call(kernel, out_shape=out_shape, grid_spec=pltpu.PrefetchScala...]
where the time goes in v5:
time: 186 us; the launch traced here: 184 us
  starting transfers between devices  56.6 us (30%)
  waiting for transfers between devices  50.7 us (27%)
  blocking collectives  37.9 us (20%)
  Pallas kernels  32.5 us (17%)
  local copies, waits for them, and re-layouts  5.04 us (3%)
    pallas_call x20, Pallas kernels, call(): pl.pallas_call(kernel, out_shape=out_shape, grid_spec=pltpu.PrefetchScala...  31.3 us
    all_to_all x1, blocking collectives, between_chips(): lax.all_to_all(rows.reshape(CHIPS, 2 * CAP, QUART), 'sp', 0, 0, tiled=Tru...  22.6 us
    all_to_all x2, starting transfers between devices, between_chips(): lax.all_to_all(rows.reshape(CHIPS, 2 * CAP, QUART), 'sp', 0, 0, tiled=Tru...  16.1 us
    all_to_all x1, blocking collectives, exchange(): lax.all_to_all(rows.reshape(8, 16, width), 'sp', 0, 0, tiled=True, axis_i...  15.3 us
    all_to_all x2, waiting for transfers between devices, between_chips(): lax.all_to_all(rows.reshape(CHIPS, 2 * CAP, QUART), 'sp', 0, 0, tiled=Tru...  13.5 us
    ppermute x1, waiting for transfers between devices, per_device(): x1 = lax.ppermute(x0, 'tp', to_right)  10.5 us
    all_to_all x2, starting transfers between devices, exchange(): lax.all_to_all(rows.reshape(8, 16, width), 'sp', 0, 0, tiled=True, axis_i...  6.95 us
    ppermute x3, starting transfers between devices, per_device(): adds = [lax.ppermute(tiles[k], 'sp', along_y(k)) for k in (2, 1, 3)]  6.84 us
  transfers between devices with their start and end apart: 30, of which 18 were waited for; matrix products, arithmetic and copies ran while one was open for 1% of the time, Pallas kernels for 12%

profile of v5, /device:TPU:2, one launch (start us, length us, event | category | flops | bytes accessed | tf_op | source)
XLA Modules:
  0.0 183.7 jit_solution(2371530918043233216)
XLA Ops:
  4.9 11.5 %all-to-all-start = ((bf16[32,16,512]{2,1,0:T(8,128)(2,1)}), bf16[32,16,512]{2,1,0:T(8,128)(2,1)S(1)}, u32[]{:S(2)}, u32[]{:S(2)}) async-start(bf16[32,16,512]{2,1,0:T(8,128)(2,1)} %bitcast.1), calls=%async_computation | async-start | bytes 1048576 | tf_op jit(solution)/shard_map/all_to_all | solution.py:438
  16.4 2.4 %shard_map.199 = (bf16[256,512]{1,0:T(8,128)(2,1)S(1)}, bf16[256,512]{1,0:T(8,128)(2,1)S(1)}, bf16[128,384]{1,0:T(8,128)(2,1)S(1)}, f32[128,128]{1,0:T(8,128)S(1)}, f32[128,128]{1,0:T(8,128)S(1)}) custom-call(s32[7]{0:T(128)S(1)} %dynamic_slice.3.q_ref, s32[2,128]{1,0:T(2,128)S(1)} %get-tuple-element.65.slot_ref, f32[2,128]{1,0:T(2,128)} %bitcast.54, ...), custom_call_target="tpu_custom_call" | custom-call | flops 300000000 | bytes 1607680 | tf_op jit(solution)/shard_map/pallas_call | solution.py:53
  20.0 1.5 collective-permute-done.1.got_ref
  22.9 11.5 %all-to-all-done = bf16[32,16,512]{2,1,0:T(8,128)(2,1)S(1)} async-done(((bf16[32,16,512]{2,1,0:T(8,128)(2,1)}), bf16[32,16,512]{2,1,0:T(8,128)(2,1)S(1)}, u32[]{:S(2)}, u32[]{:S(2)}) %all-to-all-start) | async-done | bytes 524320 | tf_op jit(solution)/shard_map/all_to_all | solution.py:438
  34.5 4.6 %all-to-all-start.1 = ((bf16[32,16,512]{2,1,0:T(8,128)(2,1)}), bf16[32,16,512]{2,1,0:T(8,128)(2,1)S(1)}, u32[]{:S(2)}, u32[]{:S(2)}) async-start(bf16[32,16,512]{2,1,0:T(8,128)(2,1)} %bitcast.4), calls=%async_computation.1 | async-start | bytes 1048576 | tf_op jit(solution)/shard_map/all_to_all | solution.py:438
  39.1 1.6 collective-permute-start.8
  41.2 10.5 %collective-permute-done.8.x1_ref = bf16[512,512]{1,0:T(8,128)(2,1)S(1)} collective-permute-done((bf16[512,512]{1,0:T(8,128)(2,1)S(1)}, bf16[512,512]{1,0:T(8,128)(2,1)S(1)}, u32[]{:S(2)}, u32[]{:S(2)}) %collective-permute-start.8) | collective-permute-done | bytes 524320 | tf_op jit(solution)/shard_map/ppermute | solution.py:478
  54.1 2.0 %all-to-all-done.1 = bf16[32,16,512]{2,1,0:T(8,128)(2,1)S(1)} async-done(((bf16[32,16,512]{2,1,0:T(8,128)(2,1)}), bf16[32,16,512]{2,1,0:T(8,128)(2,1)S(1)}, u32[]{:S(2)}, u32[]{:S(2)}) %all-to-all-start.1) | async-done | bytes 524320 | tf_op jit(solution)/shard_map/all_to_all | solution.py:438
  56.1 1.6 collective-permute-start.2
  59.2 1.8 collective-permute-start.11
  61.9 3.0 %collective-permute-start.4 = (bf16[256,512]{1,0:T(8,128)(2,1)S(1)}, bf16[256,512]{1,0:T(8,128)(2,1)S(1)}, u32[]{:S(2)}, u32[]{:S(2)}) collective-permute-start(bf16[256,512]{1,0:T(8,128)(2,1)S(1)} %bitcast.49), channel_id=1, source_target_pairs={{0,3},{1,0},{2,1},{3,2},{4,7},{5,4},{6,5},{7,6},{8,11},{9,8},{10,9... | collective-permute-start | bytes 786440 | tf_op jit(solution)/shard_map/ppermute | solution.py:487
  64.9 2.7 %collective-permute-done.2.t1_ref = bf16[256,512]{1,0:T(8,128)(2,1)S(1)} collective-permute-done((bf16[256,512]{1,0:T(8,128)(2,1)S(1)}, bf16[256,512]{1,0:T(8,128)(2,1)S(1)}, u32[]{:S(2)}, u32[]{:S(2)}) %collective-permute-start.2) | collective-permute-done | bytes 262176 | tf_op jit(solution)/shard_map/ppermute | solution.py:484
  71.6 2.6 %shard_map.202 = (f32[512,256]{1,0:T(8,128)S(1)}, f32[512,256]{1,0:T(8,128)S(1)}) custom-call(s32[7]{0:T(128)S(1)} %dynamic_slice.3.q_ref, bf16[512,512]{1,0:T(8,128)(2,1)S(1)} %bitcast.42, bf16[512,512]{1,0:T(8,128)(2,1)S(1)} %copy-done.4, bf16[512,512]{1,0:T(8,128)(2,1)} %collective-permute-done.9.x2_ref, bf16[2048,256]{1,0:T(8,128)(2,1)S(1)} %bitcast.24, ...), custom_call_target="tpu_custom_call" | custom-call | flops 800000000 | bytes 4718592 | tf_op jit(solution)/shard_map/pallas_call | solution.py:53
  77.8 1.6 collective-permute-done.7.b3_ref
  84.1 1.8 collective-permute-start.15
  86.2 2.9 %shard_map.205 = (f32[256,2048]{1,0:T(8,128)}, bf16[512,512]{1,0:T(8,128)(2,1)S(1)}) custom-call(s32[7]{0:T(128)S(1)} %dynamic_slice.3.q_ref, bf16[512,512]{1,0:T(8,128)(2,1)S(1)} %bitcast.35, bf16[256,512]{1,0:T(8,128)(2,1)S(1)} %collective-permute-done.2.t1_ref, bf16[256,512]{1,0:T(8,128)(2,1)S(1)} %collective-permute-done.3.b1_ref, ...), custom_call_target="tpu_custom_call" | custom-call | flops 800000000 | bytes 7602176 | tf_op jit(solution)/shard_map/pallas_call | solution.py:53
  92.7 4.9 %shard_map.206 = (f32[2048,256]{1,0:T(8,128)}, f32[2048,256]{1,0:T(8,128)}) custom-call(s32[7]{0:T(128)S(1)} %dynamic_slice.3.q_ref, bf16[512,512]{1,0:T(8,128)(2,1)S(1)} %bitcast.43, bf16[512,512]{1,0:T(8,128)(2,1)S(1)} %copy-done.5, bf16[512,512]{1,0:T(8,128)(2,1)} %collective-permute-done.9.x2_ref, ...), custom_call_target="tpu_custom_call" | custom-call | flops 1100000000 | bytes 6815744 | tf_op jit(solution)/shard_map/pallas_call | solution.py:53
  99.0 22.6 %all_to_all.30 = bf16[32,16,512]{2,1,0:T(8,128)(2,1)S(1)} all-to-all(bf16[32,16,512]{2,1,0:T(8,128)(2,1)S(1)} %bitcast.39), channel_id=1, replica_groups={{0,8,16,24,32,40,48,56,64,72,80,88,96,104,112,120,128,136,144,152,160,1..., dimensions={0} | all-to-all | bytes 1048576 | tf_op jit(solution)/shard_map/all_to_all | solution.py:438
  124.1 1.9 %collective-permute-start.19 = (bf16[128,512]{1,0:T(8,128)(2,1)S(1)}, bf16[128,512]{1,0:T(8,128)(2,1)S(1)}, u32[]{:S(2)}, u32[]{:S(2)}) collective-permute-start(bf16[128,512]{1,0:T(8,128)(2,1)S(1)} %shard_map.210.m0_ref), channel_id=1, source_target_pairs={{0,1},{1,2},{2,3},{3,0},{4,5},{5,6},{6,7},{7,4},{8,9},{9,10},{10,1... | collective-permute-start | bytes 393224 | tf_op jit(solution)/shard_map/ppermute | solution.py:541
  127.3 3.2 %collective-permute-start.21 = (bf16[128,512]{1,0:T(8,128)(2,1)S(1)}, bf16[128,512]{1,0:T(8,128)(2,1)S(1)}, u32[]{:S(2)}, u32[]{:S(2)}) collective-permute-start(bf16[128,512]{1,0:T(8,128)(2,1)S(1)} %shard_map.210.m0_ref), channel_id=1, source_target_pairs={{0,2},{1,3},{2,0},{3,1},{4,6},{5,7},{6,4},{7,5},{8,10},{9,11},{10,... | collective-permute-start | bytes 393224 | tf_op jit(solution)/shard_map/ppermute | solution.py:540
  131.0 1.6 collective-permute-done.20.m2_ref
  132.5 4.0 %collective-permute-done.21.m3_ref = bf16[128,512]{1,0:T(8,128)(2,1)S(1)} collective-permute-done((bf16[128,512]{1,0:T(8,128)(2,1)S(1)}, bf16[128,512]{1,0:T(8,128)(2,1)S(1)}, u32[]{:S(2)}, u32[]{:S(2)}) %collective-permute-start.21) | collective-permute-done | bytes 131104 | tf_op jit(solution)/shard_map/ppermute | solution.py:540
  137.7 1.9 %shard_map.211 = (f32[128,256]{1,0:T(8,128)S(1)}, bf16[128,640]{1,0:T(8,128)(2,1)}) custom-call(s32[7]{0:T(128)S(1)} %dynamic_slice.3.q_ref, bf16[128,512]{1,0:T(8,128)(2,1)S(1)} %shard_map.210.m0_ref, bf16[128,512]{1,0:T(8,128)(2,1)S(1)} %collective-permute-done.19.m1_ref, bf16[128,512]{1,0:T(8,128)(2,1)S(1)} %collective-permute-done.20.m2_ref, ...), custom_call_target="tpu_custom_call" | custom-call | flops 200000000 | bytes 2031616 | tf_op jit(solution)/shard_map/pallas_call | solution.py:53
  139.6 3.6 %all-to-all-start.3 = ((bf16[8,16,640]{2,1,0:T(8,128)(2,1)}), bf16[8,16,640]{2,1,0:T(8,128)(2,1)S(1)}, u32[]{:S(2)}, u32[]{:S(2)}) async-start(bf16[8,16,640]{2,1,0:T(8,128)(2,1)} %bitcast.17), calls=%async_computation.3 | async-start | bytes 327680 | tf_op jit(solution)/shard_map/all_to_all | solution.py:421
  144.0 3.6 %collective-permute-start.23 = (bf16[128,512]{1,0:T(8,128)(2,1)S(1)}, bf16[128,512]{1,0:T(8,128)(2,1)S(1)}, u32[]{:S(2)}, u32[]{:S(2)}) collective-permute-start(bf16[128,512]{1,0:T(8,128)(2,1)S(1)} %get-tuple-element.100), channel_id=1, source_target_pairs={{0,16},{4,20},{8,24},{12,28},{16,0},{20,4},{24,8},{28,12},{32,48},... | collective-permute-start | bytes 393224 | tf_op jit(solution)/shard_map/ppermute | solution.py:554
  148.2 2.7 %collective-permute-start.25 = (bf16[128,512]{1,0:T(8,128)(2,1)S(1)}, bf16[128,512]{1,0:T(8,128)(2,1)S(1)}, u32[]{:S(2)}, u32[]{:S(2)}) collective-permute-start(bf16[128,512]{1,0:T(8,128)(2,1)S(1)} %get-tuple-element.102), channel_id=1, source_target_pairs={{0,24},{4,28},{8,0},{12,4},{16,8},{20,12},{24,16},{28,20},{32,56},... | collective-permute-start | bytes 393224 | tf_op jit(solution)/shard_map/ppermute | solution.py:554
  150.9 2.2 %collective-permute-done.23.r1_ref = bf16[128,512]{1,0:T(8,128)(2,1)S(1)} collective-permute-done((bf16[128,512]{1,0:T(8,128)(2,1)S(1)}, bf16[128,512]{1,0:T(8,128)(2,1)S(1)}, u32[]{:S(2)}, u32[]{:S(2)}) %collective-permute-start.23) | collective-permute-done | bytes 131104 | tf_op jit(solution)/shard_map/ppermute | solution.py:554
  153.0 2.2 %collective-permute-done.24.r2_ref = bf16[128,512]{1,0:T(8,128)(2,1)S(1)} collective-permute-done((bf16[128,512]{1,0:T(8,128)(2,1)S(1)}, bf16[128,512]{1,0:T(8,128)(2,1)S(1)}, u32[]{:S(2)}, u32[]{:S(2)}) %collective-permute-start.24) | collective-permute-done | bytes 131104 | tf_op jit(solution)/shard_map/ppermute | solution.py:554
  156.0 15.3 %all_to_all.31 = bf16[8,16,1152]{2,1,0:T(8,128)(2,1)S(1)} all-to-all(bf16[8,16,1152]{2,1,0:T(8,128)(2,1)S(1)} %bitcast.46), channel_id=1, replica_groups={{0,32,64,96,128,160,192,224},{4,36,68,100,132,164,196,228},{8,40,72,104..., dimensions={0} | all-to-all | bytes 589824 | tf_op jit(solution)/shard_map/all_to_all | solution.py:421
  172.7 3.4 %all-to-all-start.5 = ((bf16[8,16,512]{2,1,0:T(8,128)(2,1)}), bf16[8,16,512]{2,1,0:T(8,128)(2,1)S(1)}, u32[]{:S(2)}, u32[]{:S(2)}) async-start(bf16[8,16,512]{2,1,0:T(8,128)(2,1)} %bitcast.21), calls=%async_computation.5 | async-start | bytes 262144 | tf_op jit(solution)/shard_map/all_to_all | solution.py:421
  177.5 4.6 %all-to-all-done.5 = bf16[8,16,512]{2,1,0:T(8,128)(2,1)S(1)} async-done(((bf16[8,16,512]{2,1,0:T(8,128)(2,1)}), bf16[8,16,512]{2,1,0:T(8,128)(2,1)S(1)}, u32[]{:S(2)}, u32[]{:S(2)}) %all-to-all-start.5) | async-done | bytes 131104 | tf_op jit(solution)/shard_map/all_to_all | solution.py:421
  182.1 1.6 shard_map.217
  (90 shorter events, 40.0 us)
Async XLA Ops:
  1.9 1.6 collective-permute-start
  4.9 29.6 %all-to-all-start = ((bf16[32,16,512]{2,1,0:T(8,128)(2,1)}), bf16[32,16,512]{2,1,0:T(8,128)(2,1)S(1)}, u32[]{:S(2)}, u32[]{:S(2)}) async-start(bf16[32,16,512]{2,1,0:T(8,128)(2,1)} %bitcast.1), calls=%async_computation | async-start | bytes 1048576 | tf_op jit(solution)/shard_map/all_to_all | solution.py:438
  20.0 1.5 collective-permute-start.1
  21.5 49.0 %copy-start = (bf16[1,2048,256]{2,1,0:T(8,128)(2,1)S(1)}, bf16[1,2048,256]{2,1,0:T(8,128)(2,1)}, u32[]{:S(2)}) copy-start(bf16[1,2048,256]{2,1,0:T(8,128)(2,1)} %param.18) | copy-start | bytes 3145732
  21.5 49.0 %copy-start.1 = (bf16[1,2048,256]{2,1,0:T(8,128)(2,1)S(1)}, bf16[1,2048,256]{2,1,0:T(8,128)(2,1)}, u32[]{:S(2)}) copy-start(bf16[1,2048,256]{2,1,0:T(8,128)(2,1)} %param.19) | copy-start | bytes 3145732
  34.5 21.6 %all-to-all-start.1 = ((bf16[32,16,512]{2,1,0:T(8,128)(2,1)}), bf16[32,16,512]{2,1,0:T(8,128)(2,1)S(1)}, u32[]{:S(2)}, u32[]{:S(2)}) async-start(bf16[32,16,512]{2,1,0:T(8,128)(2,1)} %bitcast.4), calls=%async_computation.1 | async-start | bytes 1048576 | tf_op jit(solution)/shard_map/all_to_all | solution.py:438
  39.1 12.6 %collective-permute-start.8 = (bf16[512,512]{1,0:T(8,128)(2,1)S(1)}, bf16[512,512]{1,0:T(8,128)(2,1)S(1)}, u32[]{:S(2)}, u32[]{:S(2)}) collective-permute-start(bf16[512,512]{1,0:T(8,128)(2,1)S(1)} %bitcast.40), channel_id=1, source_target_pairs={{0,1},{1,2},{2,3},{3,0},{4,5},{5,6},{6,7},{7,4},{8,9},{9,10},{10,1... | collective-permute-start | bytes 1572872 | tf_op jit(solution)/shard_map/ppermute | solution.py:478
  40.6 17.6 %collective-permute-start.9 = (bf16[512,512]{1,0:T(8,128)(2,1)S(1)}, bf16[512,512]{1,0:T(8,128)(2,1)}, u32[]{:S(2)}, u32[]{:S(2)}) collective-permute-start(bf16[512,512]{1,0:T(8,128)(2,1)S(1)} %bitcast.41), channel_id=1, source_target_pairs={{0,3},{1,0},{2,1},{3,2},{4,7},{5,4},{6,5},{7,6},{8,11},{9,8},{10,9... | collective-permute-start | bytes 1572872 | tf_op jit(solution)/shard_map/ppermute | solution.py:479
  52.6 9.4 %collective-permute-start.10 = (bf16[256,512]{1,0:T(8,128)(2,1)}, bf16[256,512]{1,0:T(8,128)(2,1)S(1)}, u32[]{:S(2)}, u32[]{:S(2)}) collective-permute-start(bf16[256,512]{1,0:T(8,128)(2,1)} %slice.30), channel_id=1, source_target_pairs={{0,1},{1,2},{2,3},{3,0},{4,5},{5,6},{6,7},{7,4},{8,9},{9,10},{10,1... | collective-permute-start | bytes 786440 | tf_op jit(solution)/shard_map/ppermute | solution.py:480
  56.1 11.5 %collective-permute-start.2 = (bf16[256,512]{1,0:T(8,128)(2,1)S(1)}, bf16[256,512]{1,0:T(8,128)(2,1)S(1)}, u32[]{:S(2)}, u32[]{:S(2)}) collective-permute-start(bf16[256,512]{1,0:T(8,128)(2,1)S(1)} %bitcast.48), channel_id=1, source_target_pairs={{0,1},{1,2},{2,3},{3,0},{4,5},{5,6},{6,7},{7,4},{8,9},{9,10},{10,1... | collective-permute-start | bytes 786440 | tf_op jit(solution)/shard_map/ppermute | solution.py:484
  57.7 11.4 %collective-permute-start.5 = (bf16[256,512]{1,0:T(8,128)(2,1)S(1)}, bf16[256,512]{1,0:T(8,128)(2,1)S(1)}, u32[]{:S(2)}, u32[]{:S(2)}) collective-permute-start(bf16[256,512]{1,0:T(8,128)(2,1)S(1)} %bitcast.50), channel_id=1, source_target_pairs={{0,3},{1,0},{2,1},{3,2},{4,7},{5,4},{6,5},{7,6},{8,11},{9,8},{10,9... | collective-permute-start | bytes 786440 | tf_op jit(solution)/shard_map/ppermute | solution.py:485
  59.2 15.0 %collective-permute-start.11 = (bf16[256,512]{1,0:T(8,128)(2,1)S(1)}, bf16[256,512]{1,0:T(8,128)(2,1)S(1)}, u32[]{:S(2)}, u32[]{:S(2)}) collective-permute-start(bf16[256,512]{1,0:T(8,128)(2,1)S(1)} %slice.31), channel_id=1, source_target_pairs={{0,3},{1,0},{2,1},{3,2},{4,7},{5,4},{6,5},{7,6},{8,11},{9,8},{10,9... | collective-permute-start | bytes 786440 | tf_op jit(solution)/shard_map/ppermute | solution.py:481
  61.0 14.2 %collective-permute-start.3 = (bf16[256,512]{1,0:T(8,128)(2,1)S(1)}, bf16[256,512]{1,0:T(8,128)(2,1)S(1)}, u32[]{:S(2)}, u32[]{:S(2)}) collective-permute-start(bf16[256,512]{1,0:T(8,128)(2,1)S(1)} %bitcast.51), channel_id=1, source_target_pairs={{0,1},{1,2},{2,3},{3,0},{4,5},{5,6},{6,7},{7,4},{8,9},{9,10},{10,1... | collective-permute-start | bytes 786440 | tf_op jit(solution)/shard_map/ppermute | solution.py:486
  61.9 14.7 %collective-permute-start.4 = (bf16[256,512]{1,0:T(8,128)(2,1)S(1)}, bf16[256,512]{1,0:T(8,128)(2,1)S(1)}, u32[]{:S(2)}, u32[]{:S(2)}) collective-permute-start(bf16[256,512]{1,0:T(8,128)(2,1)S(1)} %bitcast.49), channel_id=1, source_target_pairs={{0,3},{1,0},{2,1},{3,2},{4,7},{5,4},{6,5},{7,6},{8,11},{9,8},{10,9... | collective-permute-start | bytes 786440 | tf_op jit(solution)/shard_map/ppermute | solution.py:487
  67.6 10.2 %collective-permute-start.6 = (bf16[256,512]{1,0:T(8,128)(2,1)S(1)}, bf16[256,512]{1,0:T(8,128)(2,1)S(1)}, u32[]{:S(2)}, u32[]{:S(2)}) collective-permute-start(bf16[256,512]{1,0:T(8,128)(2,1)S(1)} %collective-permute-done.2.t1_ref), channel_id=1, source_target_pairs={{0,1},{1,2},{2,3},{3,0},{4,5},{5,6},{6,7},{7,4},{8,9},{9,10},{10,1... | collective-permute-start | bytes 786440 | tf_op jit(solution)/shard_map/ppermute | solution.py:488
  69.1 10.3 %collective-permute-start.7 = (bf16[256,512]{1,0:T(8,128)(2,1)S(1)}, bf16[256,512]{1,0:T(8,128)(2,1)S(1)}, u32[]{:S(2)}, u32[]{:S(2)}) collective-permute-start(bf16[256,512]{1,0:T(8,128)(2,1)S(1)} %collective-permute-done.5.b2_ref), channel_id=1, source_target_pairs={{0,3},{1,0},{2,1},{3,2},{4,7},{5,4},{6,5},{7,6},{8,11},{9,8},{10,9... | collective-permute-start | bytes 786440 | tf_op jit(solution)/shard_map/ppermute | solution.py:489
  80.7 9.3 %collective-permute-start.12 = (bf16[256,512]{1,0:T(8,128)(2,1)S(1)}, bf16[256,512]{1,0:T(8,128)(2,1)S(1)}, u32[]{:S(2)}, u32[]{:S(2)}) collective-permute-start(bf16[256,512]{1,0:T(8,128)(2,1)S(1)} %get-tuple-element.75), channel_id=1, source_target_pairs={{0,1},{1,2},{2,3},{3,0},{4,5},{5,6},{6,7},{7,4},{8,9},{9,10},{10,1... | collective-permute-start | bytes 786440 | tf_op jit(solution)/shard_map/ppermute | solution.py:506
  81.9 8.0 %collective-permute-start.13 = (bf16[256,512]{1,0:T(8,128)(2,1)S(1)}, bf16[256,512]{1,0:T(8,128)(2,1)S(1)}, u32[]{:S(2)}, u32[]{:S(2)}) collective-permute-start(bf16[256,512]{1,0:T(8,128)(2,1)S(1)} %get-tuple-element.89), channel_id=1, source_target_pairs={{0,3},{1,0},{2,1},{3,2},{4,7},{5,4},{6,5},{7,6},{8,11},{9,8},{10,9... | collective-permute-start | bytes 786440 | tf_op jit(solution)/shard_map/ppermute | solution.py:507
  84.1 13.5 %collective-permute-start.15 = (bf16[256,512]{1,0:T(8,128)(2,1)S(1)}, bf16[256,512]{1,0:T(8,128)(2,1)S(1)}, u32[]{:S(2)}, u32[]{:S(2)}) collective-permute-start(bf16[256,512]{1,0:T(8,128)(2,1)S(1)} %get-tuple-element.91), channel_id=1, source_target_pairs={{0,3},{1,0},{2,1},{3,2},{4,7},{5,4},{6,5},{7,6},{8,11},{9,8},{10,9... | collective-permute-start | bytes 786440 | tf_op jit(solution)/shard_map/ppermute | solution.py:510
  85.9 11.7 %collective-permute-start.16 = (bf16[256,512]{1,0:T(8,128)(2,1)S(1)}, bf16[256,512]{1,0:T(8,128)(2,1)S(1)}, u32[]{:S(2)}, u32[]{:S(2)}) collective-permute-start(bf16[256,512]{1,0:T(8,128)(2,1)S(1)} %get-tuple-element.92), channel_id=1, source_target_pairs={{0,1},{1,2},{2,3},{3,0},{4,5},{5,6},{6,7},{7,4},{8,9},{9,10},{10,1... | collective-permute-start | bytes 786440 | tf_op jit(solution)/shard_map/ppermute | solution.py:509
  90.6 7.0 %collective-permute-start.14 = (bf16[256,512]{1,0:T(8,128)(2,1)S(1)}, bf16[256,512]{1,0:T(8,128)(2,1)S(1)}, u32[]{:S(2)}, u32[]{:S(2)}) collective-permute-start(bf16[256,512]{1,0:T(8,128)(2,1)S(1)} %get-tuple-element.90), channel_id=1, source_target_pairs={{0,1},{1,2},{2,3},{3,0},{4,5},{5,6},{6,7},{7,4},{8,9},{9,10},{10,1... | collective-permute-start | bytes 786440 | tf_op jit(solution)/shard_map/ppermute | solution.py:519
  91.3 6.9 %collective-permute-start.17 = (bf16[256,512]{1,0:T(8,128)(2,1)S(1)}, bf16[256,512]{1,0:T(8,128)(2,1)S(1)}, u32[]{:S(2)}, u32[]{:S(2)}) collective-permute-start(bf16[256,512]{1,0:T(8,128)(2,1)S(1)} %get-tuple-element.93), channel_id=1, source_target_pairs={{0,3},{1,0},{2,1},{3,2},{4,7},{5,4},{6,5},{7,6},{8,11},{9,8},{10,9... | collective-permute-start | bytes 786440 | tf_op jit(solution)/shard_map/ppermute | solution.py:520
  121.7 1.6 collective-permute-start.18
  124.1 6.9 %collective-permute-start.19 = (bf16[128,512]{1,0:T(8,128)(2,1)S(1)}, bf16[128,512]{1,0:T(8,128)(2,1)S(1)}, u32[]{:S(2)}, u32[]{:S(2)}) collective-permute-start(bf16[128,512]{1,0:T(8,128)(2,1)S(1)} %shard_map.210.m0_ref), channel_id=1, source_target_pairs={{0,1},{1,2},{2,3},{3,0},{4,5},{5,6},{6,7},{7,4},{8,9},{9,10},{10,1... | collective-permute-start | bytes 393224 | tf_op jit(solution)/shard_map/ppermute | solution.py:541
  126.0 6.6 %collective-permute-start.20 = (bf16[128,512]{1,0:T(8,128)(2,1)S(1)}, bf16[128,512]{1,0:T(8,128)(2,1)S(1)}, u32[]{:S(2)}, u32[]{:S(2)}) collective-permute-start(bf16[128,512]{1,0:T(8,128)(2,1)S(1)} %shard_map.210.m0_ref), channel_id=1, source_target_pairs={{0,3},{1,0},{2,1},{3,2},{4,7},{5,4},{6,5},{7,6},{8,11},{9,8},{10,9... | collective-permute-start | bytes 393224 | tf_op jit(solution)/shard_map/ppermute | solution.py:542
  127.3 9.3 %collective-permute-start.21 = (bf16[128,512]{1,0:T(8,128)(2,1)S(1)}, bf16[128,512]{1,0:T(8,128)(2,1)S(1)}, u32[]{:S(2)}, u32[]{:S(2)}) collective-permute-start(bf16[128,512]{1,0:T(8,128)(2,1)S(1)} %shard_map.210.m0_ref), channel_id=1, source_target_pairs={{0,2},{1,3},{2,0},{3,1},{4,6},{5,7},{6,4},{7,5},{8,10},{9,11},{10,... | collective-permute-start | bytes 393224 | tf_op jit(solution)/shard_map/ppermute | solution.py:540
  137.6 5.6 %collective-permute-start.22 = (bf16[1024,256]{1,0:T(8,128)(2,1)S(1)}, bf16[1024,256]{1,0:T(8,128)(2,1)S(1)}, u32[]{:S(2)}, u32[]{:S(2)}) collective-permute-start(bf16[1024,256]{1,0:T(8,128)(2,1)S(1)} %get-tuple-element.98), channel_id=1, source_target_pairs={{0,4},{4,0},{8,12},{12,8},{16,20},{20,16},{24,28},{28,24},{32,36},... | collective-permute-start | bytes 1572872 | tf_op jit(solution)/shard_map/ppermute | solution.py:552
  139.6 11.2 %all-to-all-start.3 = ((bf16[8,16,640]{2,1,0:T(8,128)(2,1)}), bf16[8,16,640]{2,1,0:T(8,128)(2,1)S(1)}, u32[]{:S(2)}, u32[]{:S(2)}) async-start(bf16[8,16,640]{2,1,0:T(8,128)(2,1)} %bitcast.17), calls=%async_computation.3 | async-start | bytes 327680 | tf_op jit(solution)/shard_map/all_to_all | solution.py:421
  144.0 9.0 %collective-permute-start.23 = (bf16[128,512]{1,0:T(8,128)(2,1)S(1)}, bf16[128,512]{1,0:T(8,128)(2,1)S(1)}, u32[]{:S(2)}, u32[]{:S(2)}) collective-permute-start(bf16[128,512]{1,0:T(8,128)(2,1)S(1)} %get-tuple-element.100), channel_id=1, source_target_pairs={{0,16},{4,20},{8,24},{12,28},{16,0},{20,4},{24,8},{28,12},{32,48},... | collective-permute-start | bytes 393224 | tf_op jit(solution)/shard_map/ppermute | solution.py:554
  147.6 7.7 %collective-permute-start.24 = (bf16[128,512]{1,0:T(8,128)(2,1)S(1)}, bf16[128,512]{1,0:T(8,128)(2,1)S(1)}, u32[]{:S(2)}, u32[]{:S(2)}) collective-permute-start(bf16[128,512]{1,0:T(8,128)(2,1)S(1)} %get-tuple-element.101), channel_id=1, source_target_pairs={{0,8},{4,12},{8,16},{12,20},{16,24},{20,28},{24,0},{28,4},{32,40},... | collective-permute-start | bytes 393224 | tf_op jit(solution)/shard_map/ppermute | solution.py:554
  148.2 7.1 %collective-permute-start.25 = (bf16[128,512]{1,0:T(8,128)(2,1)S(1)}, bf16[128,512]{1,0:T(8,128)(2,1)S(1)}, u32[]{:S(2)}, u32[]{:S(2)}) collective-permute-start(bf16[128,512]{1,0:T(8,128)(2,1)S(1)} %get-tuple-element.102), channel_id=1, source_target_pairs={{0,24},{4,28},{8,0},{12,4},{16,8},{20,12},{24,16},{28,20},{32,56},... | collective-permute-start | bytes 393224 | tf_op jit(solution)/shard_map/ppermute | solution.py:554
  172.7 9.4 %all-to-all-start.5 = ((bf16[8,16,512]{2,1,0:T(8,128)(2,1)}), bf16[8,16,512]{2,1,0:T(8,128)(2,1)S(1)}, u32[]{:S(2)}, u32[]{:S(2)}) async-start(bf16[8,16,512]{2,1,0:T(8,128)(2,1)} %bitcast.21), calls=%async_computation.5 | async-start | bytes 262144 | tf_op jit(solution)/shard_map/all_to_all | solution.py:421
  (15 other events, 332.6 us)

commit v6 on v5

--- a/solution.py
+++ b/solution.py
@@ -156,24 +156,20 @@
     tile_ref[:, DV:] = jnp.where(iota((DK, LANES), 1) < HALF, high, factor - high).astype(BF)
 
 
-def gate_near_kernel(q_ref, x0_ref, x1_ref, x2_ref, wg_ref, wu_ref, g_ref, u_ref):
+def mark_kernel(q_ref, out_ref):
+    out_ref[...] = jnp.full(out_ref.shape, q_ref[0], jnp.int32)
+
+
+def gate_kernel(
+    q_ref, mark_ref, x0_ref, x1_ref, x2_ref, t3_ref, b3_ref, wg_ref, wu_ref,
+    hid_ref, to_gate_ref, to_up_ref,
+):
+    far = jnp.concatenate([t3_ref[...], b3_ref[...]], axis=0)
     g = u = None
-    for n, ref in enumerate((x0_ref, x1_ref, x2_ref)):
+    for n, x in enumerate((x0_ref[...], x1_ref[...], x2_ref[...], far)):
         rows = quarter_rows(q_ref[n])
-        x = ref[...]
         g1, u1 = dot(x, wg_ref[rows, :], 1, 0), dot(x, wu_ref[rows, :], 1, 0)
         g, u = (g1, u1) if g is None else (g + g1, u + u1)
-    g_ref[...] = g
-    u_ref[...] = u
-
-
-def gate_far_kernel(
-    q_ref, g_ref, u_ref, t3_ref, b3_ref, wg_ref, wu_ref, hid_ref, to_gate_ref, to_up_ref
-):
-    rows = quarter_rows(q_ref[3])
-    x = jnp.concatenate([t3_ref[...], b3_ref[...]], axis=0)
-    g = g_ref[...] + dot(x, wg_ref[rows, :], 1, 0)
-    u = u_ref[...] + dot(x, wu_ref[rows, :], 1, 0)
     sig = jax.nn.sigmoid(g)
     silu = g * sig
     hid_ref[...] = (silu * u).astype(BF)
@@ -489,12 +485,12 @@
     b3 = lax.ppermute(b2, "tp", to_left)
     half_type = sds((SLOTS, FF), F32)
     part_type = sds((SLOTS // 2, QUART), BF)
-    g, u = run(gate_near_kernel, (half_type,) * 2, (x0, x1, x2, wg, wu), flops=8e8)
+    mark = run(mark_kernel, sds((8, LANES), jnp.int32), (), flops=1e4)
     hidden, to_gate, to_up = run(
-        gate_far_kernel,
+        gate_kernel,
         (sds((SLOTS, FF), BF), half_type, half_type),
-        (g, u, xt3, xb3, wg, wu),
-        flops=3e8,
+        (mark, x0, x1, x2, xt3, xb3, wg, wu),
+        flops=1.1e9,
     )
     h = run(near_kernel, half_type, (y0, t1, b1, t2, b2, wd), flops=4e8)
     gate_up, p_top, p_bottom = run(

time: 186 us -> 185 us (level)
    unnamed x34 -> x36, local copies, waits for them, and re-layouts: 2.47 us -> 3.88 us
  transfers between devices with their start and end apart: 30 -> 30, of which waited for: 18 -> 19; matrix products, arithmetic and copies ran while one was open for 1% -> 1% of each run, Pallas kernels for 12% -> 12%
where the time goes in v6:
time: 185 us; the launch traced here: 183 us
  starting transfers between devices  56.2 us (30%)
  waiting for transfers between devices  50.4 us (27%)
  blocking collectives  38 us (21%)
  Pallas kernels  31.5 us (17%)
  local copies, waits for them, and re-layouts  6.45 us (3%)
    pallas_call x20, Pallas kernels, call(): pl.pallas_call(kernel, out_shape=out_shape, grid_spec=pltpu.PrefetchScala...  30.2 us
    all_to_all x1, blocking collectives, between_chips(): lax.all_to_all(rows.reshape(CHIPS, 2 * CAP, QUART), 'sp', 0, 0, tiled=Tru...  22.7 us
    all_to_all x2, starting transfers between devices, between_chips(): lax.all_to_all(rows.reshape(CHIPS, 2 * CAP, QUART), 'sp', 0, 0, tiled=Tru...  16.1 us
    all_to_all x1, blocking collectives, exchange(): lax.all_to_all(rows.reshape(8, 16, width), 'sp', 0, 0, tiled=True, axis_i...  15.3 us
    all_to_all x2, waiting for transfers between devices, between_chips(): lax.all_to_all(rows.reshape(CHIPS, 2 * CAP, QUART), 'sp', 0, 0, tiled=Tru...  12.9 us
    ppermute x1, waiting for transfers between devices, per_device(): x1 = lax.ppermute(x0, 'tp', to_right)  10.5 us
    all_to_all x2, starting transfers between devices, exchange(): lax.all_to_all(rows.reshape(8, 16, width), 'sp', 0, 0, tiled=True, axis_i...  6.94 us
    ppermute x3, starting transfers between devices, per_device(): adds = [lax.ppermute(tiles[k], 'sp', along_y(k)) for k in (2, 1, 3)]  6.84 us
  transfers between devices with their start and end apart: 30, of which 19 were waited for; matrix products, arithmetic and copies ran while one was open for 1% of the time, Pallas kernels for 12%

profile of v6, /device:TPU:2, one launch (start us, length us, event | category | flops | bytes accessed | tf_op | source)
XLA Modules:
  0.0 183.4 jit_solution(789340438856574217)
XLA Ops:
  4.9 11.5 %all-to-all-start = ((bf16[32,16,512]{2,1,0:T(8,128)(2,1)}), bf16[32,16,512]{2,1,0:T(8,128)(2,1)S(1)}, u32[]{:S(2)}, u32[]{:S(2)}) async-start(bf16[32,16,512]{2,1,0:T(8,128)(2,1)} %bitcast.1), calls=%async_computation | async-start | bytes 1048576 | tf_op jit(solution)/shard_map/all_to_all | solution.py:434
  16.4 2.4 %shard_map.199 = (bf16[256,512]{1,0:T(8,128)(2,1)S(1)}, bf16[256,512]{1,0:T(8,128)(2,1)S(1)}, bf16[128,384]{1,0:T(8,128)(2,1)S(1)}, f32[128,128]{1,0:T(8,128)S(1)}, f32[128,128]{1,0:T(8,128)S(1)}) custom-call(s32[7]{0:T(128)S(1)} %dynamic_slice.3.q_ref, s32[2,128]{1,0:T(2,128)S(1)} %get-tuple-element.63.slot_ref, f32[2,128]{1,0:T(2,128)} %bitcast.53, ...), custom_call_target="tpu_custom_call" | custom-call | flops 300000000 | bytes 1607680 | tf_op jit(solution)/shard_map/pallas_call | solution.py:53
  20.6 1.5 collective-permute-done.1.got_ref
  23.5 10.9 %all-to-all-done = bf16[32,16,512]{2,1,0:T(8,128)(2,1)S(1)} async-done(((bf16[32,16,512]{2,1,0:T(8,128)(2,1)}), bf16[32,16,512]{2,1,0:T(8,128)(2,1)S(1)}, u32[]{:S(2)}, u32[]{:S(2)}) %all-to-all-start) | async-done | bytes 524320 | tf_op jit(solution)/shard_map/all_to_all | solution.py:434
  34.5 4.6 %all-to-all-start.1 = ((bf16[32,16,512]{2,1,0:T(8,128)(2,1)}), bf16[32,16,512]{2,1,0:T(8,128)(2,1)S(1)}, u32[]{:S(2)}, u32[]{:S(2)}) async-start(bf16[32,16,512]{2,1,0:T(8,128)(2,1)} %bitcast.42), calls=%async_computation.1 | async-start | bytes 1048576 | tf_op jit(solution)/shard_map/all_to_all | solution.py:434
  39.1 1.6 collective-permute-start.8
  41.2 10.5 %collective-permute-done.8.x1_ref = bf16[512,512]{1,0:T(8,128)(2,1)S(1)} collective-permute-done((bf16[512,512]{1,0:T(8,128)(2,1)S(1)}, bf16[512,512]{1,0:T(8,128)(2,1)S(1)}, u32[]{:S(2)}, u32[]{:S(2)}) %collective-permute-start.8) | collective-permute-done | bytes 524320 | tf_op jit(solution)/shard_map/ppermute | solution.py:474
  54.1 2.0 %all-to-all-done.1 = bf16[32,16,512]{2,1,0:T(8,128)(2,1)S(1)} async-done(((bf16[32,16,512]{2,1,0:T(8,128)(2,1)}), bf16[32,16,512]{2,1,0:T(8,128)(2,1)S(1)}, u32[]{:S(2)}, u32[]{:S(2)}) %all-to-all-start.1) | async-done | bytes 524320 | tf_op jit(solution)/shard_map/all_to_all | solution.py:434
  56.1 1.6 collective-permute-start.2
  59.2 1.8 collective-permute-start.11
  61.9 3.0 %collective-permute-start.4 = (bf16[256,512]{1,0:T(8,128)(2,1)S(1)}, bf16[256,512]{1,0:T(8,128)(2,1)S(1)}, u32[]{:S(2)}, u32[]{:S(2)}) collective-permute-start(bf16[256,512]{1,0:T(8,128)(2,1)S(1)} %bitcast.48), channel_id=1, source_target_pairs={{0,3},{1,0},{2,1},{3,2},{4,7},{5,4},{6,5},{7,6},{8,11},{9,8},{10,9... | collective-permute-start | bytes 786440 | tf_op jit(solution)/shard_map/ppermute | solution.py:483
  64.9 2.7 %collective-permute-done.2.t1_ref = bf16[256,512]{1,0:T(8,128)(2,1)S(1)} collective-permute-done((bf16[256,512]{1,0:T(8,128)(2,1)S(1)}, bf16[256,512]{1,0:T(8,128)(2,1)S(1)}, u32[]{:S(2)}, u32[]{:S(2)}) %collective-permute-start.2) | collective-permute-done | bytes 262176 | tf_op jit(solution)/shard_map/ppermute | solution.py:480
  73.5 2.9 %shard_map.203 = (bf16[512,256]{1,0:T(8,128)(2,1)S(1)}, f32[512,256]{1,0:T(8,128)S(1)}, f32[512,256]{1,0:T(8,128)S(1)}) custom-call(s32[7]{0:T(128)S(1)} %dynamic_slice.3.q_ref, s32[8,128]{1,0:T(8,128)S(1)} %shard_map.202.mark_ref, bf16[512,512]{1,0:T(8,128)(2,1)S(1)} %bitcast.39, bf16[512,512]{1,0:T(8,128)(2,1)S(1)} %copy-done.5, ...), custom_call_target="tpu_custom_call" | custom-call | flops 1100000000 | bytes 5509120 | tf_op jit(solution)/shard_map/pallas_call | solution.py:53
  77.8 1.6 collective-permute-done.7.b3_ref
  84.1 1.8 collective-permute-start.15
  86.2 2.9 %shard_map.205 = (f32[256,2048]{1,0:T(8,128)}, bf16[512,512]{1,0:T(8,128)(2,1)S(1)}) custom-call(s32[7]{0:T(128)S(1)} %dynamic_slice.3.q_ref, bf16[512,512]{1,0:T(8,128)(2,1)S(1)} %bitcast.33, bf16[256,512]{1,0:T(8,128)(2,1)S(1)} %collective-permute-done.2.t1_ref, bf16[256,512]{1,0:T(8,128)(2,1)S(1)} %collective-permute-done.3.b1_ref, ...), custom_call_target="tpu_custom_call" | custom-call | flops 800000000 | bytes 7602176 | tf_op jit(solution)/shard_map/pallas_call | solution.py:53
  92.7 4.9 %shard_map.206 = (f32[2048,256]{1,0:T(8,128)}, f32[2048,256]{1,0:T(8,128)}) custom-call(s32[7]{0:T(128)S(1)} %dynamic_slice.3.q_ref, bf16[512,512]{1,0:T(8,128)(2,1)S(1)} %bitcast.40, bf16[512,512]{1,0:T(8,128)(2,1)S(1)} %copy-done.6, bf16[512,512]{1,0:T(8,128)(2,1)} %collective-permute-done.9.x2_ref, ...), custom_call_target="tpu_custom_call" | custom-call | flops 1100000000 | bytes 6815744 | tf_op jit(solution)/shard_map/pallas_call | solution.py:53
  99.0 22.7 %all_to_all.30 = bf16[32,16,512]{2,1,0:T(8,128)(2,1)S(1)} all-to-all(bf16[32,16,512]{2,1,0:T(8,128)(2,1)S(1)} %bitcast.41), channel_id=1, replica_groups={{0,8,16,24,32,40,48,56,64,72,80,88,96,104,112,120,128,136,144,152,160,1..., dimensions={0} | all-to-all | bytes 1048576 | tf_op jit(solution)/shard_map/all_to_all | solution.py:434
  124.2 1.5 collective-permute-start.19
  125.7 1.9 %collective-permute-start.20 = (bf16[128,512]{1,0:T(8,128)(2,1)S(1)}, bf16[128,512]{1,0:T(8,128)(2,1)S(1)}, u32[]{:S(2)}, u32[]{:S(2)}) collective-permute-start(bf16[128,512]{1,0:T(8,128)(2,1)S(1)} %shard_map.210.m0_ref), channel_id=1, source_target_pairs={{0,3},{1,0},{2,1},{3,2},{4,7},{5,4},{6,5},{7,6},{8,11},{9,8},{10,9... | collective-permute-start | bytes 393224 | tf_op jit(solution)/shard_map/ppermute | solution.py:538
  127.7 2.6 %collective-permute-start.21 = (bf16[128,512]{1,0:T(8,128)(2,1)S(1)}, bf16[128,512]{1,0:T(8,128)(2,1)S(1)}, u32[]{:S(2)}, u32[]{:S(2)}) collective-permute-start(bf16[128,512]{1,0:T(8,128)(2,1)S(1)} %shard_map.210.m0_ref), channel_id=1, source_target_pairs={{0,2},{1,3},{2,0},{3,1},{4,6},{5,7},{6,4},{7,5},{8,10},{9,11},{10,... | collective-permute-start | bytes 393224 | tf_op jit(solution)/shard_map/ppermute | solution.py:536
  132.3 4.0 %collective-permute-done.21.m3_ref = bf16[128,512]{1,0:T(8,128)(2,1)S(1)} collective-permute-done((bf16[128,512]{1,0:T(8,128)(2,1)S(1)}, bf16[128,512]{1,0:T(8,128)(2,1)S(1)}, u32[]{:S(2)}, u32[]{:S(2)}) %collective-permute-start.21) | collective-permute-done | bytes 131104 | tf_op jit(solution)/shard_map/ppermute | solution.py:536
  137.4 1.9 %shard_map.211 = (f32[128,256]{1,0:T(8,128)S(1)}, bf16[128,640]{1,0:T(8,128)(2,1)}) custom-call(s32[7]{0:T(128)S(1)} %dynamic_slice.3.q_ref, bf16[128,512]{1,0:T(8,128)(2,1)S(1)} %shard_map.210.m0_ref, bf16[128,512]{1,0:T(8,128)(2,1)S(1)} %collective-permute-done.19.m1_ref, bf16[128,512]{1,0:T(8,128)(2,1)S(1)} %collective-permute-done.20.m2_ref, ...), custom_call_target="tpu_custom_call" | custom-call | flops 200000000 | bytes 2031616 | tf_op jit(solution)/shard_map/pallas_call | solution.py:53
  139.4 3.6 %all-to-all-start.3 = ((bf16[8,16,640]{2,1,0:T(8,128)(2,1)}), bf16[8,16,640]{2,1,0:T(8,128)(2,1)S(1)}, u32[]{:S(2)}, u32[]{:S(2)}) async-start(bf16[8,16,640]{2,1,0:T(8,128)(2,1)} %bitcast.17), calls=%async_computation.3 | async-start | bytes 327680 | tf_op jit(solution)/shard_map/all_to_all | solution.py:417
  143.8 3.6 %collective-permute-start.23 = (bf16[128,512]{1,0:T(8,128)(2,1)S(1)}, bf16[128,512]{1,0:T(8,128)(2,1)S(1)}, u32[]{:S(2)}, u32[]{:S(2)}) collective-permute-start(bf16[128,512]{1,0:T(8,128)(2,1)S(1)} %get-tuple-element.96), channel_id=1, source_target_pairs={{0,16},{4,20},{8,24},{12,28},{16,0},{20,4},{24,8},{28,12},{32,48},... | collective-permute-start | bytes 393224 | tf_op jit(solution)/shard_map/ppermute | solution.py:550
  147.9 2.7 %collective-permute-start.25 = (bf16[128,512]{1,0:T(8,128)(2,1)S(1)}, bf16[128,512]{1,0:T(8,128)(2,1)S(1)}, u32[]{:S(2)}, u32[]{:S(2)}) collective-permute-start(bf16[128,512]{1,0:T(8,128)(2,1)S(1)} %get-tuple-element.98), channel_id=1, source_target_pairs={{0,24},{4,28},{8,0},{12,4},{16,8},{20,12},{24,16},{28,20},{32,56},... | collective-permute-start | bytes 393224 | tf_op jit(solution)/shard_map/ppermute | solution.py:550
  150.6 2.2 %collective-permute-done.23.r1_ref = bf16[128,512]{1,0:T(8,128)(2,1)S(1)} collective-permute-done((bf16[128,512]{1,0:T(8,128)(2,1)S(1)}, bf16[128,512]{1,0:T(8,128)(2,1)S(1)}, u32[]{:S(2)}, u32[]{:S(2)}) %collective-permute-start.23) | collective-permute-done | bytes 131104 | tf_op jit(solution)/shard_map/ppermute | solution.py:550
  152.8 2.2 %collective-permute-done.24.r2_ref = bf16[128,512]{1,0:T(8,128)(2,1)S(1)} collective-permute-done((bf16[128,512]{1,0:T(8,128)(2,1)S(1)}, bf16[128,512]{1,0:T(8,128)(2,1)S(1)}, u32[]{:S(2)}, u32[]{:S(2)}) %collective-permute-start.24) | collective-permute-done | bytes 131104 | tf_op jit(solution)/shard_map/ppermute | solution.py:550
  155.8 15.3 %all_to_all.31 = bf16[8,16,1152]{2,1,0:T(8,128)(2,1)S(1)} all-to-all(bf16[8,16,1152]{2,1,0:T(8,128)(2,1)S(1)} %bitcast.45), channel_id=1, replica_groups={{0,32,64,96,128,160,192,224},{4,36,68,100,132,164,196,228},{8,40,72,104..., dimensions={0} | all-to-all | bytes 589824 | tf_op jit(solution)/shard_map/all_to_all | solution.py:417
  172.4 3.4 %all-to-all-start.5 = ((bf16[8,16,512]{2,1,0:T(8,128)(2,1)}), bf16[8,16,512]{2,1,0:T(8,128)(2,1)S(1)}, u32[]{:S(2)}, u32[]{:S(2)}) async-start(bf16[8,16,512]{2,1,0:T(8,128)(2,1)} %bitcast.21), calls=%async_computation.5 | async-start | bytes 262144 | tf_op jit(solution)/shard_map/all_to_all | solution.py:417
  177.2 4.6 %all-to-all-done.5 = bf16[8,16,512]{2,1,0:T(8,128)(2,1)S(1)} async-done(((bf16[8,16,512]{2,1,0:T(8,128)(2,1)}), bf16[8,16,512]{2,1,0:T(8,128)(2,1)S(1)}, u32[]{:S(2)}, u32[]{:S(2)}) %all-to-all-start.5) | async-done | bytes 131104 | tf_op jit(solution)/shard_map/all_to_all | solution.py:417
  181.8 1.6 shard_map.217
  (92 shorter events, 40.6 us)
Async XLA Ops:
  1.9 1.6 collective-permute-start
  4.9 29.6 %all-to-all-start = ((bf16[32,16,512]{2,1,0:T(8,128)(2,1)}), bf16[32,16,512]{2,1,0:T(8,128)(2,1)S(1)}, u32[]{:S(2)}, u32[]{:S(2)}) async-start(bf16[32,16,512]{2,1,0:T(8,128)(2,1)} %bitcast.1), calls=%async_computation | async-start | bytes 1048576 | tf_op jit(solution)/shard_map/all_to_all | solution.py:434
  20.6 1.5 collective-permute-start.1
  22.2 50.3 %copy-start = (bf16[1,2048,256]{2,1,0:T(8,128)(2,1)S(1)}, bf16[1,2048,256]{2,1,0:T(8,128)(2,1)}, u32[]{:S(2)}) copy-start(bf16[1,2048,256]{2,1,0:T(8,128)(2,1)} %param.18) | copy-start | bytes 3145732
  22.2 50.3 %copy-start.1 = (bf16[1,2048,256]{2,1,0:T(8,128)(2,1)S(1)}, bf16[1,2048,256]{2,1,0:T(8,128)(2,1)}, u32[]{:S(2)}) copy-start(bf16[1,2048,256]{2,1,0:T(8,128)(2,1)} %param.19) | copy-start | bytes 3145732
  34.5 21.6 %all-to-all-start.1 = ((bf16[32,16,512]{2,1,0:T(8,128)(2,1)}), bf16[32,16,512]{2,1,0:T(8,128)(2,1)S(1)}, u32[]{:S(2)}, u32[]{:S(2)}) async-start(bf16[32,16,512]{2,1,0:T(8,128)(2,1)} %bitcast.42), calls=%async_computation.1 | async-start | bytes 1048576 | tf_op jit(solution)/shard_map/all_to_all | solution.py:434
  39.1 12.6 %collective-permute-start.8 = (bf16[512,512]{1,0:T(8,128)(2,1)S(1)}, bf16[512,512]{1,0:T(8,128)(2,1)S(1)}, u32[]{:S(2)}, u32[]{:S(2)}) collective-permute-start(bf16[512,512]{1,0:T(8,128)(2,1)S(1)} %bitcast.37), channel_id=1, source_target_pairs={{0,1},{1,2},{2,3},{3,0},{4,5},{5,6},{6,7},{7,4},{8,9},{9,10},{10,1... | collective-permute-start | bytes 1572872 | tf_op jit(solution)/shard_map/ppermute | solution.py:474
  40.6 17.6 %collective-permute-start.9 = (bf16[512,512]{1,0:T(8,128)(2,1)S(1)}, bf16[512,512]{1,0:T(8,128)(2,1)}, u32[]{:S(2)}, u32[]{:S(2)}) collective-permute-start(bf16[512,512]{1,0:T(8,128)(2,1)S(1)} %bitcast.38), channel_id=1, source_target_pairs={{0,3},{1,0},{2,1},{3,2},{4,7},{5,4},{6,5},{7,6},{8,11},{9,8},{10,9... | collective-permute-start | bytes 1572872 | tf_op jit(solution)/shard_map/ppermute | solution.py:475
  52.6 9.4 %collective-permute-start.10 = (bf16[256,512]{1,0:T(8,128)(2,1)}, bf16[256,512]{1,0:T(8,128)(2,1)S(1)}, u32[]{:S(2)}, u32[]{:S(2)}) collective-permute-start(bf16[256,512]{1,0:T(8,128)(2,1)} %slice.30), channel_id=1, source_target_pairs={{0,1},{1,2},{2,3},{3,0},{4,5},{5,6},{6,7},{7,4},{8,9},{9,10},{10,1... | collective-permute-start | bytes 786440 | tf_op jit(solution)/shard_map/ppermute | solution.py:476
  56.1 11.5 %collective-permute-start.2 = (bf16[256,512]{1,0:T(8,128)(2,1)S(1)}, bf16[256,512]{1,0:T(8,128)(2,1)S(1)}, u32[]{:S(2)}, u32[]{:S(2)}) collective-permute-start(bf16[256,512]{1,0:T(8,128)(2,1)S(1)} %bitcast.47), channel_id=1, source_target_pairs={{0,1},{1,2},{2,3},{3,0},{4,5},{5,6},{6,7},{7,4},{8,9},{9,10},{10,1... | collective-permute-start | bytes 786440 | tf_op jit(solution)/shard_map/ppermute | solution.py:480
  57.7 11.4 %collective-permute-start.5 = (bf16[256,512]{1,0:T(8,128)(2,1)S(1)}, bf16[256,512]{1,0:T(8,128)(2,1)S(1)}, u32[]{:S(2)}, u32[]{:S(2)}) collective-permute-start(bf16[256,512]{1,0:T(8,128)(2,1)S(1)} %bitcast.49), channel_id=1, source_target_pairs={{0,3},{1,0},{2,1},{3,2},{4,7},{5,4},{6,5},{7,6},{8,11},{9,8},{10,9... | collective-permute-start | bytes 786440 | tf_op jit(solution)/shard_map/ppermute | solution.py:481
  59.2 13.3 %collective-permute-start.11 = (bf16[256,512]{1,0:T(8,128)(2,1)S(1)}, bf16[256,512]{1,0:T(8,128)(2,1)S(1)}, u32[]{:S(2)}, u32[]{:S(2)}) collective-permute-start(bf16[256,512]{1,0:T(8,128)(2,1)S(1)} %slice.31), channel_id=1, source_target_pairs={{0,3},{1,0},{2,1},{3,2},{4,7},{5,4},{6,5},{7,6},{8,11},{9,8},{10,9... | collective-permute-start | bytes 786440 | tf_op jit(solution)/shard_map/ppermute | solution.py:477
  61.0 15.4 %collective-permute-start.3 = (bf16[256,512]{1,0:T(8,128)(2,1)S(1)}, bf16[256,512]{1,0:T(8,128)(2,1)S(1)}, u32[]{:S(2)}, u32[]{:S(2)}) collective-permute-start(bf16[256,512]{1,0:T(8,128)(2,1)S(1)} %bitcast.50), channel_id=1, source_target_pairs={{0,1},{1,2},{2,3},{3,0},{4,5},{5,6},{6,7},{7,4},{8,9},{9,10},{10,1... | collective-permute-start | bytes 786440 | tf_op jit(solution)/shard_map/ppermute | solution.py:482
  61.9 14.7 %collective-permute-start.4 = (bf16[256,512]{1,0:T(8,128)(2,1)S(1)}, bf16[256,512]{1,0:T(8,128)(2,1)S(1)}, u32[]{:S(2)}, u32[]{:S(2)}) collective-permute-start(bf16[256,512]{1,0:T(8,128)(2,1)S(1)} %bitcast.48), channel_id=1, source_target_pairs={{0,3},{1,0},{2,1},{3,2},{4,7},{5,4},{6,5},{7,6},{8,11},{9,8},{10,9... | collective-permute-start | bytes 786440 | tf_op jit(solution)/shard_map/ppermute | solution.py:483
  67.6 10.2 %collective-permute-start.6 = (bf16[256,512]{1,0:T(8,128)(2,1)S(1)}, bf16[256,512]{1,0:T(8,128)(2,1)S(1)}, u32[]{:S(2)}, u32[]{:S(2)}) collective-permute-start(bf16[256,512]{1,0:T(8,128)(2,1)S(1)} %collective-permute-done.2.t1_ref), channel_id=1, source_target_pairs={{0,1},{1,2},{2,3},{3,0},{4,5},{5,6},{6,7},{7,4},{8,9},{9,10},{10,1... | collective-permute-start | bytes 786440 | tf_op jit(solution)/shard_map/ppermute | solution.py:484
  69.1 10.3 %collective-permute-start.7 = (bf16[256,512]{1,0:T(8,128)(2,1)S(1)}, bf16[256,512]{1,0:T(8,128)(2,1)S(1)}, u32[]{:S(2)}, u32[]{:S(2)}) collective-permute-start(bf16[256,512]{1,0:T(8,128)(2,1)S(1)} %collective-permute-done.5.b2_ref), channel_id=1, source_target_pairs={{0,3},{1,0},{2,1},{3,2},{4,7},{5,4},{6,5},{7,6},{8,11},{9,8},{10,9... | collective-permute-start | bytes 786440 | tf_op jit(solution)/shard_map/ppermute | solution.py:485
  80.7 9.3 %collective-permute-start.12 = (bf16[256,512]{1,0:T(8,128)(2,1)S(1)}, bf16[256,512]{1,0:T(8,128)(2,1)S(1)}, u32[]{:S(2)}, u32[]{:S(2)}) collective-permute-start(bf16[256,512]{1,0:T(8,128)(2,1)S(1)} %get-tuple-element.71), channel_id=1, source_target_pairs={{0,1},{1,2},{2,3},{3,0},{4,5},{5,6},{6,7},{7,4},{8,9},{9,10},{10,1... | collective-permute-start | bytes 786440 | tf_op jit(solution)/shard_map/ppermute | solution.py:502
  81.9 8.0 %collective-permute-start.13 = (bf16[256,512]{1,0:T(8,128)(2,1)S(1)}, bf16[256,512]{1,0:T(8,128)(2,1)S(1)}, u32[]{:S(2)}, u32[]{:S(2)}) collective-permute-start(bf16[256,512]{1,0:T(8,128)(2,1)S(1)} %get-tuple-element.85), channel_id=1, source_target_pairs={{0,3},{1,0},{2,1},{3,2},{4,7},{5,4},{6,5},{7,6},{8,11},{9,8},{10,9... | collective-permute-start | bytes 786440 | tf_op jit(solution)/shard_map/ppermute | solution.py:503
  84.1 13.5 %collective-permute-start.15 = (bf16[256,512]{1,0:T(8,128)(2,1)S(1)}, bf16[256,512]{1,0:T(8,128)(2,1)S(1)}, u32[]{:S(2)}, u32[]{:S(2)}) collective-permute-start(bf16[256,512]{1,0:T(8,128)(2,1)S(1)} %get-tuple-element.87), channel_id=1, source_target_pairs={{0,3},{1,0},{2,1},{3,2},{4,7},{5,4},{6,5},{7,6},{8,11},{9,8},{10,9... | collective-permute-start | bytes 786440 | tf_op jit(solution)/shard_map/ppermute | solution.py:506
  85.9 11.7 %collective-permute-start.16 = (bf16[256,512]{1,0:T(8,128)(2,1)S(1)}, bf16[256,512]{1,0:T(8,128)(2,1)S(1)}, u32[]{:S(2)}, u32[]{:S(2)}) collective-permute-start(bf16[256,512]{1,0:T(8,128)(2,1)S(1)} %get-tuple-element.88), channel_id=1, source_target_pairs={{0,1},{1,2},{2,3},{3,0},{4,5},{5,6},{6,7},{7,4},{8,9},{9,10},{10,1... | collective-permute-start | bytes 786440 | tf_op jit(solution)/shard_map/ppermute | solution.py:505
  90.6 7.0 %collective-permute-start.14 = (bf16[256,512]{1,0:T(8,128)(2,1)S(1)}, bf16[256,512]{1,0:T(8,128)(2,1)S(1)}, u32[]{:S(2)}, u32[]{:S(2)}) collective-permute-start(bf16[256,512]{1,0:T(8,128)(2,1)S(1)} %get-tuple-element.86), channel_id=1, source_target_pairs={{0,1},{1,2},{2,3},{3,0},{4,5},{5,6},{6,7},{7,4},{8,9},{9,10},{10,1... | collective-permute-start | bytes 786440 | tf_op jit(solution)/shard_map/ppermute | solution.py:515
  91.3 7.0 %collective-permute-start.17 = (bf16[256,512]{1,0:T(8,128)(2,1)S(1)}, bf16[256,512]{1,0:T(8,128)(2,1)S(1)}, u32[]{:S(2)}, u32[]{:S(2)}) collective-permute-start(bf16[256,512]{1,0:T(8,128)(2,1)S(1)} %get-tuple-element.89), channel_id=1, source_target_pairs={{0,3},{1,0},{2,1},{3,2},{4,7},{5,4},{6,5},{7,6},{8,11},{9,8},{10,9... | collective-permute-start | bytes 786440 | tf_op jit(solution)/shard_map/ppermute | solution.py:516
  121.8 1.6 collective-permute-start.18
  124.2 7.3 %collective-permute-start.19 = (bf16[128,512]{1,0:T(8,128)(2,1)S(1)}, bf16[128,512]{1,0:T(8,128)(2,1)S(1)}, u32[]{:S(2)}, u32[]{:S(2)}) collective-permute-start(bf16[128,512]{1,0:T(8,128)(2,1)S(1)} %shard_map.210.m0_ref), channel_id=1, source_target_pairs={{0,1},{1,2},{2,3},{3,0},{4,5},{5,6},{6,7},{7,4},{8,9},{9,10},{10,1... | collective-permute-start | bytes 393224 | tf_op jit(solution)/shard_map/ppermute | solution.py:537
  125.7 6.5 %collective-permute-start.20 = (bf16[128,512]{1,0:T(8,128)(2,1)S(1)}, bf16[128,512]{1,0:T(8,128)(2,1)S(1)}, u32[]{:S(2)}, u32[]{:S(2)}) collective-permute-start(bf16[128,512]{1,0:T(8,128)(2,1)S(1)} %shard_map.210.m0_ref), channel_id=1, source_target_pairs={{0,3},{1,0},{2,1},{3,2},{4,7},{5,4},{6,5},{7,6},{8,11},{9,8},{10,9... | collective-permute-start | bytes 393224 | tf_op jit(solution)/shard_map/ppermute | solution.py:538
  127.7 8.6 %collective-permute-start.21 = (bf16[128,512]{1,0:T(8,128)(2,1)S(1)}, bf16[128,512]{1,0:T(8,128)(2,1)S(1)}, u32[]{:S(2)}, u32[]{:S(2)}) collective-permute-start(bf16[128,512]{1,0:T(8,128)(2,1)S(1)} %shard_map.210.m0_ref), channel_id=1, source_target_pairs={{0,2},{1,3},{2,0},{3,1},{4,6},{5,7},{6,4},{7,5},{8,10},{9,11},{10,... | collective-permute-start | bytes 393224 | tf_op jit(solution)/shard_map/ppermute | solution.py:536
  137.3 5.6 %collective-permute-start.22 = (bf16[1024,256]{1,0:T(8,128)(2,1)S(1)}, bf16[1024,256]{1,0:T(8,128)(2,1)S(1)}, u32[]{:S(2)}, u32[]{:S(2)}) collective-permute-start(bf16[1024,256]{1,0:T(8,128)(2,1)S(1)} %get-tuple-element.94), channel_id=1, source_target_pairs={{0,4},{4,0},{8,12},{12,8},{16,20},{20,16},{24,28},{28,24},{32,36},... | collective-permute-start | bytes 1572872 | tf_op jit(solution)/shard_map/ppermute | solution.py:548
  139.4 11.2 %all-to-all-start.3 = ((bf16[8,16,640]{2,1,0:T(8,128)(2,1)}), bf16[8,16,640]{2,1,0:T(8,128)(2,1)S(1)}, u32[]{:S(2)}, u32[]{:S(2)}) async-start(bf16[8,16,640]{2,1,0:T(8,128)(2,1)} %bitcast.17), calls=%async_computation.3 | async-start | bytes 327680 | tf_op jit(solution)/shard_map/all_to_all | solution.py:417
  143.8 9.0 %collective-permute-start.23 = (bf16[128,512]{1,0:T(8,128)(2,1)S(1)}, bf16[128,512]{1,0:T(8,128)(2,1)S(1)}, u32[]{:S(2)}, u32[]{:S(2)}) collective-permute-start(bf16[128,512]{1,0:T(8,128)(2,1)S(1)} %get-tuple-element.96), channel_id=1, source_target_pairs={{0,16},{4,20},{8,24},{12,28},{16,0},{20,4},{24,8},{28,12},{32,48},... | collective-permute-start | bytes 393224 | tf_op jit(solution)/shard_map/ppermute | solution.py:550
  147.4 7.7 %collective-permute-start.24 = (bf16[128,512]{1,0:T(8,128)(2,1)S(1)}, bf16[128,512]{1,0:T(8,128)(2,1)S(1)}, u32[]{:S(2)}, u32[]{:S(2)}) collective-permute-start(bf16[128,512]{1,0:T(8,128)(2,1)S(1)} %get-tuple-element.97), channel_id=1, source_target_pairs={{0,8},{4,12},{8,16},{12,20},{16,24},{20,28},{24,0},{28,4},{32,40},... | collective-permute-start | bytes 393224 | tf_op jit(solution)/shard_map/ppermute | solution.py:550
  147.9 7.1 %collective-permute-start.25 = (bf16[128,512]{1,0:T(8,128)(2,1)S(1)}, bf16[128,512]{1,0:T(8,128)(2,1)S(1)}, u32[]{:S(2)}, u32[]{:S(2)}) collective-permute-start(bf16[128,512]{1,0:T(8,128)(2,1)S(1)} %get-tuple-element.98), channel_id=1, source_target_pairs={{0,24},{4,28},{8,0},{12,4},{16,8},{20,12},{24,16},{28,20},{32,56},... | collective-permute-start | bytes 393224 | tf_op jit(solution)/shard_map/ppermute | solution.py:550
  172.4 9.4 %all-to-all-start.5 = ((bf16[8,16,512]{2,1,0:T(8,128)(2,1)}), bf16[8,16,512]{2,1,0:T(8,128)(2,1)S(1)}, u32[]{:S(2)}, u32[]{:S(2)}) async-start(bf16[8,16,512]{2,1,0:T(8,128)(2,1)} %bitcast.21), calls=%async_computation.5 | async-start | bytes 262144 | tf_op jit(solution)/shard_map/all_to_all | solution.py:417
  (16 other events, 301.9 us)
